TPU v7x, 256 devices: a whole 4x4x8 slice. The times are simulated.
256 devices in a mesh: sp: 16 (over y, x), dp: 16 (over z, core).
Axes of the slice: x: 4, y: 4, z: 8, core: 2. Of those that a mesh axis runs over, the one named last changes fastest.
Arguments:
- value_half: bfloat16 [16, 4096, 2048], P('dp', 'sp'), may hold values from -6 to 6
- gate_half: bfloat16 [16, 4096, 2048], P('dp', 'sp'), may hold values from -6 to 6
- upstream: bfloat16 [16, 4096, 2048], P('dp', 'sp'), may hold values from -6 to 6
- conv_taps: float32 [31, 2048], P(None, 'sp'), may hold values from -1 to 1
- norm_gain: float32 [2048], replicated, may hold values from 0.1 to 1.9
- out_weight: bfloat16 [2048, 2048], P('dp'), may hold values from -0.125 to 0.125
Outputs:
- grad_value: bfloat16 [16, 4096, 2048], P('dp', 'sp')
- grad_gate: bfloat16 [16, 4096, 2048], P('dp', 'sp')
- grad_taps: float32 [31, 2048], P(None, 'sp')
- grad_gain: float32 [2048], replicated
- grad_weight: float32 [2048, 2048], P('dp')
All inputs are finite; a program needn't handle non-finite values.
Results may differ from a plain program's by a relative error of at most 0.0062.
Values may be sent and summed in bfloat16 or wider, within the bound.
No kernel may reach another device: no remote copies, remote signals or barrier semaphores. Data moves between devices by JAX's collectives and lax.ppermute only.
A program may use at most 128 MiB of HBM per device.

v0:
```python
import functools

import jax
import jax.numpy as jnp
from jax import lax
from jax.experimental import pallas as pl
from jax.experimental.pallas import tpu as pltpu
from jax.sharding import Mesh
from jax.sharding import PartitionSpec as P

DP = ("dp_0", "dp_1")
SP = ("sp_0", "sp_1")
Y, X, Z, CORE = "sp_0", "sp_1", "dp_0", "dp_1"
NORM_EPS = 1e-05
HALO = 32
GROUP = 4
INTERPRET = False
F32, BF16 = jnp.float32, jnp.bfloat16


def call(kernel, grid, in_specs, out_specs, out_shape, scratch, flops=0, moved=0):
    return pl.pallas_call(
        kernel,
        grid_spec=pltpu.PrefetchScalarGridSpec(
            num_scalar_prefetch=1,
            grid=grid,
            in_specs=in_specs,
            out_specs=out_specs,
            scratch_shapes=scratch,
        ),
        out_shape=out_shape,
        compiler_params=pltpu.CompilerParams(
            dimension_semantics=("arbitrary",) * len(grid), vmem_limit_bytes=48 * 1024 * 1024
        ),
        cost_estimate=pl.CostEstimate(flops=flops, bytes_accessed=moved, transcendentals=0),
        interpret=INTERPRET,
    )


def shift(value, axis, amount):
    count = lax.axis_size(axis)
    return lax.ppermute(value, axis, [(i, (i + amount) % count) for i in range(count)])


def forward_kernel(ring, value, gate, halo, taps, gain, glu, act, conv, mean, inv, wide, held, total):
    step = pl.program_id(0)
    tokens = value.shape[0]
    blocks, _, lanes = held.shape

    @pl.when(step == 0)
    def _():
        total[...] = jnp.zeros_like(total)

    for i in range(GROUP):
        at = slice(i * lanes, (i + 1) * lanes)
        block = step * GROUP + i
        gated = (value[:, at].astype(F32) * jax.nn.sigmoid(gate[:, at].astype(F32))).astype(BF16)
        glu[:, at] = gated
        wide[i, pl.ds(0, HALO), :] = halo[:, at].astype(F32)
        wide[i, pl.ds(HALO, tokens), :] = gated.astype(F32)
        acc = jnp.zeros((tokens, lanes), F32)
        for j in range(31):
            acc = acc + taps[i, pl.ds(j, 1), :] * wide[i, pl.ds(2 + j, tokens), :]
        rounded = acc.astype(BF16)
        conv[:, pl.ds(pl.multiple_of(block * lanes, lanes), lanes)] = rounded
        rounded = rounded.astype(F32)
        held[block] = rounded
        total[...] += rounded

    @pl.when(step == pl.num_programs(0) - 1)
    def _():
        width = blocks * lanes
        mu = jnp.sum(total[...], axis=1, keepdims=True) / width
        mu = jnp.broadcast_to(mu, (tokens, lanes))
        mean[...] = mu

        def squares(i, acc):
            centered = held[i] - mean[...]
            return acc + centered * centered

        squared = lax.fori_loop(0, blocks, squares, jnp.zeros((tokens, lanes), F32))
        var = jnp.sum(squared, axis=1, keepdims=True) / width
        inv[...] = jnp.broadcast_to(lax.rsqrt(var + NORM_EPS), (tokens, lanes))

        def finish(i, carry):
            at = pl.ds(pl.multiple_of(i * lanes, lanes), lanes)
            scaled = (held[i] - mean[...]) * inv[...] * gain[:, at]
            act[:, at] = (scaled * jax.nn.sigmoid(scaled)).astype(BF16)
            return carry

        lax.fori_loop(0, blocks, finish, 0)


def forward(ring, value, gate, halo, taps, gain):
    tokens, width = value.shape
    lanes = width // 16
    column = lambda rows: pl.BlockSpec((rows, GROUP * lanes), lambda i, ring: (0, i))
    whole = lambda *shape: pl.BlockSpec(shape, lambda i, ring: (0,) * len(shape))
    return call(
        forward_kernel,
        (16 // GROUP,),
        [
            column(tokens),
            column(tokens),
            column(HALO),
            pl.BlockSpec((GROUP, 32, lanes), lambda i, ring: (i, 0, 0)),
            whole(1, width),
        ],
        [column(tokens), whole(tokens, width), whole(tokens, width), whole(tokens, lanes), whole(tokens, lanes)],
        [
            jax.ShapeDtypeStruct((tokens, width), BF16),
            jax.ShapeDtypeStruct((tokens, width), BF16),
            jax.ShapeDtypeStruct((tokens, width), BF16),
            jax.ShapeDtypeStruct((tokens, lanes), F32),
            jax.ShapeDtypeStruct((tokens, lanes), F32),
        ],
        [
            pltpu.VMEM((GROUP, HALO + tokens, lanes), F32),
            pltpu.VMEM((16, tokens, lanes), F32),
            pltpu.VMEM((tokens, lanes), F32),
        ],
        flops=62 * tokens * width * 100,
        moved=10 * tokens * width,
    )(ring, value, gate, halo, taps, gain)


def turn_kernel(ring, upstream, own, other):
    lanes = own.shape[1]
    core = ring[3]
    mine = upstream[:, pl.ds(pl.multiple_of(core * lanes, lanes), lanes)].astype(F32)
    own[0] = mine.T.astype(BF16)
    theirs = upstream[:, pl.ds(pl.multiple_of((1 - core) * lanes, lanes), lanes)].astype(F32)
    other[0] = theirs.T.astype(BF16)


def turn(ring, upstream):
    tokens, width = upstream.shape
    lanes = width // 16
    out = pl.BlockSpec((1, lanes, tokens), lambda i, ring: (i, 0, 0))
    shape = jax.ShapeDtypeStruct((8, lanes, tokens), BF16)
    return call(
        turn_kernel,
        (8,),
        [pl.BlockSpec((tokens, 2 * lanes), lambda i, ring: (0, i))],
        [out, out],
        [shape, shape],
        [],
        flops=tokens * width * 100,
        moved=4 * tokens * width,
    )(ring, upstream)


def outer_kernel(plan, ring, turned, turned_other, act, act_other, *outs):
    lanes = turned.shape[1]
    tokens = turned.shape[2]
    y, x = ring[0], ring[1]

    def columns(source, ky, kx):
        block = lax.rem(y + ky, 4) * 4 + lax.rem(x + kx, 4)
        return source[:, pl.ds(pl.multiple_of(block * lanes, lanes), lanes)]

    for half, k, pair, target, at in plan:
        out = outs[target]
        rows = pl.ds(4 * half, 4)
        left = turned[rows].reshape(4 * lanes, tokens)
        left_other = turned_other[rows].reshape(4 * lanes, tokens)
        spots = [(2 * pair + i, k) if half == 0 else (k, 2 * pair + i) for i in range(2)]
        right = jnp.concatenate([columns(act, *spot) for spot in spots], axis=1)
        right_other = jnp.concatenate([columns(act_other, *spot) for spot in spots], axis=1)
        product = jnp.dot(left, right, preferred_element_type=F32)
        product = product + jnp.dot(left_other, right_other, preferred_element_type=F32)
        out[at] = product[:, :lanes].astype(BF16)
        out[at + 1] = product[:, lanes:].astype(BF16)


def outer(plan, ring, turned, turned_other, act, act_other):
    tokens, width = act.shape
    lanes = width // 16
    whole = lambda *shape: pl.BlockSpec(shape, lambda i, ring: (0,) * len(shape))
    sizes = [max(at for *_, target, at in plan if target == out) + 2 for out in range(plan[-1][3] + 1)]
    return call(
        functools.partial(outer_kernel, plan),
        (1,),
        [whole(8, lanes, tokens)] * 2 + [whole(tokens, width)] * 2,
        [whole(size, 4 * lanes, lanes) for size in sizes],
        [jax.ShapeDtypeStruct((size, 4 * lanes, lanes), BF16) for size in sizes],
        [],
        flops=2 * 2 * tokens * 8 * lanes * lanes * len(plan),
        moved=8 * tokens * width,
    )(ring, turned, turned_other, act, act_other)


def add(*terms):
    return sum(term.astype(F32) for term in terms)


def tie(values, after):
    return lax.optimization_barrier((values, after))[0]


def ring_open(axis, on, back):
    return shift(on, axis, 1), shift(back, axis, -1)


def ring_sums(opened, next_low, previous_high):
    on, back = opened
    count = on.shape[0] // 2
    return add(next_low, on[:count]).astype(BF16), add(previous_high, back[:count]).astype(BF16)


def ring_close(axis, opened, sums, own_low, own_high):
    on, back = opened
    count = on.shape[0] // 2
    late_on = shift(sums[0], axis, 1)
    late_back = shift(sums[1], axis, -1)
    return add(own_low, late_on, back[count:]), add(own_high, on[count:], late_back)


def cut(low, high):
    rows = low.shape[1] // 2
    block = lambda k, h: (low, high)[k // 2][k % 2, h * rows : (h + 1) * rows]
    on = jnp.concatenate([block(2, 0), block(1, 1)]).astype(BF16)
    back = jnp.concatenate([block(2, 1), block(3, 0)]).astype(BF16)
    return (on, back), (block(1, 0), block(3, 1)), (block(0, 0), block(0, 1))


def place_kernel(ring, blocks, out):
    count, _, lanes = blocks.shape
    for i in range(count):
        block = lax.rem(ring[0] + i // 4, 4) * 4 + lax.rem(ring[1] + i % 4, 4)
        out[:, pl.ds(pl.multiple_of(block * lanes, lanes), lanes)] = blocks[i].astype(F32)


def place(ring, blocks):
    count, rows, lanes = blocks.shape
    whole = lambda *shape: pl.BlockSpec(shape, lambda i, ring: (0,) * len(shape))
    return call(
        place_kernel,
        (1,),
        [whole(count, rows, lanes)],
        whole(rows, count * lanes),
        jax.ShapeDtypeStruct((rows, count * lanes), F32),
        [],
        flops=count * rows * lanes,
        moved=6 * count * rows * lanes,
    )(ring, blocks)


def plane_row(shard):
    return jnp.stack([shard] + [shift(shard, X, -k) for k in range(1, 4)])


def plane_column(row):
    return jnp.concatenate([row] + [shift(row, Y, -k) for k in range(1, 4)])


def norm_kernel(
    ring, upstream, weight, conv, mean, inv, gain, grad, grad_head, gain_part, held, first, second
):
    step = pl.program_id(0)
    steps = held.shape[0]
    _, lanes = mean.shape
    wide = 2 * lanes

    @pl.when(step == 0)
    def _():
        first[...] = jnp.zeros_like(first)
        second[...] = jnp.zeros_like(second)

    grad_act = jnp.dot(upstream[...], weight[...], preferred_element_type=F32)
    for i in range(2):
        at = slice(i * lanes, (i + 1) * lanes)
        columns = pl.ds(pl.multiple_of((2 * step + i) * lanes, lanes), lanes)
        normed = (conv[:, columns].astype(F32) - mean[...]) * inv[...]
        scaled = normed * gain[:, at]
        sig = jax.nn.sigmoid(scaled)
        grad_scaled = grad_act[:, at] * sig * (1.0 + scaled * (1.0 - sig))
        gain_part[pl.ds(2 * step + i, 1), :] = jnp.sum(grad_scaled * normed, axis=0, keepdims=True)
        g = grad_scaled * gain[:, at]
        held[step, :, at] = g
        first[...] += g
        second[...] += g * normed

    @pl.when(step == steps - 1)
    def _():
        width = steps * wide
        first[...] = jnp.broadcast_to(jnp.sum(first[...], axis=1, keepdims=True) / width, first.shape)
        second[...] = jnp.broadcast_to(jnp.sum(second[...], axis=1, keepdims=True) / width, second.shape)

        def finish(i, carry):
            for j in range(2):
                at = slice(j * lanes, (j + 1) * lanes)
                to = pl.ds(pl.multiple_of((2 * i + j) * lanes, lanes), lanes)
                normed = (conv[:, to].astype(F32) - mean[...]) * inv[...]
                value = (inv[...] * (held[i, :, at] - first[...] - normed * second[...])).astype(BF16)
                grad[:, to] = value
                grad_head[:, to] = value[:HALO]
            return carry

        lax.fori_loop(0, steps, finish, 0)


def norm_backward(ring, upstream, weight, conv, mean, inv, gain):
    tokens, width = upstream.shape
    lanes = width // 16
    wide = 2 * lanes
    column = lambda rows: pl.BlockSpec((rows, wide), lambda i, ring: (0, i))
    whole = lambda *shape: pl.BlockSpec(shape, lambda i, ring: (0,) * len(shape))
    return call(
        norm_kernel,
        (8,),
        [
            whole(tokens, width),
            column(width),
            whole(tokens, width),
            whole(tokens, lanes),
            whole(tokens, lanes),
            column(1),
        ],
        [whole(tokens, width), whole(HALO, width), whole(16, lanes)],
        [
            jax.ShapeDtypeStruct((tokens, width), BF16),
            jax.ShapeDtypeStruct((HALO, width), BF16),
            jax.ShapeDtypeStruct((16, lanes), F32),
        ],
        [
            pltpu.VMEM((8, tokens, wide), F32),
            pltpu.VMEM((tokens, lanes), F32),
            pltpu.VMEM((tokens, lanes), F32),
        ],
        flops=2 * tokens * width * width,
        moved=2 * width * width + 6 * tokens * width,
    )(ring, upstream, weight, conv, mean, inv, gain)


def taps_kernel(ring, glu, halo, grad, gain_part, out, wide):
    tokens = glu.shape[0]
    lanes = wide.shape[2]
    for i in range(GROUP):
        at = slice(i * lanes, (i + 1) * lanes)
        wide[i, pl.ds(0, HALO), :] = halo[:, at].astype(F32)
        wide[i, pl.ds(HALO, tokens), :] = glu[:, at].astype(F32)
        g = grad[:, at].astype(F32)
        for j in range(31):
            out[i, pl.ds(j, 1), :] = jnp.sum(g * wide[i, pl.ds(2 + j, tokens), :], axis=0, keepdims=True)
        out[i, pl.ds(31, 1), :] = jnp.zeros((1, lanes), F32)
        out[i, pl.ds(32, 16), :] = gain_part[...]


def taps_backward(ring, glu, halo, grad, gain_part):
    tokens, width = glu.shape
    lanes = width // 16
    column = lambda rows: pl.BlockSpec((rows, GROUP * lanes), lambda i, ring: (0, i))
    return call(
        taps_kernel,
        (16 // GROUP,),
        [column(tokens), column(HALO), column(tokens), pl.BlockSpec((16, lanes), lambda i, ring: (0, 0))],
        pl.BlockSpec((GROUP, 48, lanes), lambda i, ring: (i, 0, 0)),
        jax.ShapeDtypeStruct((16, 48, lanes), F32),
        [pltpu.VMEM((GROUP, HALO + tokens, lanes), F32)],
        flops=62 * tokens * width * 100,
        moved=4 * tokens * width,
    )(ring, glu, halo, grad, gain_part)


def input_kernel(ring, grad, tail, taps, value, gate, grad_value, grad_gate, wide):
    tokens = grad.shape[0]
    lanes = wide.shape[2]
    for i in range(GROUP):
        at = slice(i * lanes, (i + 1) * lanes)
        wide[i, pl.ds(0, tokens), :] = grad[:, at].astype(F32)
        wide[i, pl.ds(tokens, HALO), :] = tail[:, at].astype(F32)
        acc = jnp.zeros((tokens, lanes), F32)
        for j in range(31):
            acc = acc + taps[i, pl.ds(j, 1), :] * wide[i, pl.ds(30 - j, tokens), :]
        grad_glu = acc.astype(BF16).astype(F32)
        sig = jax.nn.sigmoid(gate[:, at].astype(F32))
        grad_value[:, at] = (grad_glu * sig).astype(BF16)
        grad_gate[:, at] = (grad_glu * value[:, at].astype(F32) * sig * (1.0 - sig)).astype(BF16)


def input_backward(ring, grad, tail, taps, value, gate):
    tokens, width = grad.shape
    lanes = width // 16
    column = lambda rows: pl.BlockSpec((rows, GROUP * lanes), lambda i, ring: (0, i))
    return call(
        input_kernel,
        (16 // GROUP,),
        [
            column(tokens),
            column(HALO),
            pl.BlockSpec((GROUP, 32, lanes), lambda i, ring: (i, 0, 0)),
            column(tokens),
            column(tokens),
        ],
        [column(tokens)] * 2,
        [jax.ShapeDtypeStruct((tokens, width), BF16)] * 2,
        [pltpu.VMEM((GROUP, HALO + tokens, lanes), F32)],
        flops=62 * tokens * width * 100,
        moved=10 * tokens * width,
    )(ring, grad, tail, taps, value, gate)


def from_everyone(shard, axis):
    count = lax.axis_size(axis)
    return lax.all_to_all(jnp.broadcast_to(shard[None], (count, *shard.shape)), axis, 0, 0, tiled=True)


EARLY = [
    (half, k, pair, 2 * half + out, at)
    for half in range(2)
    for k, pair, out, at in ((2, 0, 0, 0), (1, 1, 0, 2), (2, 1, 1, 0), (3, 0, 1, 2))
]
REST = [
    (half, k, pair, 3 * half + out, at)
    for half in range(2)
    for k, pair, out, at in ((1, 0, 0, 0), (3, 1, 1, 0), (0, 0, 2, 0), (0, 1, 2, 2))
]


def step(value_half, gate_half, upstream, conv_taps, norm_gain, out_weight):
    value, gate, upstream = value_half[0], gate_half[0], upstream[0]
    tokens, width = value.shape
    lanes = width // 16
    ring = jnp.stack([lax.axis_index(axis) for axis in (Y, X, Z, CORE)]).astype(jnp.int32)
    gain = norm_gain[None]

    weight = lax.all_gather(out_weight, DP, axis=0, tiled=True)
    tail = slice(tokens - HALO, tokens)
    glu_tail = (value[tail].astype(F32) * jax.nn.sigmoid(gate[tail].astype(F32))).astype(BF16)
    halo = lax.ppermute(glu_tail, SP, [(i, i + 1) for i in range(15)])
    taps = from_everyone(jnp.pad(conv_taps, ((0, 1), (0, 0))), SP)

    turned, turned_away = turn(ring, upstream)
    turned_other = shift(turned_away, CORE, 1)

    glu, act, conv, mean, inv = forward(ring, value, gate, halo, taps, tie(gain, turned))
    act_other = shift(act, CORE, 1)
    early = outer(EARLY, ring, turned, turned_other, act, act_other)
    rest = outer(REST, ring, turned, turned_other, act, act_other)
    early, rest = (early[:2], early[2:]), (rest[:3], rest[3:])

    opened = [ring_open(axis, *part) for axis, part in zip((X, Y), early)]
    sums = [ring_sums(pair, *part[:2]) for pair, part in zip(opened, rest)]
    halves = [
        ring_close(axis, pair, late, part[2][:2], part[2][2:])
        for axis, pair, late, part in zip((X, Y), opened, sums, rest)
    ]
    grad, grad_head, gain_part = norm_backward(ring, upstream, weight, conv, mean, inv, tie(gain, sums))
    next_head = lax.ppermute(grad_head, SP, [(i + 1, i) for i in range(15)])

    pieces = [cut(*half) for half in halves]
    opened = [ring_open(axis, *piece[0]) for axis, piece in zip((Y, X), pieces)]
    sums = [ring_sums(pair, *piece[1]) for pair, piece in zip(opened, pieces)]
    closed = [ring_close(axis, pair, late, *piece[2]) for axis, pair, late, piece in zip((Y, X), opened, sums, pieces)]
    terms = taps_backward(ring, glu, halo, grad, gain_part)
    mine = lax.all_to_all(terms, SP, 0, 0, tiled=True)
    mine = jnp.sum(mine, axis=0)
    mine = mine + shift(mine, CORE, 1)

    scattered = jnp.concatenate([rows for half in closed for rows in half]).reshape(8, lanes, lanes)
    merged = jnp.concatenate([scattered, jnp.broadcast_to(mine[None], (8, *mine.shape))], axis=1)
    merged = lax.all_to_all(merged, Z, 0, 0, tiled=True)
    merged = jnp.sum(merged, axis=0)
    grad_value, grad_gate = input_backward(ring, grad, next_head, taps, value, gate)

    owned, mine = merged[:lanes].astype(BF16), merged[lanes:]
    grad_weight = place(ring, plane_column(plane_row(owned)))
    grad_taps = mine[:31]
    grad_gain = mine[32:].reshape(width)
    return grad_value[None], grad_gate[None], grad_taps, grad_gain, grad_weight


def solution(mesh):
    torus = Mesh(mesh.devices.reshape(4, 4, 8, 2), (Y, X, Z, CORE))
    placed = (P(DP, SP, None), P(DP, SP, None), P(DP, SP, None), P(None, SP), P(), P(DP, None))
    return jax.shard_map(
        step,
        mesh=torus,
        in_specs=placed,
        out_specs=(P(DP, SP, None), P(DP, SP, None), P(None, SP), P(), P(DP, None)),
        check_vma=False,
    )
```

profile of v0, /device:TPU:32, one launch (start us, length us, event | category | flops | bytes accessed | tf_op | source)
XLA Modules:
  0.0 175.2 jit_solution(432825409121915474)
XLA Ops:
  9.4 7.0 %all-to-all-start = ((f32[16,32,128]{2,1,0:T(8,128)}), f32[16,32,128]{2,1,0:T(8,128)S(1)}, u32[]{:S(2)}, u32[]{:S(2)}) async-start(f32[16,32,128]{2,1,0:T(8,128)} %broadcast_in_dim.10), calls=%async_computation | async-start | bytes 524288 | tf_op jit(solution)/shard_map/all_to_all | solution.py:406
  16.4 1.1 fusion.16
  17.4 3.8 %collective-permute-start = (bf16[32,2048]{1,0:T(8,128)(2,1)S(1)}, bf16[32,2048]{1,0:T(8,128)(2,1)S(1)}, u32[]{:S(2)}, u32[]{:S(2)}) collective-permute-start(bf16[32,2048]{1,0:T(8,128)(2,1)S(1)} %fusion.16), channel_id=1, source_target_pairs={{0,16},{16,32},{32,48},{48,64},{64,80},{80,96},{96,112},{112,128},... | collective-permute-start | bytes 393224 | tf_op jit(solution)/shard_map/ppermute | solution.py:431
  21.4 1.2 copy-done
  22.6 1.7 shard_map.101
  25.1 1.2 copy-done.2
  26.3 1.2 copy-done.4
  28.2 8.3 %shard_map.102 = (bf16[256,2048]{1,0:T(8,128)(2,1)S(1)}, bf16[256,2048]{1,0:T(8,128)(2,1)S(1)}, bf16[256,2048]{1,0:T(8,128)(2,1)S(1)}, f32[256,128]{1,0:T(8,128)S(1)}, f32[256,128]{1,0:T(8,128)S(1)}) custom-call(s32[4]{0:T(128)S(1)} %pad_add_fusion.ring, bf16[256,2048]{1,0:T(8,128)(2,1)S(1)} %bitcast.89, bf16[256,2048]{1,0:T(8,128)(2,1)S(1)} %bitcast.91, ...), custom_call_target="tpu_custom_call" | custom-call | flops 3250585600 | bytes 5242880 | tf_op jit(solution)/shard_map/pallas_call | solution.py:99
  36.6 1.0 copy-done.10
  38.1 3.3 %collective-permute-done.1.turned_other = bf16[8,128,256]{2,1,0:T(8,128)(2,1)S(1)} collective-permute-done((bf16[8,128,256]{2,1,0:T(8,128)(2,1)S(1)}, bf16[8,128,256]{2,1,0:T(8,128)(2,1)S(1)}, u32[]{:S(2)}, u32[]{:S(2)}) %collective-permute-start.1) | collective-permute-done | bytes 524320 | tf_op jit(solution)/shard_map/ppermute | solution.py:42
  41.3 1.9 %shard_map.104 = (bf16[4,512,128]{2,1,0:T(8,128)(2,1)S(1)}, bf16[4,512,128]{2,1,0:T(8,128)(2,1)S(1)}, bf16[4,512,128]{2,1,0:T(8,128)(2,1)S(1)}, bf16[4,512,128]{2,1,0:T(8,128)(2,1)S(1)}) custom-call(s32[4]{0:T(128)S(1)} %pad_add_fusion.ring, bf16[8,128,256]{2,1,0:T(8,128)(2,1)S(1)} %get-tuple-element.29.turned, ...), custom_call_target="tpu_custom_call" | custom-call | flops 1073741824 | bytes 4194304 | tf_op jit(solution)/shard_map/pallas_call | solution.py:181
  43.2 2.4 %collective-permute-start.4 = (bf16[4,512,128]{2,1,0:T(8,128)(2,1)S(1)}, bf16[4,512,128]{2,1,0:T(8,128)(2,1)S(1)}, u32[]{:S(2)}, u32[]{:S(2)}) collective-permute-start(bf16[4,512,128]{2,1,0:T(8,128)(2,1)S(1)} %get-tuple-element.39), channel_id=1, source_target_pairs={{0,48},{16,0},{32,16},{48,32},{1,49},{17,1},{33,17},{49,33},{2,50}... | collective-permute-start | bytes 1572872 | tf_op jit(solution)/shard_map/ppermute | solution.py:42
  45.7 4.1 %collective-permute-start.6 = (bf16[4,512,128]{2,1,0:T(8,128)(2,1)S(1)}, bf16[4,512,128]{2,1,0:T(8,128)(2,1)S(1)}, u32[]{:S(2)}, u32[]{:S(2)}) collective-permute-start(bf16[4,512,128]{2,1,0:T(8,128)(2,1)S(1)} %get-tuple-element.43), channel_id=1, source_target_pairs={{0,192},{64,0},{128,64},{192,128},{1,193},{65,1},{129,65},{193,129... | collective-permute-start | bytes 1572872 | tf_op jit(solution)/shard_map/ppermute | solution.py:42
  49.8 1.9 %shard_map.103 = (bf16[2,512,128]{2,1,0:T(8,128)(2,1)S(1)}, bf16[2,512,128]{2,1,0:T(8,128)(2,1)S(1)}, bf16[4,512,128]{2,1,0:T(8,128)(2,1)S(1)}, bf16[2,512,128]{...) custom-call(s32[4]{0:T(128)S(1)} %pad_add_fusion.ring, ...), custom_call_target="tpu_custom_call" | custom-call | flops 1073741824 | bytes 4194304 | tf_op jit(solution)/shard_map/pallas_call | solution.py:181
  51.6 5.6 %collective-permute-done.4 = bf16[4,512,128]{2,1,0:T(8,128)(2,1)S(1)} collective-permute-done((bf16[4,512,128]{2,1,0:T(8,128)(2,1)S(1)}, bf16[4,512,128]{2,1,0:T(8,128)(2,1)S(1)}, u32[]{:S(2)}, u32[]{:S(2)}) %collective-permute-start.4) | collective-permute-done | bytes 524320 | tf_op jit(solution)/shard_map/ppermute | solution.py:42
  57.3 3.7 %collective-permute-start.9 = (bf16[2,512,128]{2,1,0:T(8,128)(2,1)S(1)}, bf16[2,512,128]{2,1,0:T(8,128)(2,1)S(1)}, u32[]{:S(2)}, u32[]{:S(2)}) collective-permute-start(bf16[2,512,128]{2,1,0:T(8,128)(2,1)S(1)} %add_convert_fusion.2), channel_id=1, source_target_pairs={{0,48},{16,0},{32,16},{48,32},{1,49},{17,1},{33,17},{49,33},{2,50}... | collective-permute-start | bytes 786440 | tf_op jit(solution)/shard_map/ppermute | solution.py:42
  61.3 3.3 %collective-permute-start.15 = (bf16[2,512,128]{2,1,0:T(8,128)(2,1)S(1)}, bf16[2,512,128]{2,1,0:T(8,128)(2,1)S(1)}, u32[]{:S(2)}, u32[]{:S(2)}) collective-permute-start(bf16[2,512,128]{2,1,0:T(8,128)(2,1)S(1)} %add_convert_fusion), channel_id=1, source_target_pairs={{0,192},{64,0},{128,64},{192,128},{1,193},{65,1},{129,65},{193,129... | collective-permute-start | bytes 786440 | tf_op jit(solution)/shard_map/ppermute | solution.py:42
  64.9 1.1 collective-permute-done.9
  66.0 3.6 %collective-permute-done.8 = bf16[2,512,128]{2,1,0:T(8,128)(2,1)S(1)} collective-permute-done((bf16[2,512,128]{2,1,0:T(8,128)(2,1)S(1)}, bf16[2,512,128]{2,1,0:T(8,128)(2,1)S(1)}, u32[]{:S(2)}, u32[]{:S(2)}) %collective-permute-start.8) | collective-permute-done | bytes 262176 | tf_op jit(solution)/shard_map/ppermute | solution.py:42
  69.8 2.7 %collective-permute-start.12 = (bf16[512,128]{1,0:T(8,128)(2,1)S(1)}, bf16[512,128]{1,0:T(8,128)(2,1)S(1)}, u32[]{:S(2)}, u32[]{:S(2)}) collective-permute-start(bf16[512,128]{1,0:T(8,128)(2,1)S(1)} %pad_maximum_fusion.3), channel_id=1, source_target_pairs={{0,192},{64,0},{128,64},{192,128},{1,193},{65,1},{129,65},{193,129... | collective-permute-start | bytes 393224 | tf_op jit(solution)/shard_map/ppermute | solution.py:42
  73.0 3.4 %collective-permute-start.18 = (bf16[512,128]{1,0:T(8,128)(2,1)S(1)}, bf16[512,128]{1,0:T(8,128)(2,1)S(1)}, u32[]{:S(2)}, u32[]{:S(2)}) collective-permute-start(bf16[512,128]{1,0:T(8,128)(2,1)S(1)} %pad_maximum_fusion.5), channel_id=1, source_target_pairs={{0,48},{16,0},{32,16},{48,32},{1,49},{17,1},{33,17},{49,33},{2,50}... | collective-permute-start | bytes 393224 | tf_op jit(solution)/shard_map/ppermute | solution.py:42
  76.5 2.3 %collective-permute-start.13 = (bf16[256,128]{1,0:T(8,128)(2,1)S(1)}, bf16[256,128]{1,0:T(8,128)(2,1)S(1)}, u32[]{:S(2)}, u32[]{:S(2)}) collective-permute-start(bf16[256,128]{1,0:T(8,128)(2,1)S(1)} %fusion.9), channel_id=1, source_target_pairs={{0,192},{64,0},{128,64},{192,128},{1,193},{65,1},{129,65},{193,129... | collective-permute-start | bytes 196616 | tf_op jit(solution)/shard_map/ppermute | solution.py:42
  78.9 3.8 %collective-permute-start.19 = (bf16[256,128]{1,0:T(8,128)(2,1)S(1)}, bf16[256,128]{1,0:T(8,128)(2,1)S(1)}, u32[]{:S(2)}, u32[]{:S(2)}) collective-permute-start(bf16[256,128]{1,0:T(8,128)(2,1)S(1)} %fusion.1), channel_id=1, source_target_pairs={{0,48},{16,0},{32,16},{48,32},{1,49},{17,1},{33,17},{49,33},{2,50}... | collective-permute-start | bytes 196616 | tf_op jit(solution)/shard_map/ppermute | solution.py:42
  83.3 1.2 collective-permute-done.19
  85.3 9.1 %shard_map.105 = (bf16[256,2048]{1,0:T(8,128)(2,1)S(1)}, bf16[32,2048]{1,0:T(8,128)(2,1)S(1)}, f32[16,128]{1,0:T(8,128)S(1)}) custom-call(s32[4]{0:T(128)S(1)} %pad_add_fusion.ring, bf16[256,2048]{1,0:T(8,128)(2,1)S(1)} %bitcast.88, bf16[2048,2048]{1,0:T(8,128)(2,1)} %all-gather.2.cloned.1.call-done.weight, bf16[256,2048]{1,0:T(8,128)(2,1)S(1)} %get-tuple-element.31.conv, ...), custom_call_target="tpu_custom_call" | custom-call | flops 2147483648 | bytes 11534336 | tf_op jit(solution)/shard_map/pallas_call | solution.py:309
  94.5 6.6 %shard_map.107 = f32[16,48,128]{2,1,0:T(8,128)} custom-call(s32[4]{0:T(128)S(1)} %pad_add_fusion.ring, bf16[256,2048]{1,0:T(8,128)(2,1)S(1)} %copy-done.11, bf16[32,2048]{1,0:T(8,128)(2,1)S(1)} %collective-permute-done.halo, bf16[256,2048]{1,0:T(8,128)(2,1)S(1)} %get-tuple-element.45.grad, f32[16,128]{1,0:T(8,128)S(1)} %get-tuple-element.52.gain_part), custom_call_target="tpu_custom_call" | custom-call | flops 3250585600 | bytes 2097152 | tf_op jit(solution)/shard_map/pallas_call | solution.py:354
  101.1 1.0 copy-done.8
  102.0 6.4 %all-to-all-start.1 = ((f32[16,48,128]{2,1,0:T(8,128)}), f32[16,48,128]{2,1,0:T(8,128)S(1)}, u32[]{:S(2)}, u32[]{:S(2)}) async-start(f32[16,48,128]{2,1,0:T(8,128)} %shard_map.107), calls=%async_computation.1 | async-start | bytes 786432 | tf_op jit(solution)/shard_map/all_to_all | solution.py:457
  108.4 0.9 fusion.15
  109.4 0.9 fusion.7
  110.3 7.5 %all-to-all-done.1 = f32[16,48,128]{2,1,0:T(8,128)S(1)} async-done(((f32[16,48,128]{2,1,0:T(8,128)}), f32[16,48,128]{2,1,0:T(8,128)S(1)}, u32[]{:S(2)}, u32[]{:S(2)}) %all-to-all-start.1) | async-done | bytes 393248 | tf_op jit(solution)/shard_map/all_to_all | solution.py:457
  118.0 1.1 collective-permute-done.20
  119.1 0.9 pad_maximum_fusion
  120.1 8.5 %all-to-all-start.2 = ((f32[8,176,128]{2,1,0:T(8,128)}), f32[8,176,128]{2,1,0:T(8,128)S(1)}, u32[]{:S(2)}, u32[]{:S(2)}) async-start(f32[8,176,128]{2,1,0:T(8,128)} %pad_maximum_fusion), calls=%async_computation.2 | async-start | bytes 1441792 | tf_op jit(solution)/shard_map/all_to_all | solution.py:463
  128.6 1.3 collective-permute-start.7
  129.9 5.6 %collective-permute-done.7.tail = bf16[32,2048]{1,0:T(8,128)(2,1)S(1)} collective-permute-done((bf16[32,2048]{1,0:T(8,128)(2,1)S(1)}, bf16[32,2048]{1,0:T(8,128)(2,1)S(1)}, u32[]{:S(2)}, u32[]{:S(2)}) %collective-permute-start.7) | collective-permute-done | bytes 131104 | tf_op jit(solution)/shard_map/ppermute | solution.py:450
  135.5 1.2 copy-done.9
  136.7 8.1 %shard_map.106 = (bf16[256,2048]{1,0:T(8,128)(2,1)}, bf16[256,2048]{1,0:T(8,128)(2,1)}) custom-call(s32[4]{0:T(128)S(1)} %pad_add_fusion.ring, bf16[256,2048]{1,0:T(8,128)(2,1)S(1)} %copy-done.9, bf16[32,2048]{1,0:T(8,128)(2,1)S(1)} %collective-permute-done.7.tail, f32[16,32,128]{2,1,0:T(8,128)S(1)} %all-to-all-done.taps, bf16[256,2048]{1,0:T(8,128)(2,1)S(1)} %bitcast.90, ...), custom_call_target="tpu_custom_call" | custom-call | flops 3250585600 | bytes 5242880 | tf_op jit(solution)/shard_map/pallas_call | solution.py:386
  144.8 4.3 %all-to-all-done.2 = f32[8,176,128]{2,1,0:T(8,128)S(1)} async-done(((f32[8,176,128]{2,1,0:T(8,128)}), f32[8,176,128]{2,1,0:T(8,128)S(1)}, u32[]{:S(2)}, u32[]{:S(2)}) %all-to-all-start.2) | async-done | bytes 720928 | tf_op jit(solution)/shard_map/all_to_all | solution.py:463
  150.1 2.1 %collective-permute-start.22 = (bf16[128,128]{1,0:T(8,128)(2,1)S(1)}, bf16[128,128]{1,0:T(8,128)(2,1)S(1)}, u32[]{:S(2)}, u32[]{:S(2)}) collective-permute-start(bf16[128,128]{1,0:T(8,128)(2,1)S(1)} %get-tuple-element.54), channel_id=1, source_target_pairs={{0,32},{16,48},{32,0},{48,16},{1,33},{17,49},{33,1},{49,17},{2,34}... | collective-permute-start | bytes 98312 | tf_op jit(solution)/shard_map/ppermute | solution.py:42
  153.4 2.1 %collective-permute-done.22 = bf16[128,128]{1,0:T(8,128)(2,1)S(1)} collective-permute-done((bf16[128,128]{1,0:T(8,128)(2,1)S(1)}, bf16[128,128]{1,0:T(8,128)(2,1)S(1)}, u32[]{:S(2)}, u32[]{:S(2)}) %collective-permute-start.22) | collective-permute-done | bytes 32800 | tf_op jit(solution)/shard_map/ppermute | solution.py:42
  155.5 1.8 %collective-permute-done.23 = bf16[128,128]{1,0:T(8,128)(2,1)S(1)} collective-permute-done((bf16[128,128]{1,0:T(8,128)(2,1)S(1)}, bf16[128,128]{1,0:T(8,128)(2,1)S(1)}, u32[]{:S(2)}, u32[]{:S(2)}) %collective-permute-start.23) | collective-permute-done | bytes 32800 | tf_op jit(solution)/shard_map/ppermute | solution.py:42
  157.3 0.9 collective-permute-start.24
  158.2 0.9 collective-permute-start.25
  159.7 2.7 %collective-permute-done.24 = bf16[4,128,128]{2,1,0:T(8,128)(2,1)S(1)} collective-permute-done((bf16[4,128,128]{2,1,0:T(8,128)(2,1)S(1)}, bf16[4,128,128]{2,1,0:T(8,128)(2,1)S(1)}, u32[]{:S(2)}, u32[]{:S(2)}) %collective-permute-start.24) | collective-permute-done | bytes 131104 | tf_op jit(solution)/shard_map/ppermute | solution.py:42
  162.4 2.4 %collective-permute-done.25 = bf16[4,128,128]{2,1,0:T(8,128)(2,1)S(1)} collective-permute-done((bf16[4,128,128]{2,1,0:T(8,128)(2,1)S(1)}, bf16[4,128,128]{2,1,0:T(8,128)(2,1)S(1)}, u32[]{:S(2)}, u32[]{:S(2)}) %collective-permute-start.25) | collective-permute-done | bytes 131104 | tf_op jit(solution)/shard_map/ppermute | solution.py:42
  164.8 1.3 collective-permute-done.26
  166.8 1.6 shard_map.108
  (99 shorter events, 10.8 us)
Async XLA Ops:
  7.2 78.1 %all-gather.2.cloned.1.call-start = ((), (), s32[]{:S(2)}) async-start(), calls=%async_computation.3 | async-start | bytes 8912896 | tf_op jit(solution)/shard_map/all_gather | solution.py:428
  9.4 15.7 %all-to-all-start = ((f32[16,32,128]{2,1,0:T(8,128)}), f32[16,32,128]{2,1,0:T(8,128)S(1)}, u32[]{:S(2)}, u32[]{:S(2)}) async-start(f32[16,32,128]{2,1,0:T(8,128)} %broadcast_in_dim.10), calls=%async_computation | async-start | bytes 524288 | tf_op jit(solution)/shard_map/all_to_all | solution.py:406
  17.4 6.8 %collective-permute-start = (bf16[32,2048]{1,0:T(8,128)(2,1)S(1)}, bf16[32,2048]{1,0:T(8,128)(2,1)S(1)}, u32[]{:S(2)}, u32[]{:S(2)}) collective-permute-start(bf16[32,2048]{1,0:T(8,128)(2,1)S(1)} %fusion.16), channel_id=1, source_target_pairs={{0,16},{16,32},{32,48},{48,64},{64,80},{80,96},{96,112},{112,128},... | collective-permute-start | bytes 393224 | tf_op jit(solution)/shard_map/ppermute | solution.py:431
  21.4 1.2 copy-start
  25.1 1.2 copy-start.2
  26.3 1.2 copy-start.4
  36.6 1.0 copy-start.10
  37.6 3.8 %collective-permute-start.2 = (bf16[256,2048]{1,0:T(8,128)(2,1)S(1)}, bf16[256,2048]{1,0:T(8,128)(2,1)S(1)}, u32[]{:S(2)}, u32[]{:S(2)}) collective-permute-start(bf16[256,2048]{1,0:T(8,128)(2,1)S(1)} %get-tuple-element.35.act), channel_id=1, source_target_pairs={{0,1},{1,0},{2,3},{3,2},{4,5},{5,4},{6,7},{7,6},{8,9},{9,8},{10,11... | collective-permute-start | bytes 3145736 | tf_op jit(solution)/shard_map/ppermute | solution.py:42
  37.6 3.8 %collective-permute-start.1 = (bf16[8,128,256]{2,1,0:T(8,128)(2,1)S(1)}, bf16[8,128,256]{2,1,0:T(8,128)(2,1)S(1)}, u32[]{:S(2)}, u32[]{:S(2)}) collective-permute-start(bf16[8,128,256]{2,1,0:T(8,128)(2,1)S(1)} %get-tuple-element.34), channel_id=1, source_target_pairs={{0,1},{1,0},{2,3},{3,2},{4,5},{5,4},{6,7},{7,6},{8,9},{9,8},{10,11... | collective-permute-start | bytes 1572872 | tf_op jit(solution)/shard_map/ppermute | solution.py:42
  43.2 14.0 %collective-permute-start.4 = (bf16[4,512,128]{2,1,0:T(8,128)(2,1)S(1)}, bf16[4,512,128]{2,1,0:T(8,128)(2,1)S(1)}, u32[]{:S(2)}, u32[]{:S(2)}) collective-permute-start(bf16[4,512,128]{2,1,0:T(8,128)(2,1)S(1)} %get-tuple-element.39), channel_id=1, source_target_pairs={{0,48},{16,0},{32,16},{48,32},{1,49},{17,1},{33,17},{49,33},{2,50}... | collective-permute-start | bytes 1572872 | tf_op jit(solution)/shard_map/ppermute | solution.py:42
  45.7 15.3 %collective-permute-start.3 = (bf16[4,512,128]{2,1,0:T(8,128)(2,1)S(1)}, bf16[4,512,128]{2,1,0:T(8,128)(2,1)S(1)}, u32[]{:S(2)}, u32[]{:S(2)}) collective-permute-start(bf16[4,512,128]{2,1,0:T(8,128)(2,1)S(1)} %get-tuple-element.37), channel_id=1, source_target_pairs={{0,16},{16,32},{32,48},{48,0},{1,17},{17,33},{33,49},{49,1},{2,18}... | collective-permute-start | bytes 1572872 | tf_op jit(solution)/shard_map/ppermute | solution.py:42
  45.7 15.5 %collective-permute-start.6 = (bf16[4,512,128]{2,1,0:T(8,128)(2,1)S(1)}, bf16[4,512,128]{2,1,0:T(8,128)(2,1)S(1)}, u32[]{:S(2)}, u32[]{:S(2)}) collective-permute-start(bf16[4,512,128]{2,1,0:T(8,128)(2,1)S(1)} %get-tuple-element.43), channel_id=1, source_target_pairs={{0,192},{64,0},{128,64},{192,128},{1,193},{65,1},{129,65},{193,129... | collective-permute-start | bytes 1572872 | tf_op jit(solution)/shard_map/ppermute | solution.py:42
  49.7 35.5 %copy-start.1 = (bf16[1,256,2048]{2,1,0:T(8,128)(2,1)S(1)}, bf16[1,256,2048]{2,1,0:T(8,128)(2,1)}, u32[]{:S(2)}) copy-start(bf16[1,256,2048]{2,1,0:T(8,128)(2,1)} %param.8) | copy-start | bytes 3145732
  49.8 35.5 %copy-start.7 = (f32[2048]{0:T(1024)S(1)}, f32[2048]{0:T(1024)}, u32[]{:S(2)}) copy-start(f32[2048]{0:T(1024)} %param.10) | copy-start | bytes 24580
  49.8 14.8 %collective-permute-start.5 = (bf16[4,512,128]{2,1,0:T(8,128)(2,1)S(1)}, bf16[4,512,128]{2,1,0:T(8,128)(2,1)S(1)}, u32[]{:S(2)}, u32[]{:S(2)}) collective-permute-start(bf16[4,512,128]{2,1,0:T(8,128)(2,1)S(1)} %get-tuple-element.41), channel_id=1, source_target_pairs={{0,64},{64,128},{128,192},{192,0},{1,65},{65,129},{129,193},{193,1... | collective-permute-start | bytes 1572872 | tf_op jit(solution)/shard_map/ppermute | solution.py:42
  57.3 8.7 %collective-permute-start.9 = (bf16[2,512,128]{2,1,0:T(8,128)(2,1)S(1)}, bf16[2,512,128]{2,1,0:T(8,128)(2,1)S(1)}, u32[]{:S(2)}, u32[]{:S(2)}) collective-permute-start(bf16[2,512,128]{2,1,0:T(8,128)(2,1)S(1)} %add_convert_fusion.2), channel_id=1, source_target_pairs={{0,48},{16,0},{32,16},{48,32},{1,49},{17,1},{33,17},{49,33},{2,50}... | collective-permute-start | bytes 786440 | tf_op jit(solution)/shard_map/ppermute | solution.py:42
  61.1 8.5 %collective-permute-start.8 = (bf16[2,512,128]{2,1,0:T(8,128)(2,1)S(1)}, bf16[2,512,128]{2,1,0:T(8,128)(2,1)S(1)}, u32[]{:S(2)}, u32[]{:S(2)}) collective-permute-start(bf16[2,512,128]{2,1,0:T(8,128)(2,1)S(1)} %add_convert_fusion.3), channel_id=1, source_target_pairs={{0,16},{16,32},{32,48},{48,0},{1,17},{17,33},{33,49},{49,1},{2,18}... | collective-permute-start | bytes 786440 | tf_op jit(solution)/shard_map/ppermute | solution.py:42
  61.3 11.4 %collective-permute-start.15 = (bf16[2,512,128]{2,1,0:T(8,128)(2,1)S(1)}, bf16[2,512,128]{2,1,0:T(8,128)(2,1)S(1)}, u32[]{:S(2)}, u32[]{:S(2)}) collective-permute-start(bf16[2,512,128]{2,1,0:T(8,128)(2,1)S(1)} %add_convert_fusion), channel_id=1, source_target_pairs={{0,192},{64,0},{128,64},{192,128},{1,193},{65,1},{129,65},{193,129... | collective-permute-start | bytes 786440 | tf_op jit(solution)/shard_map/ppermute | solution.py:42
  64.6 8.1 %collective-permute-start.14 = (bf16[2,512,128]{2,1,0:T(8,128)(2,1)S(1)}, bf16[2,512,128]{2,1,0:T(8,128)(2,1)S(1)}, u32[]{:S(2)}, u32[]{:S(2)}) collective-permute-start(bf16[2,512,128]{2,1,0:T(8,128)(2,1)S(1)} %add_convert_fusion.1), channel_id=1, source_target_pairs={{0,64},{64,128},{128,192},{192,0},{1,65},{65,129},{129,193},{193,1... | collective-permute-start | bytes 786440 | tf_op jit(solution)/shard_map/ppermute | solution.py:42
  69.8 12.9 %copy-start.12 = (f32[2,512,128]{2,1,0:T(8,128)}, f32[2,512,128]{2,1,0:T(8,128)S(1)}, u32[]{:S(2)}) copy-start(f32[2,512,128]{2,1,0:T(8,128)S(1)} %get-tuple-element.63) | copy-start | bytes 1572868
  69.8 6.6 %collective-permute-start.12 = (bf16[512,128]{1,0:T(8,128)(2,1)S(1)}, bf16[512,128]{1,0:T(8,128)(2,1)S(1)}, u32[]{:S(2)}, u32[]{:S(2)}) collective-permute-start(bf16[512,128]{1,0:T(8,128)(2,1)S(1)} %pad_maximum_fusion.3), channel_id=1, source_target_pairs={{0,192},{64,0},{128,64},{192,128},{1,193},{65,1},{129,65},{193,129... | collective-permute-start | bytes 393224 | tf_op jit(solution)/shard_map/ppermute | solution.py:42
  72.5 10.1 %collective-permute-start.10 = (bf16[512,128]{1,0:T(8,128)(2,1)S(1)}, bf16[512,128]{1,0:T(8,128)(2,1)S(1)}, u32[]{:S(2)}, u32[]{:S(2)}) collective-permute-start(bf16[512,128]{1,0:T(8,128)(2,1)S(1)} %pad_maximum_fusion.2), channel_id=1, source_target_pairs={{0,64},{64,128},{128,192},{192,0},{1,65},{65,129},{129,193},{193,1... | collective-permute-start | bytes 393224 | tf_op jit(solution)/shard_map/ppermute | solution.py:42
  72.9 12.4 %copy-start.13 = (f32[2,512,128]{2,1,0:T(8,128)}, f32[2,512,128]{2,1,0:T(8,128)S(1)}, u32[]{:S(2)}) copy-start(f32[2,512,128]{2,1,0:T(8,128)S(1)} %get-tuple-element.64) | copy-start | bytes 1572868
  73.0 5.9 %collective-permute-start.18 = (bf16[512,128]{1,0:T(8,128)(2,1)S(1)}, bf16[512,128]{1,0:T(8,128)(2,1)S(1)}, u32[]{:S(2)}, u32[]{:S(2)}) collective-permute-start(bf16[512,128]{1,0:T(8,128)(2,1)S(1)} %pad_maximum_fusion.5), channel_id=1, source_target_pairs={{0,48},{16,0},{32,16},{48,32},{1,49},{17,1},{33,17},{49,33},{2,50}... | collective-permute-start | bytes 393224 | tf_op jit(solution)/shard_map/ppermute | solution.py:42
  76.4 6.9 %collective-permute-start.16 = (bf16[512,128]{1,0:T(8,128)(2,1)S(1)}, bf16[512,128]{1,0:T(8,128)(2,1)S(1)}, u32[]{:S(2)}, u32[]{:S(2)}) collective-permute-start(bf16[512,128]{1,0:T(8,128)(2,1)S(1)} %pad_maximum_fusion.4), channel_id=1, source_target_pairs={{0,16},{16,32},{32,48},{48,0},{1,17},{17,33},{33,49},{49,1},{2,18}... | collective-permute-start | bytes 393224 | tf_op jit(solution)/shard_map/ppermute | solution.py:42
  76.5 8.8 %copy-start.14 = (bf16[512,128]{1,0:T(8,128)(2,1)}, bf16[512,128]{1,0:T(8,128)(2,1)S(1)}, u32[]{:S(2)}) copy-start(bf16[512,128]{1,0:T(8,128)(2,1)S(1)} %collective-permute-done.12) | copy-start | bytes 393220
  76.5 6.1 %collective-permute-start.13 = (bf16[256,128]{1,0:T(8,128)(2,1)S(1)}, bf16[256,128]{1,0:T(8,128)(2,1)S(1)}, u32[]{:S(2)}, u32[]{:S(2)}) collective-permute-start(bf16[256,128]{1,0:T(8,128)(2,1)S(1)} %fusion.9), channel_id=1, source_target_pairs={{0,192},{64,0},{128,64},{192,128},{1,193},{65,1},{129,65},{193,129... | collective-permute-start | bytes 196616 | tf_op jit(solution)/shard_map/ppermute | solution.py:42
  78.9 6.4 %copy-start.16 = (bf16[512,128]{1,0:T(8,128)(2,1)}, bf16[512,128]{1,0:T(8,128)(2,1)S(1)}, u32[]{:S(2)}) copy-start(bf16[512,128]{1,0:T(8,128)(2,1)S(1)} %collective-permute-done.18) | copy-start | bytes 393220
  78.9 5.7 %collective-permute-start.19 = (bf16[256,128]{1,0:T(8,128)(2,1)S(1)}, bf16[256,128]{1,0:T(8,128)(2,1)S(1)}, u32[]{:S(2)}, u32[]{:S(2)}) collective-permute-start(bf16[256,128]{1,0:T(8,128)(2,1)S(1)} %fusion.1), channel_id=1, source_target_pairs={{0,48},{16,0},{32,16},{48,32},{1,49},{17,1},{33,17},{49,33},{2,50}... | collective-permute-start | bytes 196616 | tf_op jit(solution)/shard_map/ppermute | solution.py:42
  83.3 25.1 %collective-permute-start.11 = (bf16[256,128]{1,0:T(8,128)(2,1)}, bf16[256,128]{1,0:T(8,128)(2,1)}, u32[]{:S(2)}, u32[]{:S(2)}) collective-permute-start(bf16[256,128]{1,0:T(8,128)(2,1)} %get-tuple-element.59), channel_id=1, source_target_pairs={{0,64},{64,128},{128,192},{192,0},{1,65},{65,129},{129,193},{193,1... | collective-permute-start | bytes 196616 | tf_op jit(solution)/shard_map/ppermute | solution.py:42
  85.2 24.1 %collective-permute-start.17 = (bf16[256,128]{1,0:T(8,128)(2,1)}, bf16[256,128]{1,0:T(8,128)(2,1)}, u32[]{:S(2)}, u32[]{:S(2)}) collective-permute-start(bf16[256,128]{1,0:T(8,128)(2,1)} %get-tuple-element.61), channel_id=1, source_target_pairs={{0,16},{16,32},{32,48},{48,0},{1,17},{17,33},{33,49},{49,1},{2,18}... | collective-permute-start | bytes 196616 | tf_op jit(solution)/shard_map/ppermute | solution.py:42
  85.3 9.2 %copy-start.11 = (bf16[256,2048]{1,0:T(8,128)(2,1)S(1)}, bf16[256,2048]{1,0:T(8,128)(2,1)}, u32[]{:S(2)}) copy-start(bf16[256,2048]{1,0:T(8,128)(2,1)} %copy-done.10) | copy-start | bytes 3145732
  94.4 14.0 %copy-start.15 = (bf16[512,128]{1,0:T(8,128)(2,1)S(1)}, bf16[512,128]{1,0:T(8,128)(2,1)}, u32[]{:S(2)}) copy-start(bf16[512,128]{1,0:T(8,128)(2,1)} %copy-done.14) | copy-start | bytes 393220
  94.4 15.0 %copy-start.17 = (bf16[512,128]{1,0:T(8,128)(2,1)S(1)}, bf16[512,128]{1,0:T(8,128)(2,1)}, u32[]{:S(2)}) copy-start(bf16[512,128]{1,0:T(8,128)(2,1)} %copy-done.16) | copy-start | bytes 393220
  94.4 41.0 %copy-start.3 = (bf16[1,256,2048]{2,1,0:T(8,128)(2,1)S(1)}, bf16[1,256,2048]{2,1,0:T(8,128)(2,1)}, u32[]{:S(2)}) copy-start(bf16[1,256,2048]{2,1,0:T(8,128)(2,1)} %param.6) | copy-start | bytes 3145732
  94.5 41.0 %copy-start.5 = (bf16[1,256,2048]{2,1,0:T(8,128)(2,1)S(1)}, bf16[1,256,2048]{2,1,0:T(8,128)(2,1)}, u32[]{:S(2)}) copy-start(bf16[1,256,2048]{2,1,0:T(8,128)(2,1)} %param.7) | copy-start | bytes 3145732
  101.1 1.0 copy-start.8
  102.0 15.8 %all-to-all-start.1 = ((f32[16,48,128]{2,1,0:T(8,128)}), f32[16,48,128]{2,1,0:T(8,128)S(1)}, u32[]{:S(2)}, u32[]{:S(2)}) async-start(f32[16,48,128]{2,1,0:T(8,128)} %shard_map.107), calls=%async_computation.1 | async-start | bytes 786432 | tf_op jit(solution)/shard_map/all_to_all | solution.py:457
  117.8 1.3 collective-permute-start.20
  120.1 29.1 %all-to-all-start.2 = ((f32[8,176,128]{2,1,0:T(8,128)}), f32[8,176,128]{2,1,0:T(8,128)S(1)}, u32[]{:S(2)}, u32[]{:S(2)}) async-start(f32[8,176,128]{2,1,0:T(8,128)} %pad_maximum_fusion), calls=%async_computation.2 | async-start | bytes 1441792 | tf_op jit(solution)/shard_map/all_to_all | solution.py:463
  128.6 6.9 %collective-permute-start.7 = (bf16[32,2048]{1,0:T(8,128)(2,1)S(1)}, bf16[32,2048]{1,0:T(8,128)(2,1)S(1)}, u32[]{:S(2)}, u32[]{:S(2)}) collective-permute-start(bf16[32,2048]{1,0:T(8,128)(2,1)S(1)} %get-tuple-element.46), channel_id=1, source_target_pairs={{16,0},{32,16},{48,32},{64,48},{80,64},{96,80},{112,96},{128,112},... | collective-permute-start | bytes 393224 | tf_op jit(solution)/shard_map/ppermute | solution.py:450
  135.5 1.2 copy-start.9
  149.2 4.2 %collective-permute-start.21 = (bf16[128,128]{1,0:T(8,128)(2,1)S(1)}, bf16[128,128]{1,0:T(8,128)(2,1)S(1)}, u32[]{:S(2)}, u32[]{:S(2)}) collective-permute-start(bf16[128,128]{1,0:T(8,128)(2,1)S(1)} %get-tuple-element.54), channel_id=1, source_target_pairs={{0,48},{16,0},{32,16},{48,32},{1,49},{17,1},{33,17},{49,33},{2,50}... | collective-permute-start | bytes 98312 | tf_op jit(solution)/shard_map/ppermute | solution.py:42
  150.1 5.4 %collective-permute-start.22 = (bf16[128,128]{1,0:T(8,128)(2,1)S(1)}, bf16[128,128]{1,0:T(8,128)(2,1)S(1)}, u32[]{:S(2)}, u32[]{:S(2)}) collective-permute-start(bf16[128,128]{1,0:T(8,128)(2,1)S(1)} %get-tuple-element.54), channel_id=1, source_target_pairs={{0,32},{16,48},{32,0},{48,16},{1,33},{17,49},{33,1},{49,17},{2,34}... | collective-permute-start | bytes 98312 | tf_op jit(solution)/shard_map/ppermute | solution.py:42
  152.2 5.1 %collective-permute-start.23 = (bf16[128,128]{1,0:T(8,128)(2,1)S(1)}, bf16[128,128]{1,0:T(8,128)(2,1)S(1)}, u32[]{:S(2)}, u32[]{:S(2)}) collective-permute-start(bf16[128,128]{1,0:T(8,128)(2,1)S(1)} %get-tuple-element.54), channel_id=1, source_target_pairs={{0,16},{16,32},{32,48},{48,0},{1,17},{17,33},{33,49},{49,1},{2,18}... | collective-permute-start | bytes 98312 | tf_op jit(solution)/shard_map/ppermute | solution.py:42
  157.3 5.0 %collective-permute-start.24 = (bf16[4,128,128]{2,1,0:T(8,128)(2,1)S(1)}, bf16[4,128,128]{2,1,0:T(8,128)(2,1)S(1)}, u32[]{:S(2)}, u32[]{:S(2)}) collective-permute-start(bf16[4,128,128]{2,1,0:T(8,128)(2,1)S(1)} %pad_maximum_fusion.6), channel_id=1, source_target_pairs={{0,192},{64,0},{128,64},{192,128},{1,193},{65,1},{129,65},{193,129... | collective-permute-start | bytes 393224 | tf_op jit(solution)/shard_map/ppermute | solution.py:42
  158.2 6.6 %collective-permute-start.25 = (bf16[4,128,128]{2,1,0:T(8,128)(2,1)S(1)}, bf16[4,128,128]{2,1,0:T(8,128)(2,1)S(1)}, u32[]{:S(2)}, u32[]{:S(2)}) collective-permute-start(bf16[4,128,128]{2,1,0:T(8,128)(2,1)S(1)} %pad_maximum_fusion.6), channel_id=1, source_target_pairs={{0,128},{64,192},{128,0},{192,64},{1,129},{65,193},{129,1},{193,65... | collective-permute-start | bytes 393224 | tf_op jit(solution)/shard_map/ppermute | solution.py:42
  159.1 7.0 %collective-permute-start.26 = (bf16[4,128,128]{2,1,0:T(8,128)(2,1)S(1)}, bf16[4,128,128]{2,1,0:T(8,128)(2,1)S(1)}, u32[]{:S(2)}, u32[]{:S(2)}) collective-permute-start(bf16[4,128,128]{2,1,0:T(8,128)(2,1)S(1)} %pad_maximum_fusion.6), channel_id=1, source_target_pairs={{0,64},{64,128},{128,192},{192,0},{1,65},{65,129},{129,193},{193,1... | collective-permute-start | bytes 393224 | tf_op jit(solution)/shard_map/ppermute | solution.py:42
  (1 other events, 0.7 us)
Sparse Core Ops, SparseCore 0:
  9.8 56.6 all-gather.1
where the time goes:
time: 176 us; the launch traced here: 175 us
  starting transfers between devices  59 us (34%)
  waiting for transfers between devices  46 us (26%)
  Pallas kernels  39.2 us (22%)
  between operations  14.5 us (8%)
  local copies, waits for them, and re-layouts  10.4 us (6%)
  other arithmetic  6.13 us (3%)
    ppermute x25, starting transfers between devices, shift(): lax.ppermute(value, axis, [(i, (i + amount) % count) for i in range(count)])  32 us
    ppermute x25, waiting for transfers between devices, shift(): lax.ppermute(value, axis, [(i, (i + amount) % count) for i in range(count)])  27 us
    pallas_call x1, Pallas kernels, norm_backward(): call(norm_kernel, (8,), [whole(tokens, width), column(width), whole(token...  9.1 us
    all_to_all x1, starting transfers between devices, step(): merged = lax.all_to_all(merged, Z, 0, 0, tiled=True)  8.52 us
    pallas_call x1, Pallas kernels, forward(): call(forward_kernel, (16 // GROUP,), [column(tokens), column(tokens), col...  8.34 us
    pallas_call x1, Pallas kernels, input_backward(): call(input_kernel, (16 // GROUP,), [column(tokens), column(HALO), pl.Bloc...  8.12 us
    unnamed x42, local copies, waits for them, and re-layouts  7.66 us
    all_to_all x1, waiting for transfers between devices, step(): mine = lax.all_to_all(terms, SP, 0, 0, tiled=True)  7.49 us
  transfers between devices with their start and end apart: 31, of which 18 were waited for; matrix products, arithmetic and copies ran while one was open for 4% of the time, Pallas kernels for 21%

commit v1 on v0

--- a/solution.py
+++ b/solution.py
@@ -14,6 +14,7 @@
 NORM_EPS = 1e-05
 HALO = 32
 GROUP = 4
+VMEM_LIMIT = 60
 INTERPRET = False
 F32, BF16 = jnp.float32, jnp.bfloat16
 
@@ -30,7 +31,7 @@
         ),
         out_shape=out_shape,
         compiler_params=pltpu.CompilerParams(
-            dimension_semantics=("arbitrary",) * len(grid), vmem_limit_bytes=48 * 1024 * 1024
+            dimension_semantics=("arbitrary",) * len(grid), vmem_limit_bytes=VMEM_LIMIT * 1024 * 1024
         ),
         cost_estimate=pl.CostEstimate(flops=flops, bytes_accessed=moved, transcendentals=0),
         interpret=INTERPRET,
@@ -44,6 +45,7 @@
 
 def forward_kernel(ring, value, gate, halo, taps, gain, glu, act, conv, mean, inv, wide, held, total):
     step = pl.program_id(0)
+    start = ring[0] + ring[1] == 0
     tokens = value.shape[0]
     blocks, _, lanes = held.shape
 
@@ -56,7 +58,7 @@
         block = step * GROUP + i
         gated = (value[:, at].astype(F32) * jax.nn.sigmoid(gate[:, at].astype(F32))).astype(BF16)
         glu[:, at] = gated
-        wide[i, pl.ds(0, HALO), :] = halo[:, at].astype(F32)
+        wide[i, pl.ds(0, HALO), :] = jnp.where(start, 0.0, halo[:, at].astype(F32))
         wide[i, pl.ds(HALO, tokens), :] = gated.astype(F32)
         acc = jnp.zeros((tokens, lanes), F32)
         for j in range(31):
@@ -334,11 +336,12 @@
 
 
 def taps_kernel(ring, glu, halo, grad, gain_part, out, wide):
+    start = ring[0] + ring[1] == 0
     tokens = glu.shape[0]
     lanes = wide.shape[2]
     for i in range(GROUP):
         at = slice(i * lanes, (i + 1) * lanes)
-        wide[i, pl.ds(0, HALO), :] = halo[:, at].astype(F32)
+        wide[i, pl.ds(0, HALO), :] = jnp.where(start, 0.0, halo[:, at].astype(F32))
         wide[i, pl.ds(HALO, tokens), :] = glu[:, at].astype(F32)
         g = grad[:, at].astype(F32)
         for j in range(31):
@@ -364,12 +367,13 @@
 
 
 def input_kernel(ring, grad, tail, taps, value, gate, grad_value, grad_gate, wide):
+    end = ring[0] + ring[1] == 6
     tokens = grad.shape[0]
     lanes = wide.shape[2]
     for i in range(GROUP):
         at = slice(i * lanes, (i + 1) * lanes)
         wide[i, pl.ds(0, tokens), :] = grad[:, at].astype(F32)
-        wide[i, pl.ds(tokens, HALO), :] = tail[:, at].astype(F32)
+        wide[i, pl.ds(tokens, HALO), :] = jnp.where(end, 0.0, tail[:, at].astype(F32))
         acc = jnp.zeros((tokens, lanes), F32)
         for j in range(31):
             acc = acc + taps[i, pl.ds(j, 1), :] * wide[i, pl.ds(30 - j, tokens), :]
@@ -428,7 +432,7 @@
     weight = lax.all_gather(out_weight, DP, axis=0, tiled=True)
     tail = slice(tokens - HALO, tokens)
     glu_tail = (value[tail].astype(F32) * jax.nn.sigmoid(gate[tail].astype(F32))).astype(BF16)
-    halo = lax.ppermute(glu_tail, SP, [(i, i + 1) for i in range(15)])
+    halo = lax.ppermute(glu_tail, SP, [(i, (i + 1) % 16) for i in range(16)])
     taps = from_everyone(jnp.pad(conv_taps, ((0, 1), (0, 0))), SP)
 
     turned, turned_away = turn(ring, upstream)
@@ -447,7 +451,7 @@
         for axis, pair, late, part in zip((X, Y), opened, sums, rest)
     ]
     grad, grad_head, gain_part = norm_backward(ring, upstream, weight, conv, mean, inv, tie(gain, sums))
-    next_head = lax.ppermute(grad_head, SP, [(i + 1, i) for i in range(15)])
+    next_head = lax.ppermute(grad_head, SP, [((i + 1) % 16, i) for i in range(16)])
 
     pieces = [cut(*half) for half in halves]
     opened = [ring_open(axis, *piece[0]) for axis, piece in zip((Y, X), pieces)]
@@ -459,9 +463,9 @@
     mine = mine + shift(mine, CORE, 1)
 
     scattered = jnp.concatenate([rows for half in closed for rows in half]).reshape(8, lanes, lanes)
-    merged = jnp.concatenate([scattered, jnp.broadcast_to(mine[None], (8, *mine.shape))], axis=1)
+    merged = jnp.concatenate([scattered, jnp.broadcast_to(mine[None], (8, *mine.shape))], axis=1).astype(BF16)
     merged = lax.all_to_all(merged, Z, 0, 0, tiled=True)
-    merged = jnp.sum(merged, axis=0)
+    merged = jnp.sum(merged.astype(F32), axis=0)
     grad_value, grad_gate = input_backward(ring, grad, next_head, taps, value, gate)
 
     owned, mine = merged[:lanes].astype(BF16), merged[lanes:]

time: 176 us -> 186 us (1.057)
  Pallas kernels: 39.2 us -> 57.6 us
  starting transfers between devices: 59 us -> 53.8 us
  local copies, waits for them, and re-layouts: 10.4 us -> 6.18 us
  other arithmetic: 6.13 us -> 9.32 us
  waiting for transfers between devices: 46 us -> 43.9 us
    pallas_call x2, Pallas kernels: 3.74 us -> 9.72 us  [outer(): call(functools.partial(outer_kernel, plan), (1,), [whole(8, lanes, tokens...]
    pallas_call x1, Pallas kernels: 1.65 us -> 6.2 us  [turn(): call(turn_kernel, (8,), [pl.BlockSpec((tokens, 2 * lanes), lambda i, ring...]
    all_to_all x1, waiting for transfers between devices: 4.34 us -> 0.01 us  [step(): merged = lax.all_to_all(merged, Z, 0, 0, tiled=True)]
    unnamed x42 -> x22, local copies, waits for them, and re-layouts: 7.66 us -> 3.4 us
    ppermute x25, starting transfers between devices: 32 us -> 28.2 us  [shift(): lax.ppermute(value, axis, [(i, (i + amount) % count) for i in range(count)])]
    pallas_call x1, Pallas kernels: 8.34 us -> 10.9 us  [forward(): call(forward_kernel, (16 // GROUP,), [column(tokens), column(tokens), col...]
    another operation x2 -> x5, other arithmetic: 0.38 us -> 2.5 us
    pallas_call x1, Pallas kernels: 9.1 us -> 11.1 us  [norm_backward(): call(norm_kernel, (8,), [whole(tokens, width), column(width), whole(token...]
  transfers between devices with their start and end apart: 31 -> 31, of which waited for: 18 -> 13; matrix products, arithmetic and copies ran while one was open for 4% -> 6% of each run, Pallas kernels for 21% -> 30%
where the time goes in v1:
time: 186 us; the launch traced here: 185 us
  Pallas kernels  57.6 us (31%)
  starting transfers between devices  53.8 us (29%)
  waiting for transfers between devices  43.9 us (24%)
  between operations  14.3 us (8%)
  other arithmetic  9.32 us (5%)
  local copies, waits for them, and re-layouts  6.18 us (3%)
    ppermute x25, waiting for transfers between devices, shift(): lax.ppermute(value, axis, [(i, (i + amount) % count) for i in range(count)])  28.7 us
    ppermute x25, starting transfers between devices, shift(): lax.ppermute(value, axis, [(i, (i + amount) % count) for i in range(count)])  28.2 us
    pallas_call x1, Pallas kernels, norm_backward(): call(norm_kernel, (8,), [whole(tokens, width), column(width), whole(token...  11.1 us
    pallas_call x1, Pallas kernels, forward(): call(forward_kernel, (16 // GROUP,), [column(tokens), column(tokens), col...  10.9 us
    pallas_call x2, Pallas kernels, outer(): call(functools.partial(outer_kernel, plan), (1,), [whole(8, lanes, tokens...  9.72 us
    all_to_all x1, waiting for transfers between devices, step(): mine = lax.all_to_all(terms, SP, 0, 0, tiled=True)  9.3 us
    pallas_call x1, Pallas kernels, input_backward(): call(input_kernel, (16 // GROUP,), [column(tokens), column(HALO), pl.Bloc...  9.05 us
    all_to_all x1, starting transfers between devices, step(): merged = lax.all_to_all(merged, Z, 0, 0, tiled=True)  8.56 us
  transfers between devices with their start and end apart: 31, of which 13 were waited for; matrix products, arithmetic and copies ran while one was open for 6% of the time, Pallas kernels for 30%

profile of v1, /device:TPU:32, one launch (start us, length us, event | category | flops | bytes accessed | tf_op | source)
XLA Modules:
  0.0 185.2 jit_solution(6834953279321683548)
XLA Ops:
  9.4 7.0 %all-to-all-start = ((f32[16,32,128]{2,1,0:T(8,128)}), f32[16,32,128]{2,1,0:T(8,128)S(1)}, u32[]{:S(2)}, u32[]{:S(2)}) async-start(f32[16,32,128]{2,1,0:T(8,128)} %broadcast_in_dim.10), calls=%async_computation | async-start | bytes 524288 | tf_op jit(solution)/shard_map/all_to_all | solution.py:410
  16.4 1.1 fusion.20
  17.4 2.0 %collective-permute-start = (bf16[32,2048]{1,0:T(8,128)(2,1)S(1)}, bf16[32,2048]{1,0:T(8,128)(2,1)S(1)}, u32[]{:S(2)}, u32[]{:S(2)}) collective-permute-start(bf16[32,2048]{1,0:T(8,128)(2,1)S(1)} %fusion.20), channel_id=1, source_target_pairs={{0,16},{16,32},{32,48},{48,64},{64,80},{80,96},{96,112},{112,128},... | collective-permute-start | bytes 393224 | tf_op jit(solution)/shard_map/ppermute | solution.py:435
  20.1 6.2 %shard_map.101 = (bf16[8,128,256]{2,1,0:T(8,128)(2,1)}, bf16[8,128,256]{2,1,0:T(8,128)(2,1)}) custom-call(s32[4]{0:T(128)} %pad_add_fusion.ring, bf16[256,2048]{1,0:T(8,128)(2,1)} %bitcast.95), custom_call_target="tpu_custom_call" | custom-call | flops 52428800 | bytes 2097152 | tf_op jit(solution)/shard_map/pallas_call | solution.py:143
  26.3 1.3 collective-permute-done.halo
  28.4 10.9 %shard_map.102 = (bf16[256,2048]{1,0:T(8,128)(2,1)}, bf16[256,2048]{1,0:T(8,128)(2,1)}, bf16[256,2048]{1,0:T(8,128)(2,1)}, f32[256,128]{1,0:T(8,128)}, f32[256,128]{1,0:T(8,128)}) custom-call(s32[4]{0:T(128)} %pad_add_fusion.ring, bf16[256,2048]{1,0:T(8,128)(2,1)} %bitcast.102, bf16[256,2048]{1,0:T(8,128)(2,1)} %bitcast.104, bf16[32,2048]{1,0:T(8,128)(2,1)} %copy-done.5, ...), custom_call_target="tpu_custom_call" | custom-call | flops 3250585600 | bytes 5242880 | tf_op jit(solution)/shard_map/pallas_call | solution.py:101
  39.9 3.5 %collective-permute-done.1.turned_other = bf16[8,128,256]{2,1,0:T(8,128)(2,1)S(1)} collective-permute-done((bf16[8,128,256]{2,1,0:T(8,128)(2,1)S(1)}, bf16[8,128,256]{2,1,0:T(8,128)(2,1)S(1)}, u32[]{:S(2)}, u32[]{:S(2)}) %collective-permute-start.1) | collective-permute-done | bytes 524320 | tf_op jit(solution)/shard_map/ppermute | solution.py:43
  43.4 0.8 copy-done.3
  44.2 1.0 copy-done.2
  45.1 4.9 %shard_map.104 = (bf16[4,512,128]{2,1,0:T(8,128)(2,1)}, bf16[4,512,128]{2,1,0:T(8,128)(2,1)}, bf16[4,512,128]{2,1,0:T(8,128)(2,1)}, bf16[4,512,128]{2,1,0:T(8,128)(2,1)}) custom-call(s32[4]{0:T(128)} %pad_add_fusion.ring, bf16[8,128,256]{2,1,0:T(8,128)(2,1)} %get-tuple-element.29.turned, bf16[8,128,256]{2,1,0:T(8,128)(2,1)} %copy-done.3, ...), custom_call_target="tpu_custom_call" | custom-call | flops 1073741824 | bytes 4194304 | tf_op jit(solution)/shard_map/pallas_call | solution.py:183
  50.0 1.4 collective-permute-start.4
  52.0 1.4 collective-permute-start.6
  54.1 4.8 %shard_map.103 = (bf16[2,512,128]{2,1,0:T(8,128)(2,1)}, bf16[2,512,128]{2,1,0:T(8,128)(2,1)}, bf16[4,512,128]{2,1,0:T(8,128)(2,1)}, bf16[2,512,128]{2,1,0:T(8,12...) custom-call(s32[4]{0:T(128)} %pad_add_fusion.ring, bf16[8,128,256]{2,1,0:T(8,128)(2,1)} %get-tuple-element.29.turned, ...), custom_call_target="tpu_custom_call" | custom-call | flops 1073741824 | bytes 4194304 | tf_op jit(solution)/shard_map/pallas_call | solution.py:183
  58.9 5.3 %collective-permute-done.4 = bf16[4,512,128]{2,1,0:T(8,128)(2,1)S(1)} collective-permute-done((bf16[4,512,128]{2,1,0:T(8,128)(2,1)}, bf16[4,512,128]{2,1,0:T(8,128)(2,1)S(1)}, u32[]{:S(2)}, u32[]{:S(2)}) %collective-permute-start.4) | collective-permute-done | bytes 524320 | tf_op jit(solution)/shard_map/ppermute | solution.py:43
  64.2 1.0 add_convert_fusion.2
  65.2 2.6 %collective-permute-start.9 = (bf16[2,512,128]{2,1,0:T(8,128)(2,1)S(1)}, bf16[2,512,128]{2,1,0:T(8,128)(2,1)S(1)}, u32[]{:S(2)}, u32[]{:S(2)}) collective-permute-start(bf16[2,512,128]{2,1,0:T(8,128)(2,1)S(1)} %add_convert_fusion.2), channel_id=1, source_target_pairs={{0,48},{16,0},{32,16},{48,32},{1,49},{17,1},{33,17},{49,33},{2,50}... | collective-permute-start | bytes 786440 | tf_op jit(solution)/shard_map/ppermute | solution.py:43
  67.9 1.0 add_convert_fusion.3
  69.0 1.0 add_convert_fusion
  70.0 1.6 collective-permute-start.15
  71.6 1.0 add_convert_fusion.1
  72.6 0.8 collective-permute-start.14
  73.4 4.0 %collective-permute-done.8 = bf16[2,512,128]{2,1,0:T(8,128)(2,1)S(1)} collective-permute-done((bf16[2,512,128]{2,1,0:T(8,128)(2,1)S(1)}, bf16[2,512,128]{2,1,0:T(8,128)(2,1)S(1)}, u32[]{:S(2)}, u32[]{:S(2)}) %collective-permute-start.8) | collective-permute-done | bytes 262176 | tf_op jit(solution)/shard_map/ppermute | solution.py:43
  77.4 1.2 fusion.23
  78.6 1.4 collective-permute-start.12
  80.1 0.8 collective-permute-start.10
  80.9 1.2 fusion.24
  82.1 4.4 %collective-permute-start.18 = (bf16[512,128]{1,0:T(8,128)(2,1)S(1)}, bf16[512,128]{1,0:T(8,128)(2,1)S(1)}, u32[]{:S(2)}, u32[]{:S(2)}) collective-permute-start(bf16[512,128]{1,0:T(8,128)(2,1)S(1)} %pad_maximum_fusion.5), channel_id=1, source_target_pairs={{0,48},{16,0},{32,16},{48,32},{1,49},{17,1},{33,17},{49,33},{2,50}... | collective-permute-start | bytes 393224 | tf_op jit(solution)/shard_map/ppermute | solution.py:43
  87.4 2.3 %collective-permute-done.18 = bf16[512,128]{1,0:T(8,128)(2,1)S(1)} collective-permute-done((bf16[512,128]{1,0:T(8,128)(2,1)S(1)}, bf16[512,128]{1,0:T(8,128)(2,1)S(1)}, u32[]{:S(2)}, u32[]{:S(2)}) %collective-permute-start.18) | collective-permute-done | bytes 131104 | tf_op jit(solution)/shard_map/ppermute | solution.py:43
  89.7 3.8 %collective-permute-start.19 = (bf16[256,128]{1,0:T(8,128)(2,1)S(1)}, bf16[256,128]{1,0:T(8,128)(2,1)S(1)}, u32[]{:S(2)}, u32[]{:S(2)}) collective-permute-start(bf16[256,128]{1,0:T(8,128)(2,1)S(1)} %fusion.1), channel_id=1, source_target_pairs={{0,48},{16,0},{32,16},{48,32},{1,49},{17,1},{33,17},{49,33},{2,50}... | collective-permute-start | bytes 196616 | tf_op jit(solution)/shard_map/ppermute | solution.py:43
  93.6 1.8 collective-permute-done.19
  95.6 11.1 %shard_map.105 = (bf16[256,2048]{1,0:T(8,128)(2,1)}, bf16[32,2048]{1,0:T(8,128)(2,1)}, f32[16,128]{1,0:T(8,128)}) custom-call(s32[4]{0:T(128)} %pad_add_fusion.ring, bf16[256,2048]{1,0:T(8,128)(2,1)} %bitcast.96, bf16[2048,2048]{1,0:T(8,128)(2,1)} %all-gather.2.cloned.1.call-done.weight, bf16[256,2048]{1,0:T(8,128)(2,1)} %get-tuple-element.31.conv, ...), custom_call_target="tpu_custom_call" | custom-call | flops 2147483648 | bytes 11534336 | tf_op jit(solution)/shard_map/pallas_call | solution.py:311
  106.6 7.9 %shard_map.107 = f32[16,48,128]{2,1,0:T(8,128)} custom-call(s32[4]{0:T(128)} %pad_add_fusion.ring, bf16[256,2048]{1,0:T(8,128)(2,1)} %get-tuple-element.51.glu, bf16[32,2048]{1,0:T(8,128)(2,1)} %copy-done.5, bf16[256,2048]{1,0:T(8,128)(2,1)} %get-tuple-element.45.grad, f32[16,128]{1,0:T(8,128)} %get-tuple-element.52.gain_part), custom_call_target="tpu_custom_call" | custom-call | flops 3250585600 | bytes 2097152 | tf_op jit(solution)/shard_map/pallas_call | solution.py:357
  114.5 6.8 %all-to-all-start.1 = ((f32[16,48,128]{2,1,0:T(8,128)}), f32[16,48,128]{2,1,0:T(8,128)S(1)}, u32[]{:S(2)}, u32[]{:S(2)}) async-start(f32[16,48,128]{2,1,0:T(8,128)} %shard_map.107), calls=%async_computation.1 | async-start | bytes 786432 | tf_op jit(solution)/shard_map/all_to_all | solution.py:461
  121.4 9.3 %all-to-all-done.1 = f32[16,48,128]{2,1,0:T(8,128)S(1)} async-done(((f32[16,48,128]{2,1,0:T(8,128)}), f32[16,48,128]{2,1,0:T(8,128)S(1)}, u32[]{:S(2)}, u32[]{:S(2)}) %all-to-all-start.1) | async-done | bytes 393248 | tf_op jit(solution)/shard_map/all_to_all | solution.py:461
  130.9 1.2 collective-permute-done.20
  132.1 0.8 pad_maximum_fusion
  132.8 8.6 %all-to-all-start.2 = ((bf16[8,176,128]{2,1,0:T(8,128)(2,1)}), bf16[8,176,128]{2,1,0:T(8,128)(2,1)S(1)}, u32[]{:S(2)}, u32[]{:S(2)}) async-start(bf16[8,176,128]{2,1,0:T(8,128)(2,1)} %pad_maximum_fusion), calls=%async_computation.2 | async-start | bytes 720896 | tf_op jit(solution)/shard_map/all_to_all | solution.py:467
  141.4 1.2 collective-permute-start.7
  142.5 3.8 %collective-permute-done.7.tail = bf16[32,2048]{1,0:T(8,128)(2,1)S(1)} collective-permute-done((bf16[32,2048]{1,0:T(8,128)(2,1)S(1)}, bf16[32,2048]{1,0:T(8,128)(2,1)S(1)}, u32[]{:S(2)}, u32[]{:S(2)}) %collective-permute-start.7) | collective-permute-done | bytes 131104 | tf_op jit(solution)/shard_map/ppermute | solution.py:454
  147.0 9.1 %shard_map.106 = (bf16[256,2048]{1,0:T(8,128)(2,1)}, bf16[256,2048]{1,0:T(8,128)(2,1)}) custom-call(s32[4]{0:T(128)} %pad_add_fusion.ring, bf16[256,2048]{1,0:T(8,128)(2,1)} %get-tuple-element.45.grad, bf16[32,2048]{1,0:T(8,128)(2,1)} %copy-done.7, f32[16,32,128]{2,1,0:T(8,128)} %copy-done.1, bf16[256,2048]{1,0:T(8,128)(2,1)} %bitcast.103, ...), custom_call_target="tpu_custom_call" | custom-call | flops 3250585600 | bytes 5242880 | tf_op jit(solution)/shard_map/pallas_call | solution.py:390
  156.2 2.7 %collective-permute-start.21 = (bf16[128,128]{1,0:T(8,128)(2,1)S(1)}, bf16[128,128]{1,0:T(8,128)(2,1)S(1)}, u32[]{:S(2)}, u32[]{:S(2)}) collective-permute-start(bf16[128,128]{1,0:T(8,128)(2,1)S(1)} %get-tuple-element.54), channel_id=1, source_target_pairs={{0,48},{16,0},{32,16},{48,32},{1,49},{17,1},{33,17},{49,33},{2,50}... | collective-permute-start | bytes 98312 | tf_op jit(solution)/shard_map/ppermute | solution.py:43
  158.9 1.0 collective-permute-start.23
  160.5 3.9 %collective-permute-done.22 = bf16[128,128]{1,0:T(8,128)(2,1)S(1)} collective-permute-done((bf16[128,128]{1,0:T(8,128)(2,1)S(1)}, bf16[128,128]{1,0:T(8,128)(2,1)S(1)}, u32[]{:S(2)}, u32[]{:S(2)}) %collective-permute-start.22) | collective-permute-done | bytes 32800 | tf_op jit(solution)/shard_map/ppermute | solution.py:43
  164.4 2.5 %collective-permute-start.24 = (bf16[4,128,128]{2,1,0:T(8,128)(2,1)S(1)}, bf16[4,128,128]{2,1,0:T(8,128)(2,1)S(1)}, u32[]{:S(2)}, u32[]{:S(2)}) collective-permute-start(bf16[4,128,128]{2,1,0:T(8,128)(2,1)S(1)} %pad_maximum_fusion.6), channel_id=1, source_target_pairs={{0,192},{64,0},{128,64},{192,128},{1,193},{65,1},{129,65},{193,129... | collective-permute-start | bytes 393224 | tf_op jit(solution)/shard_map/ppermute | solution.py:43
  167.9 2.9 %collective-permute-done.24 = bf16[4,128,128]{2,1,0:T(8,128)(2,1)S(1)} collective-permute-done((bf16[4,128,128]{2,1,0:T(8,128)(2,1)S(1)}, bf16[4,128,128]{2,1,0:T(8,128)(2,1)S(1)}, u32[]{:S(2)}, u32[]{:S(2)}) %collective-permute-start.24) | collective-permute-done | bytes 131104 | tf_op jit(solution)/shard_map/ppermute | solution.py:43
  170.8 2.6 %collective-permute-done.25 = bf16[4,128,128]{2,1,0:T(8,128)(2,1)S(1)} collective-permute-done((bf16[4,128,128]{2,1,0:T(8,128)(2,1)S(1)}, bf16[4,128,128]{2,1,0:T(8,128)(2,1)S(1)}, u32[]{:S(2)}, u32[]{:S(2)}) %collective-permute-start.25) | collective-permute-done | bytes 131104 | tf_op jit(solution)/shard_map/ppermute | solution.py:43
  173.5 1.2 collective-permute-done.26
  175.5 2.8 %shard_map.108 = f32[128,2048]{1,0:T(8,128)} custom-call(s32[4]{0:T(128)} %pad_add_fusion.ring, bf16[16,128,128]{2,1,0:T(8,128)(2,1)} %copy-done), custom_call_target="tpu_custom_call" | custom-call | flops 262144 | bytes 1572864 | tf_op jit(solution)/shard_map/pallas_call | solution.py:239
  (79 shorter events, 10.2 us)
Async XLA Ops:
  7.2 88.4 %all-gather.2.cloned.1.call-start = ((), (), s32[]{:S(2)}) async-start(), calls=%async_computation.3 | async-start | bytes 8912896 | tf_op jit(solution)/shard_map/all_gather | solution.py:432
  9.4 18.2 %all-to-all-start = ((f32[16,32,128]{2,1,0:T(8,128)}), f32[16,32,128]{2,1,0:T(8,128)S(1)}, u32[]{:S(2)}, u32[]{:S(2)}) async-start(f32[16,32,128]{2,1,0:T(8,128)} %broadcast_in_dim.10), calls=%async_computation | async-start | bytes 524288 | tf_op jit(solution)/shard_map/all_to_all | solution.py:410
  17.4 10.1 %collective-permute-start = (bf16[32,2048]{1,0:T(8,128)(2,1)S(1)}, bf16[32,2048]{1,0:T(8,128)(2,1)S(1)}, u32[]{:S(2)}, u32[]{:S(2)}) collective-permute-start(bf16[32,2048]{1,0:T(8,128)(2,1)S(1)} %fusion.20), channel_id=1, source_target_pairs={{0,16},{16,32},{32,48},{48,64},{64,80},{80,96},{96,112},{112,128},... | collective-permute-start | bytes 393224 | tf_op jit(solution)/shard_map/ppermute | solution.py:435
  26.3 13.1 %copy-start.4 = (bf16[8,128,256]{2,1,0:T(8,128)(2,1)S(1)}, bf16[8,128,256]{2,1,0:T(8,128)(2,1)}, u32[]{:S(2)}) copy-start(bf16[8,128,256]{2,1,0:T(8,128)(2,1)} %get-tuple-element.34) | copy-start | bytes 1572868
  27.6 0.6 copy-start.5
  27.6 0.8 copy-start.1
  39.3 4.1 %collective-permute-start.2 = (bf16[256,2048]{1,0:T(8,128)(2,1)}, bf16[256,2048]{1,0:T(8,128)(2,1)S(1)}, u32[]{:S(2)}, u32[]{:S(2)}) collective-permute-start(bf16[256,2048]{1,0:T(8,128)(2,1)} %get-tuple-element.35.act), channel_id=1, source_target_pairs={{0,1},{1,0},{2,3},{3,2},{4,5},{5,4},{6,7},{7,6},{8,9},{9,8},{10,11... | collective-permute-start | bytes 3145736 | tf_op jit(solution)/shard_map/ppermute | solution.py:43
  39.4 4.0 %collective-permute-start.1 = (bf16[8,128,256]{2,1,0:T(8,128)(2,1)S(1)}, bf16[8,128,256]{2,1,0:T(8,128)(2,1)S(1)}, u32[]{:S(2)}, u32[]{:S(2)}) collective-permute-start(bf16[8,128,256]{2,1,0:T(8,128)(2,1)S(1)} %copy-done.4), channel_id=1, source_target_pairs={{0,1},{1,0},{2,3},{3,2},{4,5},{5,4},{6,7},{7,6},{8,9},{9,8},{10,11... | collective-permute-start | bytes 1572872 | tf_op jit(solution)/shard_map/ppermute | solution.py:43
  43.4 0.8 copy-start.3
  44.2 1.0 copy-start.2
  50.0 14.2 %collective-permute-start.4 = (bf16[4,512,128]{2,1,0:T(8,128)(2,1)}, bf16[4,512,128]{2,1,0:T(8,128)(2,1)S(1)}, u32[]{:S(2)}, u32[]{:S(2)}) collective-permute-start(bf16[4,512,128]{2,1,0:T(8,128)(2,1)} %get-tuple-element.39), channel_id=1, source_target_pairs={{0,48},{16,0},{32,16},{48,32},{1,49},{17,1},{33,17},{49,33},{2,50}... | collective-permute-start | bytes 1572872 | tf_op jit(solution)/shard_map/ppermute | solution.py:43
  51.4 16.5 %collective-permute-start.3 = (bf16[4,512,128]{2,1,0:T(8,128)(2,1)}, bf16[4,512,128]{2,1,0:T(8,128)(2,1)S(1)}, u32[]{:S(2)}, u32[]{:S(2)}) collective-permute-start(bf16[4,512,128]{2,1,0:T(8,128)(2,1)} %get-tuple-element.37), channel_id=1, source_target_pairs={{0,16},{16,32},{32,48},{48,0},{1,17},{17,33},{33,49},{49,1},{2,18}... | collective-permute-start | bytes 1572872 | tf_op jit(solution)/shard_map/ppermute | solution.py:43
  52.0 16.9 %collective-permute-start.6 = (bf16[4,512,128]{2,1,0:T(8,128)(2,1)}, bf16[4,512,128]{2,1,0:T(8,128)(2,1)S(1)}, u32[]{:S(2)}, u32[]{:S(2)}) collective-permute-start(bf16[4,512,128]{2,1,0:T(8,128)(2,1)} %get-tuple-element.43), channel_id=1, source_target_pairs={{0,192},{64,0},{128,64},{192,128},{1,193},{65,1},{129,65},{193,129... | collective-permute-start | bytes 1572872 | tf_op jit(solution)/shard_map/ppermute | solution.py:43
  53.4 18.2 %collective-permute-start.5 = (bf16[4,512,128]{2,1,0:T(8,128)(2,1)}, bf16[4,512,128]{2,1,0:T(8,128)(2,1)S(1)}, u32[]{:S(2)}, u32[]{:S(2)}) collective-permute-start(bf16[4,512,128]{2,1,0:T(8,128)(2,1)} %get-tuple-element.41), channel_id=1, source_target_pairs={{0,64},{64,128},{128,192},{192,0},{1,65},{65,129},{129,193},{193,1... | collective-permute-start | bytes 1572872 | tf_op jit(solution)/shard_map/ppermute | solution.py:43
  65.2 8.2 %collective-permute-start.9 = (bf16[2,512,128]{2,1,0:T(8,128)(2,1)S(1)}, bf16[2,512,128]{2,1,0:T(8,128)(2,1)S(1)}, u32[]{:S(2)}, u32[]{:S(2)}) collective-permute-start(bf16[2,512,128]{2,1,0:T(8,128)(2,1)S(1)} %add_convert_fusion.2), channel_id=1, source_target_pairs={{0,48},{16,0},{32,16},{48,32},{1,49},{17,1},{33,17},{49,33},{2,50}... | collective-permute-start | bytes 786440 | tf_op jit(solution)/shard_map/ppermute | solution.py:43
  68.9 8.5 %collective-permute-start.8 = (bf16[2,512,128]{2,1,0:T(8,128)(2,1)S(1)}, bf16[2,512,128]{2,1,0:T(8,128)(2,1)S(1)}, u32[]{:S(2)}, u32[]{:S(2)}) collective-permute-start(bf16[2,512,128]{2,1,0:T(8,128)(2,1)S(1)} %add_convert_fusion.3), channel_id=1, source_target_pairs={{0,16},{16,32},{32,48},{48,0},{1,17},{17,33},{33,49},{49,1},{2,18}... | collective-permute-start | bytes 786440 | tf_op jit(solution)/shard_map/ppermute | solution.py:43
  70.0 10.8 %collective-permute-start.15 = (bf16[2,512,128]{2,1,0:T(8,128)(2,1)S(1)}, bf16[2,512,128]{2,1,0:T(8,128)(2,1)S(1)}, u32[]{:S(2)}, u32[]{:S(2)}) collective-permute-start(bf16[2,512,128]{2,1,0:T(8,128)(2,1)S(1)} %add_convert_fusion), channel_id=1, source_target_pairs={{0,192},{64,0},{128,64},{192,128},{1,193},{65,1},{129,65},{193,129... | collective-permute-start | bytes 786440 | tf_op jit(solution)/shard_map/ppermute | solution.py:43
  72.6 8.2 %collective-permute-start.14 = (bf16[2,512,128]{2,1,0:T(8,128)(2,1)S(1)}, bf16[2,512,128]{2,1,0:T(8,128)(2,1)S(1)}, u32[]{:S(2)}, u32[]{:S(2)}) collective-permute-start(bf16[2,512,128]{2,1,0:T(8,128)(2,1)S(1)} %add_convert_fusion.1), channel_id=1, source_target_pairs={{0,64},{64,128},{128,192},{192,0},{1,65},{65,129},{129,193},{193,1... | collective-permute-start | bytes 786440 | tf_op jit(solution)/shard_map/ppermute | solution.py:43
  78.6 8.0 %collective-permute-start.12 = (bf16[512,128]{1,0:T(8,128)(2,1)S(1)}, bf16[512,128]{1,0:T(8,128)(2,1)S(1)}, u32[]{:S(2)}, u32[]{:S(2)}) collective-permute-start(bf16[512,128]{1,0:T(8,128)(2,1)S(1)} %pad_maximum_fusion.3), channel_id=1, source_target_pairs={{0,192},{64,0},{128,64},{192,128},{1,193},{65,1},{129,65},{193,129... | collective-permute-start | bytes 393224 | tf_op jit(solution)/shard_map/ppermute | solution.py:43
  80.1 13.4 %collective-permute-start.10 = (bf16[512,128]{1,0:T(8,128)(2,1)S(1)}, bf16[512,128]{1,0:T(8,128)(2,1)S(1)}, u32[]{:S(2)}, u32[]{:S(2)}) collective-permute-start(bf16[512,128]{1,0:T(8,128)(2,1)S(1)} %pad_maximum_fusion.2), channel_id=1, source_target_pairs={{0,64},{64,128},{128,192},{192,0},{1,65},{65,129},{129,193},{193,1... | collective-permute-start | bytes 393224 | tf_op jit(solution)/shard_map/ppermute | solution.py:43
  82.1 7.6 %collective-permute-start.18 = (bf16[512,128]{1,0:T(8,128)(2,1)S(1)}, bf16[512,128]{1,0:T(8,128)(2,1)S(1)}, u32[]{:S(2)}, u32[]{:S(2)}) collective-permute-start(bf16[512,128]{1,0:T(8,128)(2,1)S(1)} %pad_maximum_fusion.5), channel_id=1, source_target_pairs={{0,48},{16,0},{32,16},{48,32},{1,49},{17,1},{33,17},{49,33},{2,50}... | collective-permute-start | bytes 393224 | tf_op jit(solution)/shard_map/ppermute | solution.py:43
  86.5 7.1 %collective-permute-start.16 = (bf16[512,128]{1,0:T(8,128)(2,1)S(1)}, bf16[512,128]{1,0:T(8,128)(2,1)S(1)}, u32[]{:S(2)}, u32[]{:S(2)}) collective-permute-start(bf16[512,128]{1,0:T(8,128)(2,1)S(1)} %pad_maximum_fusion.4), channel_id=1, source_target_pairs={{0,16},{16,32},{32,48},{48,0},{1,17},{17,33},{33,49},{49,1},{2,18}... | collective-permute-start | bytes 393224 | tf_op jit(solution)/shard_map/ppermute | solution.py:43
  86.7 6.8 %collective-permute-start.13 = (bf16[256,128]{1,0:T(8,128)(2,1)S(1)}, bf16[256,128]{1,0:T(8,128)(2,1)S(1)}, u32[]{:S(2)}, u32[]{:S(2)}) collective-permute-start(bf16[256,128]{1,0:T(8,128)(2,1)S(1)} %fusion.11), channel_id=1, source_target_pairs={{0,192},{64,0},{128,64},{192,128},{1,193},{65,1},{129,65},{193,129... | collective-permute-start | bytes 196616 | tf_op jit(solution)/shard_map/ppermute | solution.py:43
  89.7 5.7 %collective-permute-start.19 = (bf16[256,128]{1,0:T(8,128)(2,1)S(1)}, bf16[256,128]{1,0:T(8,128)(2,1)S(1)}, u32[]{:S(2)}, u32[]{:S(2)}) collective-permute-start(bf16[256,128]{1,0:T(8,128)(2,1)S(1)} %fusion.1), channel_id=1, source_target_pairs={{0,48},{16,0},{32,16},{48,32},{1,49},{17,1},{33,17},{49,33},{2,50}... | collective-permute-start | bytes 196616 | tf_op jit(solution)/shard_map/ppermute | solution.py:43
  93.5 27.8 %collective-permute-start.11 = (bf16[256,128]{1,0:T(8,128)(2,1)S(1)}, bf16[256,128]{1,0:T(8,128)(2,1)S(1)}, u32[]{:S(2)}, u32[]{:S(2)}) collective-permute-start(bf16[256,128]{1,0:T(8,128)(2,1)S(1)} %get-tuple-element.59), channel_id=1, source_target_pairs={{0,64},{64,128},{128,192},{192,0},{1,65},{65,129},{129,193},{193,1... | collective-permute-start | bytes 196616 | tf_op jit(solution)/shard_map/ppermute | solution.py:43
  95.4 25.9 %collective-permute-start.17 = (bf16[256,128]{1,0:T(8,128)(2,1)S(1)}, bf16[256,128]{1,0:T(8,128)(2,1)S(1)}, u32[]{:S(2)}, u32[]{:S(2)}) collective-permute-start(bf16[256,128]{1,0:T(8,128)(2,1)S(1)} %get-tuple-element.61), channel_id=1, source_target_pairs={{0,16},{16,32},{32,48},{48,0},{1,17},{17,33},{33,49},{49,1},{2,18}... | collective-permute-start | bytes 196616 | tf_op jit(solution)/shard_map/ppermute | solution.py:43
  106.6 34.7 %copy-start.6 = (bf16[32,2048]{1,0:T(8,128)(2,1)S(1)}, bf16[32,2048]{1,0:T(8,128)(2,1)}, u32[]{:S(2)}) copy-start(bf16[32,2048]{1,0:T(8,128)(2,1)} %get-tuple-element.46) | copy-start | bytes 393220
  114.5 16.2 %all-to-all-start.1 = ((f32[16,48,128]{2,1,0:T(8,128)}), f32[16,48,128]{2,1,0:T(8,128)S(1)}, u32[]{:S(2)}, u32[]{:S(2)}) async-start(f32[16,48,128]{2,1,0:T(8,128)} %shard_map.107), calls=%async_computation.1 | async-start | bytes 786432 | tf_op jit(solution)/shard_map/all_to_all | solution.py:461
  130.7 1.3 collective-permute-start.20
  132.8 23.3 %all-to-all-start.2 = ((bf16[8,176,128]{2,1,0:T(8,128)(2,1)}), bf16[8,176,128]{2,1,0:T(8,128)(2,1)S(1)}, u32[]{:S(2)}, u32[]{:S(2)}) async-start(bf16[8,176,128]{2,1,0:T(8,128)(2,1)} %pad_maximum_fusion), calls=%async_computation.2 | async-start | bytes 720896 | tf_op jit(solution)/shard_map/all_to_all | solution.py:467
  141.4 5.0 %collective-permute-start.7 = (bf16[32,2048]{1,0:T(8,128)(2,1)S(1)}, bf16[32,2048]{1,0:T(8,128)(2,1)S(1)}, u32[]{:S(2)}, u32[]{:S(2)}) collective-permute-start(bf16[32,2048]{1,0:T(8,128)(2,1)S(1)} %copy-done.6), channel_id=1, source_target_pairs={{16,0},{32,16},{48,32},{64,48},{80,64},{96,80},{112,96},{128,112},... | collective-permute-start | bytes 393224 | tf_op jit(solution)/shard_map/ppermute | solution.py:454
  146.4 0.7 copy-start.7
  156.2 4.3 %collective-permute-start.21 = (bf16[128,128]{1,0:T(8,128)(2,1)S(1)}, bf16[128,128]{1,0:T(8,128)(2,1)S(1)}, u32[]{:S(2)}, u32[]{:S(2)}) collective-permute-start(bf16[128,128]{1,0:T(8,128)(2,1)S(1)} %get-tuple-element.54), channel_id=1, source_target_pairs={{0,48},{16,0},{32,16},{48,32},{1,49},{17,1},{33,17},{49,33},{2,50}... | collective-permute-start | bytes 98312 | tf_op jit(solution)/shard_map/ppermute | solution.py:43
  158.9 5.5 %collective-permute-start.22 = (bf16[128,128]{1,0:T(8,128)(2,1)S(1)}, bf16[128,128]{1,0:T(8,128)(2,1)S(1)}, u32[]{:S(2)}, u32[]{:S(2)}) collective-permute-start(bf16[128,128]{1,0:T(8,128)(2,1)S(1)} %get-tuple-element.54), channel_id=1, source_target_pairs={{0,32},{16,48},{32,0},{48,16},{1,33},{17,49},{33,1},{49,17},{2,34}... | collective-permute-start | bytes 98312 | tf_op jit(solution)/shard_map/ppermute | solution.py:43
  158.9 5.5 %collective-permute-start.23 = (bf16[128,128]{1,0:T(8,128)(2,1)S(1)}, bf16[128,128]{1,0:T(8,128)(2,1)S(1)}, u32[]{:S(2)}, u32[]{:S(2)}) collective-permute-start(bf16[128,128]{1,0:T(8,128)(2,1)S(1)} %get-tuple-element.54), channel_id=1, source_target_pairs={{0,16},{16,32},{32,48},{48,0},{1,17},{17,33},{33,49},{49,1},{2,18}... | collective-permute-start | bytes 98312 | tf_op jit(solution)/shard_map/ppermute | solution.py:43
  164.4 6.4 %collective-permute-start.24 = (bf16[4,128,128]{2,1,0:T(8,128)(2,1)S(1)}, bf16[4,128,128]{2,1,0:T(8,128)(2,1)S(1)}, u32[]{:S(2)}, u32[]{:S(2)}) collective-permute-start(bf16[4,128,128]{2,1,0:T(8,128)(2,1)S(1)} %pad_maximum_fusion.6), channel_id=1, source_target_pairs={{0,192},{64,0},{128,64},{192,128},{1,193},{65,1},{129,65},{193,129... | collective-permute-start | bytes 393224 | tf_op jit(solution)/shard_map/ppermute | solution.py:43
  166.9 6.6 %collective-permute-start.25 = (bf16[4,128,128]{2,1,0:T(8,128)(2,1)S(1)}, bf16[4,128,128]{2,1,0:T(8,128)(2,1)S(1)}, u32[]{:S(2)}, u32[]{:S(2)}) collective-permute-start(bf16[4,128,128]{2,1,0:T(8,128)(2,1)S(1)} %pad_maximum_fusion.6), channel_id=1, source_target_pairs={{0,128},{64,192},{128,0},{192,64},{1,129},{65,193},{129,1},{193,65... | collective-permute-start | bytes 393224 | tf_op jit(solution)/shard_map/ppermute | solution.py:43
  167.1 7.6 %collective-permute-start.26 = (bf16[4,128,128]{2,1,0:T(8,128)(2,1)S(1)}, bf16[4,128,128]{2,1,0:T(8,128)(2,1)S(1)}, u32[]{:S(2)}, u32[]{:S(2)}) collective-permute-start(bf16[4,128,128]{2,1,0:T(8,128)(2,1)S(1)} %pad_maximum_fusion.6), channel_id=1, source_target_pairs={{0,64},{64,128},{128,192},{192,0},{1,65},{65,129},{129,193},{193,1... | collective-permute-start | bytes 393224 | tf_op jit(solution)/shard_map/ppermute | solution.py:43
  174.7 0.8 copy-start
Sparse Core Ops, SparseCore 0:
  9.8 56.6 all-gather.1

commit v2 on v1

--- a/solution.py
+++ b/solution.py
@@ -14,12 +14,12 @@
 NORM_EPS = 1e-05
 HALO = 32
 GROUP = 4
-VMEM_LIMIT = 60
+VMEM_MIB = {'forward': 60, 'input_backward': 60, 'turn': 16, 'outer_early': 16, 'outer_rest': 16, 'place': 16, 'taps_backward': 16, 'norm_backward': 52}
 INTERPRET = False
 F32, BF16 = jnp.float32, jnp.bfloat16
 
 
-def call(kernel, grid, in_specs, out_specs, out_shape, scratch, flops=0, moved=0):
+def call(kernel, name, grid, in_specs, out_specs, out_shape, scratch, flops=0, moved=0):
     return pl.pallas_call(
         kernel,
         grid_spec=pltpu.PrefetchScalarGridSpec(
@@ -31,7 +31,7 @@
         ),
         out_shape=out_shape,
         compiler_params=pltpu.CompilerParams(
-            dimension_semantics=("arbitrary",) * len(grid), vmem_limit_bytes=VMEM_LIMIT * 1024 * 1024
+            dimension_semantics=("arbitrary",) * len(grid), vmem_limit_bytes=VMEM_MIB.get(name, 48) * 1024 * 1024
         ),
         cost_estimate=pl.CostEstimate(flops=flops, bytes_accessed=moved, transcendentals=0),
         interpret=INTERPRET,
@@ -100,6 +100,7 @@
     whole = lambda *shape: pl.BlockSpec(shape, lambda i, ring: (0,) * len(shape))
     return call(
         forward_kernel,
+        "forward",
         (16 // GROUP,),
         [
             column(tokens),
@@ -142,6 +143,7 @@
     shape = jax.ShapeDtypeStruct((8, lanes, tokens), BF16)
     return call(
         turn_kernel,
+        "turn",
         (8,),
         [pl.BlockSpec((tokens, 2 * lanes), lambda i, ring: (0, i))],
         [out, out],
@@ -175,13 +177,14 @@
         out[at + 1] = product[:, lanes:].astype(BF16)
 
 
-def outer(plan, ring, turned, turned_other, act, act_other):
+def outer(name, plan, ring, turned, turned_other, act, act_other):
     tokens, width = act.shape
     lanes = width // 16
     whole = lambda *shape: pl.BlockSpec(shape, lambda i, ring: (0,) * len(shape))
     sizes = [max(at for *_, target, at in plan if target == out) + 2 for out in range(plan[-1][3] + 1)]
     return call(
         functools.partial(outer_kernel, plan),
+        name,
         (1,),
         [whole(8, lanes, tokens)] * 2 + [whole(tokens, width)] * 2,
         [whole(size, 4 * lanes, lanes) for size in sizes],
@@ -238,6 +241,7 @@
     whole = lambda *shape: pl.BlockSpec(shape, lambda i, ring: (0,) * len(shape))
     return call(
         place_kernel,
+        "place",
         (1,),
         [whole(count, rows, lanes)],
         whole(rows, count * lanes),
@@ -310,6 +314,7 @@
     whole = lambda *shape: pl.BlockSpec(shape, lambda i, ring: (0,) * len(shape))
     return call(
         norm_kernel,
+        "norm_backward",
         (8,),
         [
             whole(tokens, width),
@@ -356,6 +361,7 @@
     column = lambda rows: pl.BlockSpec((rows, GROUP * lanes), lambda i, ring: (0, i))
     return call(
         taps_kernel,
+        "taps_backward",
         (16 // GROUP,),
         [column(tokens), column(HALO), column(tokens), pl.BlockSpec((16, lanes), lambda i, ring: (0, 0))],
         pl.BlockSpec((GROUP, 48, lanes), lambda i, ring: (i, 0, 0)),
@@ -389,6 +395,7 @@
     column = lambda rows: pl.BlockSpec((rows, GROUP * lanes), lambda i, ring: (0, i))
     return call(
         input_kernel,
+        "input_backward",
         (16 // GROUP,),
         [
             column(tokens),
@@ -435,13 +442,12 @@
     halo = lax.ppermute(glu_tail, SP, [(i, (i + 1) % 16) for i in range(16)])
     taps = from_everyone(jnp.pad(conv_taps, ((0, 1), (0, 0))), SP)
 
-    turned, turned_away = turn(ring, upstream)
+    glu, act, conv, mean, inv = forward(ring, value, gate, halo, taps, gain)
+    act_other = shift(act, CORE, 1)
+    turned, turned_away = turn(tie(ring, act), upstream)
     turned_other = shift(turned_away, CORE, 1)
-
-    glu, act, conv, mean, inv = forward(ring, value, gate, halo, taps, tie(gain, turned))
-    act_other = shift(act, CORE, 1)
-    early = outer(EARLY, ring, turned, turned_other, act, act_other)
-    rest = outer(REST, ring, turned, turned_other, act, act_other)
+    early = outer("outer_early", EARLY, ring, turned, turned_other, act, act_other)
+    rest = outer("outer_rest", REST, ring, turned, turned_other, act, act_other)
     early, rest = (early[:2], early[2:]), (rest[:3], rest[3:])
 
     opened = [ring_open(axis, *part) for axis, part in zip((X, Y), early)]

time: 186 us -> 171 us (0.919)
  Pallas kernels: 57.6 us -> 43.5 us
  waiting for transfers between devices: 43.9 us -> 49.2 us
  other arithmetic: 9.32 us -> 6.4 us
  starting transfers between devices: 53.8 us -> 51.6 us
    pallas_call x8, Pallas kernels: 57.6 us -> 43.5 us  [the longest x1 10.9 us: forward(): call(forward_kernel, 'forward', (16 // GROUP,), [column(tokens), column(t...]
    ppermute x1, waiting for transfers between devices: 1.31 us -> 7.54 us  [step(): halo = lax.ppermute(glu_tail, SP, [(i, (i + 1) % 16) for i in range(16)])]
    ppermute x25, starting transfers between devices: 28.2 us -> 26.3 us  [shift(): lax.ppermute(value, axis, [(i, (i + amount) % count) for i in range(count)])]
    convert_element_type x4, other arithmetic: 2.1 us -> 0.19 us  [ring_sums(): add(previous_high, back[:count]).astype(BF16)]
  transfers between devices with their start and end apart: 31 -> 31, of which waited for: 13 -> 15; matrix products, arithmetic and copies ran while one was open for 6% -> 5% of each run, Pallas kernels for 30% -> 25%
where the time goes in v2:
time: 171 us
  starting transfers between devices  51.6 us (30%)
  waiting for transfers between devices  49.2 us (29%)
  Pallas kernels  43.5 us (25%)
  between operations  14.4 us (8%)
  other arithmetic  6.4 us (4%)
  local copies, waits for them, and re-layouts  5.52 us (3%)
    ppermute x25, waiting for transfers between devices, shift(): lax.ppermute(value, axis, [(i, (i + amount) % count) for i in range(count)])  29.6 us
    ppermute x25, starting transfers between devices, shift(): lax.ppermute(value, axis, [(i, (i + amount) % count) for i in range(count)])  26.3 us
    pallas_call x1, Pallas kernels, forward(): call(forward_kernel, 'forward', (16 // GROUP,), [column(tokens), column(t...  10.9 us
    pallas_call x1, Pallas kernels, norm_backward(): call(norm_kernel, 'norm_backward', (8,), [whole(tokens, width), column(wi...  9.84 us
    pallas_call x1, Pallas kernels, input_backward(): call(input_kernel, 'input_backward', (16 // GROUP,), [column(tokens), col...  9.05 us
    all_to_all x1, starting transfers between devices, step(): merged = lax.all_to_all(merged, Z, 0, 0, tiled=True)  8.65 us
    all_to_all x1, waiting for transfers between devices, step(): mine = lax.all_to_all(terms, SP, 0, 0, tiled=True)  7.55 us
    ppermute x1, waiting for transfers between devices, step(): halo = lax.ppermute(glu_tail, SP, [(i, (i + 1) % 16) for i in range(16)])  7.54 us
  transfers between devices with their start and end apart: 31, of which 15 were waited for; matrix products, arithmetic and copies ran while one was open for 5% of the time, Pallas kernels for 25%

profile of v2, /device:TPU:32, one launch (start us, length us, event | category | flops | bytes accessed | tf_op | source)
XLA Modules:
  0.0 170.6 jit_solution(9140315342199834597)
XLA Ops:
  7.2 0.7 all-gather.2.cloned.1.call-update
  7.9 0.7 pad.4
  8.6 0.7 broadcast_in_dim.10
  9.4 7.0 %all-to-all-start = ((f32[16,32,128]{2,1,0:T(8,128)}), f32[16,32,128]{2,1,0:T(8,128)S(1)}, u32[]{:S(2)}, u32[]{:S(2)}) async-start(f32[16,32,128]{2,1,0:T(8,128)} %broadcast_in_dim.10), calls=%async_computation | async-start | bytes 524288 | tf_op jit(solution)/shard_map/all_to_all | solution.py:417
  16.4 1.1 fusion.20
  17.5 2.0 %collective-permute-start = (bf16[32,2048]{1,0:T(8,128)(2,1)S(1)}, bf16[32,2048]{1,0:T(8,128)(2,1)S(1)}, u32[]{:S(2)}, u32[]{:S(2)}) collective-permute-start(bf16[32,2048]{1,0:T(8,128)(2,1)S(1)} %fusion.20), channel_id=1, source_target_pairs={{0,16},{16,32},{32,48},{48,64},{64,80},{80,96},{96,112},{112,128},... | collective-permute-start | bytes 393224 | tf_op jit(solution)/shard_map/ppermute | solution.py:442
  20.1 7.5 %collective-permute-done.halo = bf16[32,2048]{1,0:T(8,128)(2,1)S(1)} collective-permute-done((bf16[32,2048]{1,0:T(8,128)(2,1)S(1)}, bf16[32,2048]{1,0:T(8,128)(2,1)S(1)}, u32[]{:S(2)}, u32[]{:S(2)}) %collective-permute-start) | collective-permute-done | bytes 131104 | tf_op jit(solution)/shard_map/ppermute | solution.py:442
  28.4 10.9 %shard_map.101 = (bf16[256,2048]{1,0:T(8,128)(2,1)}, bf16[256,2048]{1,0:T(8,128)(2,1)}, bf16[256,2048]{1,0:T(8,128)(2,1)}, f32[256,128]{1,0:T(8,128)}, f32[256,128]{1,0:T(8,128)}) custom-call(s32[4]{0:T(128)} %pad_add_fusion.ring, bf16[256,2048]{1,0:T(8,128)(2,1)} %bitcast.104, bf16[256,2048]{1,0:T(8,128)(2,1)} %bitcast.106, bf16[32,2048]{1,0:T(8,128)(2,1)} %copy-done.8, ...), custom_call_target="tpu_custom_call" | custom-call | flops 3250585600 | bytes 5242880 | tf_op jit(solution)/shard_map/pallas_call | solution.py:101
  39.4 1.7 shard_map.102
  41.7 1.7 %collective-permute-done.1.turned_other = bf16[8,128,256]{2,1,0:T(8,128)(2,1)S(1)} collective-permute-done((bf16[8,128,256]{2,1,0:T(8,128)(2,1)S(1)}, bf16[8,128,256]{2,1,0:T(8,128)(2,1)S(1)}, u32[]{:S(2)}, u32[]{:S(2)}) %collective-permute-start.1) | collective-permute-done | bytes 524320 | tf_op jit(solution)/shard_map/ppermute | solution.py:43
  43.4 1.2 copy-done.7
  44.6 1.9 %shard_map.104 = (bf16[4,512,128]{2,1,0:T(8,128)(2,1)S(1)}, bf16[4,512,128]{2,1,0:T(8,128)(2,1)S(1)}, bf16[4,512,128]{2,1,0:T(8,128)(2,1)S(1)}, bf16[4,512,128]{2,1,0:T(8,128)(2,1)S(1)}) custom-call(s32[4]{0:T(128)S(1)} %copy-done.4, bf16[8,128,256]{2,1,0:T(8,128)(2,1)S(1)} %get-tuple-element.34.turned, ...), custom_call_target="tpu_custom_call" | custom-call | flops 1073741824 | bytes 4194304 | tf_op jit(solution)/shard_map/pallas_call | solution.py:185
  46.6 2.0 %collective-permute-start.3 = (bf16[4,512,128]{2,1,0:T(8,128)(2,1)S(1)}, bf16[4,512,128]{2,1,0:T(8,128)(2,1)S(1)}, u32[]{:S(2)}, u32[]{:S(2)}) collective-permute-start(bf16[4,512,128]{2,1,0:T(8,128)(2,1)S(1)} %get-tuple-element.37), channel_id=1, source_target_pairs={{0,16},{16,32},{32,48},{48,0},{1,17},{17,33},{33,49},{49,1},{2,18}... | collective-permute-start | bytes 1572872 | tf_op jit(solution)/shard_map/ppermute | solution.py:43
  48.7 1.0 collective-permute-start.6
  49.7 1.0 collective-permute-start.5
  50.7 1.9 %shard_map.103 = (bf16[2,512,128]{2,1,0:T(8,128)(2,1)S(1)}, bf16[2,512,128]{2,1,0:T(8,128)(2,1)S(1)}, bf16[4,512,128]{2,1,0:T(8,128)(2,1)S(1)}, bf16[2,512,128]{...) custom-call(s32[4]{0:T(128)S(1)} %copy-done.4, ...), custom_call_target="tpu_custom_call" | custom-call | flops 1073741824 | bytes 4194304 | tf_op jit(solution)/shard_map/pallas_call | solution.py:185
  52.6 8.2 %collective-permute-done.4 = bf16[4,512,128]{2,1,0:T(8,128)(2,1)S(1)} collective-permute-done((bf16[4,512,128]{2,1,0:T(8,128)(2,1)S(1)}, bf16[4,512,128]{2,1,0:T(8,128)(2,1)S(1)}, u32[]{:S(2)}, u32[]{:S(2)}) %collective-permute-start.4) | collective-permute-done | bytes 524320 | tf_op jit(solution)/shard_map/ppermute | solution.py:43
  60.8 1.6 collective-permute-start.9
  63.2 1.7 collective-permute-start.15
  65.6 3.0 %collective-permute-done.9 = bf16[2,512,128]{2,1,0:T(8,128)(2,1)S(1)} collective-permute-done((bf16[2,512,128]{2,1,0:T(8,128)(2,1)S(1)}, bf16[2,512,128]{2,1,0:T(8,128)(2,1)S(1)}, u32[]{:S(2)}, u32[]{:S(2)}) %collective-permute-start.9) | collective-permute-done | bytes 262176 | tf_op jit(solution)/shard_map/ppermute | solution.py:43
  68.6 2.8 %collective-permute-done.8 = bf16[2,512,128]{2,1,0:T(8,128)(2,1)S(1)} collective-permute-done((bf16[2,512,128]{2,1,0:T(8,128)(2,1)S(1)}, bf16[2,512,128]{2,1,0:T(8,128)(2,1)S(1)}, u32[]{:S(2)}, u32[]{:S(2)}) %collective-permute-start.8) | collective-permute-done | bytes 262176 | tf_op jit(solution)/shard_map/ppermute | solution.py:43
  71.6 1.0 collective-permute-start.12
  72.6 1.2 collective-permute-start.10
  74.1 2.1 %collective-permute-start.18 = (bf16[512,128]{1,0:T(8,128)(2,1)S(1)}, bf16[512,128]{1,0:T(8,128)(2,1)S(1)}, u32[]{:S(2)}, u32[]{:S(2)}) collective-permute-start(bf16[512,128]{1,0:T(8,128)(2,1)S(1)} %pad_maximum_fusion.5), channel_id=1, source_target_pairs={{0,48},{16,0},{32,16},{48,32},{1,49},{17,1},{33,17},{49,33},{2,50}... | collective-permute-start | bytes 393224 | tf_op jit(solution)/shard_map/ppermute | solution.py:43
  76.7 2.2 %collective-permute-start.13 = (bf16[256,128]{1,0:T(8,128)(2,1)S(1)}, bf16[256,128]{1,0:T(8,128)(2,1)S(1)}, u32[]{:S(2)}, u32[]{:S(2)}) collective-permute-start(bf16[256,128]{1,0:T(8,128)(2,1)S(1)} %fusion.11), channel_id=1, source_target_pairs={{0,192},{64,0},{128,64},{192,128},{1,193},{65,1},{129,65},{193,129... | collective-permute-start | bytes 196616 | tf_op jit(solution)/shard_map/ppermute | solution.py:43
  79.3 3.2 %collective-permute-start.19 = (bf16[256,128]{1,0:T(8,128)(2,1)S(1)}, bf16[256,128]{1,0:T(8,128)(2,1)S(1)}, u32[]{:S(2)}, u32[]{:S(2)}) collective-permute-start(bf16[256,128]{1,0:T(8,128)(2,1)S(1)} %fusion.1), channel_id=1, source_target_pairs={{0,48},{16,0},{32,16},{48,32},{1,49},{17,1},{33,17},{49,33},{2,50}... | collective-permute-start | bytes 196616 | tf_op jit(solution)/shard_map/ppermute | solution.py:43
  83.2 1.2 collective-permute-done.19
  85.1 9.8 %shard_map.105 = (bf16[256,2048]{1,0:T(8,128)(2,1)S(1)}, bf16[32,2048]{1,0:T(8,128)(2,1)S(1)}, f32[16,128]{1,0:T(8,128)S(1)}) custom-call(s32[4]{0:T(128)S(1)} %copy-done.4, bf16[256,2048]{1,0:T(8,128)(2,1)} %bitcast.95, bf16[2048,2048]{1,0:T(8,128)(2,1)} %all-gather.2.cloned.1.call-done.weight, bf16[256,2048]{1,0:T(8,128)(2,1)} %get-tuple-element.29.conv, ...), custom_call_target="tpu_custom_call" | custom-call | flops 2147483648 | bytes 11534336 | tf_op jit(solution)/shard_map/pallas_call | solution.py:315
  95.0 6.7 %shard_map.107 = f32[16,48,128]{2,1,0:T(8,128)} custom-call(s32[4]{0:T(128)S(1)} %copy-done.4, bf16[256,2048]{1,0:T(8,128)(2,1)S(1)} %copy-done.10, bf16[32,2048]{1,0:T(8,128)(2,1)S(1)} %copy-done.9, bf16[256,2048]{1,0:T(8,128)(2,1)S(1)} %get-tuple-element.45.grad, f32[16,128]{1,0:T(8,128)S(1)} %get-tuple-element.52.gain_part), custom_call_target="tpu_custom_call" | custom-call | flops 3250585600 | bytes 2097152 | tf_op jit(solution)/shard_map/pallas_call | solution.py:362
  101.7 6.4 %all-to-all-start.1 = ((f32[16,48,128]{2,1,0:T(8,128)}), f32[16,48,128]{2,1,0:T(8,128)S(1)}, u32[]{:S(2)}, u32[]{:S(2)}) async-start(f32[16,48,128]{2,1,0:T(8,128)} %shard_map.107), calls=%async_computation.1 | async-start | bytes 786432 | tf_op jit(solution)/shard_map/all_to_all | solution.py:467
  108.1 0.9 fusion.19
  109.0 0.9 fusion.9
  109.9 7.6 %all-to-all-done.1 = f32[16,48,128]{2,1,0:T(8,128)S(1)} async-done(((f32[16,48,128]{2,1,0:T(8,128)}), f32[16,48,128]{2,1,0:T(8,128)S(1)}, u32[]{:S(2)}, u32[]{:S(2)}) %all-to-all-start.1) | async-done | bytes 393248 | tf_op jit(solution)/shard_map/all_to_all | solution.py:467
  117.6 1.2 collective-permute-done.20
  118.8 0.8 pad_maximum_fusion
  119.6 8.7 %all-to-all-start.2 = ((bf16[8,176,128]{2,1,0:T(8,128)(2,1)}), bf16[8,176,128]{2,1,0:T(8,128)(2,1)S(1)}, u32[]{:S(2)}, u32[]{:S(2)}) async-start(bf16[8,176,128]{2,1,0:T(8,128)(2,1)} %pad_maximum_fusion), calls=%async_computation.2 | async-start | bytes 720896 | tf_op jit(solution)/shard_map/all_to_all | solution.py:473
  128.2 1.2 collective-permute-start.7
  129.4 3.8 %collective-permute-done.7.tail = bf16[32,2048]{1,0:T(8,128)(2,1)S(1)} collective-permute-done((bf16[32,2048]{1,0:T(8,128)(2,1)S(1)}, bf16[32,2048]{1,0:T(8,128)(2,1)S(1)}, u32[]{:S(2)}, u32[]{:S(2)}) %collective-permute-start.7) | collective-permute-done | bytes 131104 | tf_op jit(solution)/shard_map/ppermute | solution.py:460
  133.9 9.1 %shard_map.106 = (bf16[256,2048]{1,0:T(8,128)(2,1)}, bf16[256,2048]{1,0:T(8,128)(2,1)}) custom-call(s32[4]{0:T(128)} %pad_add_fusion.ring, bf16[256,2048]{1,0:T(8,128)(2,1)} %copy-done.6, bf16[32,2048]{1,0:T(8,128)(2,1)} %copy-done.13, f32[16,32,128]{2,1,0:T(8,128)} %copy-done.12, bf16[256,2048]{1,0:T(8,128)(2,1)} %bitcast.105, bf16[256,2048]{1,0:T(8,128)(2,1)} %bitcast.107), custom_call_target="tpu_custom_call" | custom-call | flops 3250585600 | bytes 5242880 | tf_op jit(solution)/shard_map/pallas_call | solution.py:396
  143.0 2.7 %collective-permute-start.21 = (bf16[128,128]{1,0:T(8,128)(2,1)S(1)}, bf16[128,128]{1,0:T(8,128)(2,1)S(1)}, u32[]{:S(2)}, u32[]{:S(2)}) collective-permute-start(bf16[128,128]{1,0:T(8,128)(2,1)S(1)} %get-tuple-element.54), channel_id=1, source_target_pairs={{0,48},{16,0},{32,16},{48,32},{1,49},{17,1},{33,17},{49,33},{2,50}... | collective-permute-start | bytes 98312 | tf_op jit(solution)/shard_map/ppermute | solution.py:43
  145.7 1.0 collective-permute-start.23
  147.3 3.9 %collective-permute-done.22 = bf16[128,128]{1,0:T(8,128)(2,1)S(1)} collective-permute-done((bf16[128,128]{1,0:T(8,128)(2,1)S(1)}, bf16[128,128]{1,0:T(8,128)(2,1)S(1)}, u32[]{:S(2)}, u32[]{:S(2)}) %collective-permute-start.22) | collective-permute-done | bytes 32800 | tf_op jit(solution)/shard_map/ppermute | solution.py:43
  151.2 2.5 %collective-permute-start.24 = (bf16[4,128,128]{2,1,0:T(8,128)(2,1)S(1)}, bf16[4,128,128]{2,1,0:T(8,128)(2,1)S(1)}, u32[]{:S(2)}, u32[]{:S(2)}) collective-permute-start(bf16[4,128,128]{2,1,0:T(8,128)(2,1)S(1)} %pad_maximum_fusion.6), channel_id=1, source_target_pairs={{0,192},{64,0},{128,64},{192,128},{1,193},{65,1},{129,65},{193,129... | collective-permute-start | bytes 393224 | tf_op jit(solution)/shard_map/ppermute | solution.py:43
  154.0 0.7 collective-permute-start.26
  154.7 2.9 %collective-permute-done.24 = bf16[4,128,128]{2,1,0:T(8,128)(2,1)S(1)} collective-permute-done((bf16[4,128,128]{2,1,0:T(8,128)(2,1)S(1)}, bf16[4,128,128]{2,1,0:T(8,128)(2,1)S(1)}, u32[]{:S(2)}, u32[]{:S(2)}) %collective-permute-start.24) | collective-permute-done | bytes 131104 | tf_op jit(solution)/shard_map/ppermute | solution.py:43
  157.7 2.6 %collective-permute-done.25 = bf16[4,128,128]{2,1,0:T(8,128)(2,1)S(1)} collective-permute-done((bf16[4,128,128]{2,1,0:T(8,128)(2,1)S(1)}, bf16[4,128,128]{2,1,0:T(8,128)(2,1)S(1)}, u32[]{:S(2)}, u32[]{:S(2)}) %collective-permute-start.25) | collective-permute-done | bytes 131104 | tf_op jit(solution)/shard_map/ppermute | solution.py:43
  160.3 1.2 collective-permute-done.26
  162.2 1.6 shard_map.108
  (91 shorter events, 8.9 us)
Async XLA Ops:
  7.2 32.3 %copy-start = (bf16[1,256,2048]{2,1,0:T(8,128)(2,1)S(1)}, bf16[1,256,2048]{2,1,0:T(8,128)(2,1)}, u32[]{:S(2)}) copy-start(bf16[1,256,2048]{2,1,0:T(8,128)(2,1)} %param.8) | copy-start | bytes 3145732
  7.2 77.9 %all-gather.2.cloned.1.call-start = ((), (), s32[]{:S(2)}) async-start(), calls=%async_computation.3 | async-start | bytes 8912896 | tf_op jit(solution)/shard_map/all_gather | solution.py:439
  9.4 18.2 %all-to-all-start = ((f32[16,32,128]{2,1,0:T(8,128)}), f32[16,32,128]{2,1,0:T(8,128)S(1)}, u32[]{:S(2)}, u32[]{:S(2)}) async-start(f32[16,32,128]{2,1,0:T(8,128)} %broadcast_in_dim.10), calls=%async_computation | async-start | bytes 524288 | tf_op jit(solution)/shard_map/all_to_all | solution.py:417
  17.5 10.1 %collective-permute-start = (bf16[32,2048]{1,0:T(8,128)(2,1)S(1)}, bf16[32,2048]{1,0:T(8,128)(2,1)S(1)}, u32[]{:S(2)}, u32[]{:S(2)}) collective-permute-start(bf16[32,2048]{1,0:T(8,128)(2,1)S(1)} %fusion.20), channel_id=1, source_target_pairs={{0,16},{16,32},{32,48},{48,64},{64,80},{80,96},{96,112},{112,128},... | collective-permute-start | bytes 393224 | tf_op jit(solution)/shard_map/ppermute | solution.py:442
  20.1 19.4 %copy-start.4 = (s32[4]{0:T(128)S(1)}, s32[4]{0:T(128)}, u32[]{:S(2)}) copy-start(s32[4]{0:T(128)} %pad_add_fusion.ring) | copy-start | bytes 52
  27.6 0.7 copy-start.8
  27.6 0.8 copy-start.12
  39.3 4.1 %collective-permute-start.2 = (bf16[256,2048]{1,0:T(8,128)(2,1)}, bf16[256,2048]{1,0:T(8,128)(2,1)S(1)}, u32[]{:S(2)}, u32[]{:S(2)}) collective-permute-start(bf16[256,2048]{1,0:T(8,128)(2,1)} %get-tuple-element.32.act), channel_id=1, source_target_pairs={{0,1},{1,0},{2,3},{3,2},{4,5},{5,4},{6,7},{7,6},{8,9},{9,8},{10,11... | collective-permute-start | bytes 3145736 | tf_op jit(solution)/shard_map/ppermute | solution.py:43
  41.1 2.3 %collective-permute-start.1 = (bf16[8,128,256]{2,1,0:T(8,128)(2,1)S(1)}, bf16[8,128,256]{2,1,0:T(8,128)(2,1)S(1)}, u32[]{:S(2)}, u32[]{:S(2)}) collective-permute-start(bf16[8,128,256]{2,1,0:T(8,128)(2,1)S(1)} %get-tuple-element.35), channel_id=1, source_target_pairs={{0,1},{1,0},{2,3},{3,2},{4,5},{5,4},{6,7},{7,6},{8,9},{9,8},{10,11... | collective-permute-start | bytes 1572872 | tf_op jit(solution)/shard_map/ppermute | solution.py:43
  43.4 1.2 copy-start.7
  46.5 38.6 %copy-start.1 = (f32[256,128]{1,0:T(8,128)S(1)}, f32[256,128]{1,0:T(8,128)}, u32[]{:S(2)}) copy-start(f32[256,128]{1,0:T(8,128)} %get-tuple-element.30.mean) | copy-start | bytes 393220
  46.5 38.6 %copy-start.2 = (f32[256,128]{1,0:T(8,128)S(1)}, f32[256,128]{1,0:T(8,128)}, u32[]{:S(2)}) copy-start(f32[256,128]{1,0:T(8,128)} %get-tuple-element.31.inv) | copy-start | bytes 393220
  46.5 38.5 %copy-start.3 = (f32[2048]{0:T(1024)S(1)}, f32[2048]{0:T(1024)}, u32[]{:S(2)}) copy-start(f32[2048]{0:T(1024)} %param.10) | copy-start | bytes 24580
  46.6 14.2 %collective-permute-start.4 = (bf16[4,512,128]{2,1,0:T(8,128)(2,1)S(1)}, bf16[4,512,128]{2,1,0:T(8,128)(2,1)S(1)}, u32[]{:S(2)}, u32[]{:S(2)}) collective-permute-start(bf16[4,512,128]{2,1,0:T(8,128)(2,1)S(1)} %get-tuple-element.39), channel_id=1, source_target_pairs={{0,48},{16,0},{32,16},{48,32},{1,49},{17,1},{33,17},{49,33},{2,50}... | collective-permute-start | bytes 1572872 | tf_op jit(solution)/shard_map/ppermute | solution.py:43
  46.6 15.7 %collective-permute-start.3 = (bf16[4,512,128]{2,1,0:T(8,128)(2,1)S(1)}, bf16[4,512,128]{2,1,0:T(8,128)(2,1)S(1)}, u32[]{:S(2)}, u32[]{:S(2)}) collective-permute-start(bf16[4,512,128]{2,1,0:T(8,128)(2,1)S(1)} %get-tuple-element.37), channel_id=1, source_target_pairs={{0,16},{16,32},{32,48},{48,0},{1,17},{17,33},{33,49},{49,1},{2,18}... | collective-permute-start | bytes 1572872 | tf_op jit(solution)/shard_map/ppermute | solution.py:43
  48.7 14.4 %collective-permute-start.6 = (bf16[4,512,128]{2,1,0:T(8,128)(2,1)S(1)}, bf16[4,512,128]{2,1,0:T(8,128)(2,1)S(1)}, u32[]{:S(2)}, u32[]{:S(2)}) collective-permute-start(bf16[4,512,128]{2,1,0:T(8,128)(2,1)S(1)} %get-tuple-element.43), channel_id=1, source_target_pairs={{0,192},{64,0},{128,64},{192,128},{1,193},{65,1},{129,65},{193,129... | collective-permute-start | bytes 1572872 | tf_op jit(solution)/shard_map/ppermute | solution.py:43
  49.7 15.2 %collective-permute-start.5 = (bf16[4,512,128]{2,1,0:T(8,128)(2,1)S(1)}, bf16[4,512,128]{2,1,0:T(8,128)(2,1)S(1)}, u32[]{:S(2)}, u32[]{:S(2)}) collective-permute-start(bf16[4,512,128]{2,1,0:T(8,128)(2,1)S(1)} %get-tuple-element.41), channel_id=1, source_target_pairs={{0,64},{64,128},{128,192},{192,0},{1,65},{65,129},{129,193},{193,1... | collective-permute-start | bytes 1572872 | tf_op jit(solution)/shard_map/ppermute | solution.py:43
  60.8 7.8 %collective-permute-start.9 = (bf16[2,512,128]{2,1,0:T(8,128)(2,1)S(1)}, bf16[2,512,128]{2,1,0:T(8,128)(2,1)S(1)}, u32[]{:S(2)}, u32[]{:S(2)}) collective-permute-start(bf16[2,512,128]{2,1,0:T(8,128)(2,1)S(1)} %add_convert_fusion.2), channel_id=1, source_target_pairs={{0,48},{16,0},{32,16},{48,32},{1,49},{17,1},{33,17},{49,33},{2,50}... | collective-permute-start | bytes 786440 | tf_op jit(solution)/shard_map/ppermute | solution.py:43
  62.5 8.9 %collective-permute-start.8 = (bf16[2,512,128]{2,1,0:T(8,128)(2,1)S(1)}, bf16[2,512,128]{2,1,0:T(8,128)(2,1)S(1)}, u32[]{:S(2)}, u32[]{:S(2)}) collective-permute-start(bf16[2,512,128]{2,1,0:T(8,128)(2,1)S(1)} %add_convert_fusion.3), channel_id=1, source_target_pairs={{0,16},{16,32},{32,48},{48,0},{1,17},{17,33},{33,49},{49,1},{2,18}... | collective-permute-start | bytes 786440 | tf_op jit(solution)/shard_map/ppermute | solution.py:43
  63.2 10.7 %collective-permute-start.15 = (bf16[2,512,128]{2,1,0:T(8,128)(2,1)S(1)}, bf16[2,512,128]{2,1,0:T(8,128)(2,1)S(1)}, u32[]{:S(2)}, u32[]{:S(2)}) collective-permute-start(bf16[2,512,128]{2,1,0:T(8,128)(2,1)S(1)} %add_convert_fusion), channel_id=1, source_target_pairs={{0,192},{64,0},{128,64},{192,128},{1,193},{65,1},{129,65},{193,129... | collective-permute-start | bytes 786440 | tf_op jit(solution)/shard_map/ppermute | solution.py:43
  64.9 8.9 %collective-permute-start.14 = (bf16[2,512,128]{2,1,0:T(8,128)(2,1)S(1)}, bf16[2,512,128]{2,1,0:T(8,128)(2,1)S(1)}, u32[]{:S(2)}, u32[]{:S(2)}) collective-permute-start(bf16[2,512,128]{2,1,0:T(8,128)(2,1)S(1)} %add_convert_fusion.1), channel_id=1, source_target_pairs={{0,64},{64,128},{128,192},{192,0},{1,65},{65,129},{129,193},{193,1... | collective-permute-start | bytes 786440 | tf_op jit(solution)/shard_map/ppermute | solution.py:43
  71.6 5.0 %collective-permute-start.12 = (bf16[512,128]{1,0:T(8,128)(2,1)S(1)}, bf16[512,128]{1,0:T(8,128)(2,1)S(1)}, u32[]{:S(2)}, u32[]{:S(2)}) collective-permute-start(bf16[512,128]{1,0:T(8,128)(2,1)S(1)} %pad_maximum_fusion.3), channel_id=1, source_target_pairs={{0,192},{64,0},{128,64},{192,128},{1,193},{65,1},{129,65},{193,129... | collective-permute-start | bytes 393224 | tf_op jit(solution)/shard_map/ppermute | solution.py:43
  72.6 22.3 %copy-start.9 = (bf16[32,2048]{1,0:T(8,128)(2,1)S(1)}, bf16[32,2048]{1,0:T(8,128)(2,1)}, u32[]{:S(2)}) copy-start(bf16[32,2048]{1,0:T(8,128)(2,1)} %copy-done.8) | copy-start | bytes 393220
  72.6 22.4 %copy-start.10 = (bf16[256,2048]{1,0:T(8,128)(2,1)S(1)}, bf16[256,2048]{1,0:T(8,128)(2,1)}, u32[]{:S(2)}) copy-start(bf16[256,2048]{1,0:T(8,128)(2,1)} %get-tuple-element.51.glu) | copy-start | bytes 3145732
  72.6 9.9 %collective-permute-start.10 = (bf16[512,128]{1,0:T(8,128)(2,1)S(1)}, bf16[512,128]{1,0:T(8,128)(2,1)S(1)}, u32[]{:S(2)}, u32[]{:S(2)}) collective-permute-start(bf16[512,128]{1,0:T(8,128)(2,1)S(1)} %pad_maximum_fusion.2), channel_id=1, source_target_pairs={{0,64},{64,128},{128,192},{192,0},{1,65},{65,129},{129,193},{193,1... | collective-permute-start | bytes 393224 | tf_op jit(solution)/shard_map/ppermute | solution.py:43
  74.0 10.4 %copy-start.11 = (f32[2,512,128]{2,1,0:T(8,128)}, f32[2,512,128]{2,1,0:T(8,128)S(1)}, u32[]{:S(2)}) copy-start(f32[2,512,128]{2,1,0:T(8,128)S(1)} %get-tuple-element.64) | copy-start | bytes 1572868
  74.1 5.2 %collective-permute-start.18 = (bf16[512,128]{1,0:T(8,128)(2,1)S(1)}, bf16[512,128]{1,0:T(8,128)(2,1)S(1)}, u32[]{:S(2)}, u32[]{:S(2)}) collective-permute-start(bf16[512,128]{1,0:T(8,128)(2,1)S(1)} %pad_maximum_fusion.5), channel_id=1, source_target_pairs={{0,48},{16,0},{32,16},{48,32},{1,49},{17,1},{33,17},{49,33},{2,50}... | collective-permute-start | bytes 393224 | tf_op jit(solution)/shard_map/ppermute | solution.py:43
  76.3 6.9 %collective-permute-start.16 = (bf16[512,128]{1,0:T(8,128)(2,1)S(1)}, bf16[512,128]{1,0:T(8,128)(2,1)S(1)}, u32[]{:S(2)}, u32[]{:S(2)}) collective-permute-start(bf16[512,128]{1,0:T(8,128)(2,1)S(1)} %pad_maximum_fusion.4), channel_id=1, source_target_pairs={{0,16},{16,32},{32,48},{48,0},{1,17},{17,33},{33,49},{49,1},{2,18}... | collective-permute-start | bytes 393224 | tf_op jit(solution)/shard_map/ppermute | solution.py:43
  76.7 5.8 %collective-permute-start.13 = (bf16[256,128]{1,0:T(8,128)(2,1)S(1)}, bf16[256,128]{1,0:T(8,128)(2,1)S(1)}, u32[]{:S(2)}, u32[]{:S(2)}) collective-permute-start(bf16[256,128]{1,0:T(8,128)(2,1)S(1)} %fusion.11), channel_id=1, source_target_pairs={{0,192},{64,0},{128,64},{192,128},{1,193},{65,1},{129,65},{193,129... | collective-permute-start | bytes 196616 | tf_op jit(solution)/shard_map/ppermute | solution.py:43
  79.3 5.1 %collective-permute-start.19 = (bf16[256,128]{1,0:T(8,128)(2,1)S(1)}, bf16[256,128]{1,0:T(8,128)(2,1)S(1)}, u32[]{:S(2)}, u32[]{:S(2)}) collective-permute-start(bf16[256,128]{1,0:T(8,128)(2,1)S(1)} %fusion.1), channel_id=1, source_target_pairs={{0,48},{16,0},{32,16},{48,32},{1,49},{17,1},{33,17},{49,33},{2,50}... | collective-permute-start | bytes 196616 | tf_op jit(solution)/shard_map/ppermute | solution.py:43
  83.2 24.9 %collective-permute-start.11 = (bf16[256,128]{1,0:T(8,128)(2,1)}, bf16[256,128]{1,0:T(8,128)(2,1)}, u32[]{:S(2)}, u32[]{:S(2)}) collective-permute-start(bf16[256,128]{1,0:T(8,128)(2,1)} %get-tuple-element.59), channel_id=1, source_target_pairs={{0,64},{64,128},{128,192},{192,0},{1,65},{65,129},{129,193},{193,1... | collective-permute-start | bytes 196616 | tf_op jit(solution)/shard_map/ppermute | solution.py:43
  85.1 23.9 %collective-permute-start.17 = (bf16[256,128]{1,0:T(8,128)(2,1)}, bf16[256,128]{1,0:T(8,128)(2,1)}, u32[]{:S(2)}, u32[]{:S(2)}) collective-permute-start(bf16[256,128]{1,0:T(8,128)(2,1)} %get-tuple-element.61), channel_id=1, source_target_pairs={{0,16},{16,32},{32,48},{48,0},{1,17},{17,33},{33,49},{49,1},{2,18}... | collective-permute-start | bytes 196616 | tf_op jit(solution)/shard_map/ppermute | solution.py:43
  94.9 38.3 %copy-start.6 = (bf16[256,2048]{1,0:T(8,128)(2,1)}, bf16[256,2048]{1,0:T(8,128)(2,1)S(1)}, u32[]{:S(2)}) copy-start(bf16[256,2048]{1,0:T(8,128)(2,1)S(1)} %get-tuple-element.45.grad) | copy-start | bytes 3145732
  101.7 15.8 %all-to-all-start.1 = ((f32[16,48,128]{2,1,0:T(8,128)}), f32[16,48,128]{2,1,0:T(8,128)S(1)}, u32[]{:S(2)}, u32[]{:S(2)}) async-start(f32[16,48,128]{2,1,0:T(8,128)} %shard_map.107), calls=%async_computation.1 | async-start | bytes 786432 | tf_op jit(solution)/shard_map/all_to_all | solution.py:467
  108.9 53.2 %copy-start.5 = (s32[4]{0:T(128)S(1)}, s32[4]{0:T(128)}, u32[]{:S(2)}) copy-start(s32[4]{0:T(128)} %pad_add_fusion.ring) | copy-start | bytes 52
  117.5 1.3 collective-permute-start.20
  119.6 23.4 %all-to-all-start.2 = ((bf16[8,176,128]{2,1,0:T(8,128)(2,1)}), bf16[8,176,128]{2,1,0:T(8,128)(2,1)S(1)}, u32[]{:S(2)}, u32[]{:S(2)}) async-start(bf16[8,176,128]{2,1,0:T(8,128)(2,1)} %pad_maximum_fusion), calls=%async_computation.2 | async-start | bytes 720896 | tf_op jit(solution)/shard_map/all_to_all | solution.py:473
  128.2 5.0 %collective-permute-start.7 = (bf16[32,2048]{1,0:T(8,128)(2,1)S(1)}, bf16[32,2048]{1,0:T(8,128)(2,1)S(1)}, u32[]{:S(2)}, u32[]{:S(2)}) collective-permute-start(bf16[32,2048]{1,0:T(8,128)(2,1)S(1)} %get-tuple-element.46), channel_id=1, source_target_pairs={{16,0},{32,16},{48,32},{64,48},{80,64},{96,80},{112,96},{128,112},... | collective-permute-start | bytes 393224 | tf_op jit(solution)/shard_map/ppermute | solution.py:460
  133.2 0.6 copy-start.13
  143.0 4.3 %collective-permute-start.21 = (bf16[128,128]{1,0:T(8,128)(2,1)S(1)}, bf16[128,128]{1,0:T(8,128)(2,1)S(1)}, u32[]{:S(2)}, u32[]{:S(2)}) collective-permute-start(bf16[128,128]{1,0:T(8,128)(2,1)S(1)} %get-tuple-element.54), channel_id=1, source_target_pairs={{0,48},{16,0},{32,16},{48,32},{1,49},{17,1},{33,17},{49,33},{2,50}... | collective-permute-start | bytes 98312 | tf_op jit(solution)/shard_map/ppermute | solution.py:43
  145.7 5.5 %collective-permute-start.22 = (bf16[128,128]{1,0:T(8,128)(2,1)S(1)}, bf16[128,128]{1,0:T(8,128)(2,1)S(1)}, u32[]{:S(2)}, u32[]{:S(2)}) collective-permute-start(bf16[128,128]{1,0:T(8,128)(2,1)S(1)} %get-tuple-element.54), channel_id=1, source_target_pairs={{0,32},{16,48},{32,0},{48,16},{1,33},{17,49},{33,1},{49,17},{2,34}... | collective-permute-start | bytes 98312 | tf_op jit(solution)/shard_map/ppermute | solution.py:43
  145.7 5.5 %collective-permute-start.23 = (bf16[128,128]{1,0:T(8,128)(2,1)S(1)}, bf16[128,128]{1,0:T(8,128)(2,1)S(1)}, u32[]{:S(2)}, u32[]{:S(2)}) collective-permute-start(bf16[128,128]{1,0:T(8,128)(2,1)S(1)} %get-tuple-element.54), channel_id=1, source_target_pairs={{0,16},{16,32},{32,48},{48,0},{1,17},{17,33},{33,49},{49,1},{2,18}... | collective-permute-start | bytes 98312 | tf_op jit(solution)/shard_map/ppermute | solution.py:43
  151.2 6.4 %collective-permute-start.24 = (bf16[4,128,128]{2,1,0:T(8,128)(2,1)S(1)}, bf16[4,128,128]{2,1,0:T(8,128)(2,1)S(1)}, u32[]{:S(2)}, u32[]{:S(2)}) collective-permute-start(bf16[4,128,128]{2,1,0:T(8,128)(2,1)S(1)} %pad_maximum_fusion.6), channel_id=1, source_target_pairs={{0,192},{64,0},{128,64},{192,128},{1,193},{65,1},{129,65},{193,129... | collective-permute-start | bytes 393224 | tf_op jit(solution)/shard_map/ppermute | solution.py:43
  153.7 6.6 %collective-permute-start.25 = (bf16[4,128,128]{2,1,0:T(8,128)(2,1)S(1)}, bf16[4,128,128]{2,1,0:T(8,128)(2,1)S(1)}, u32[]{:S(2)}, u32[]{:S(2)}) collective-permute-start(bf16[4,128,128]{2,1,0:T(8,128)(2,1)S(1)} %pad_maximum_fusion.6), channel_id=1, source_target_pairs={{0,128},{64,192},{128,0},{192,64},{1,129},{65,193},{129,1},{193,65... | collective-permute-start | bytes 393224 | tf_op jit(solution)/shard_map/ppermute | solution.py:43
  154.0 7.6 %collective-permute-start.26 = (bf16[4,128,128]{2,1,0:T(8,128)(2,1)S(1)}, bf16[4,128,128]{2,1,0:T(8,128)(2,1)S(1)}, u32[]{:S(2)}, u32[]{:S(2)}) collective-permute-start(bf16[4,128,128]{2,1,0:T(8,128)(2,1)S(1)} %pad_maximum_fusion.6), channel_id=1, source_target_pairs={{0,64},{64,128},{128,192},{192,0},{1,65},{65,129},{129,193},{193,1... | collective-permute-start | bytes 393224 | tf_op jit(solution)/shard_map/ppermute | solution.py:43
Sparse Core Ops, SparseCore 0:
  9.8 56.6 all-gather.1

commit v3 on v2

--- a/solution.py
+++ b/solution.py
@@ -221,14 +221,6 @@
     return add(own_low, late_on, back[count:]), add(own_high, on[count:], late_back)
 
 
-def cut(low, high):
-    rows = low.shape[1] // 2
-    block = lambda k, h: (low, high)[k // 2][k % 2, h * rows : (h + 1) * rows]
-    on = jnp.concatenate([block(2, 0), block(1, 1)]).astype(BF16)
-    back = jnp.concatenate([block(2, 1), block(3, 0)]).astype(BF16)
-    return (on, back), (block(1, 0), block(3, 1)), (block(0, 0), block(0, 1))
-
-
 def place_kernel(ring, blocks, out):
     count, _, lanes = blocks.shape
     for i in range(count):
@@ -459,16 +451,16 @@
     grad, grad_head, gain_part = norm_backward(ring, upstream, weight, conv, mean, inv, tie(gain, sums))
     next_head = lax.ppermute(grad_head, SP, [((i + 1) % 16, i) for i in range(16)])
 
-    pieces = [cut(*half) for half in halves]
-    opened = [ring_open(axis, *piece[0]) for axis, piece in zip((Y, X), pieces)]
-    sums = [ring_sums(pair, *piece[1]) for pair, piece in zip(opened, pieces)]
-    closed = [ring_close(axis, pair, late, *piece[2]) for axis, pair, late, piece in zip((Y, X), opened, sums, pieces)]
+    closed = []
+    for axis, (low, high) in zip((Y, X), halves):
+        sent = ((1, low[1]), (2, high[0]), (3, high[1]))
+        closed.append(add(low[0], *[shift(block.astype(BF16), axis, k) for k, block in sent]))
     terms = taps_backward(ring, glu, halo, grad, gain_part)
     mine = lax.all_to_all(terms, SP, 0, 0, tiled=True)
     mine = jnp.sum(mine, axis=0)
     mine = mine + shift(mine, CORE, 1)
 
-    scattered = jnp.concatenate([rows for half in closed for rows in half]).reshape(8, lanes, lanes)
+    scattered = jnp.concatenate(closed).reshape(8, lanes, lanes)
     merged = jnp.concatenate([scattered, jnp.broadcast_to(mine[None], (8, *mine.shape))], axis=1).astype(BF16)
     merged = lax.all_to_all(merged, Z, 0, 0, tiled=True)
     merged = jnp.sum(merged.astype(F32), axis=0)

time: 171 us -> 166 us (0.971)
  waiting for transfers between devices: 49.2 us -> 43.2 us
    all_to_all x1, waiting for transfers between devices: 7.55 us -> 0.01 us  [step(): mine = lax.all_to_all(terms, SP, 0, 0, tiled=True)]
    ppermute x25 -> x23, waiting for transfers between devices: 29.6 us -> 32.5 us  [shift(): lax.ppermute(value, axis, [(i, (i + amount) % count) for i in range(count)])]
    ppermute x1, starting transfers between devices: 1.17 us -> 2.97 us  [step(): lax.ppermute(grad_head, SP, [((i + 1) % 16, i) for i in range(16)])]
    ppermute x25 -> x23, starting transfers between devices: 26.3 us -> 25.1 us  [shift(): lax.ppermute(value, axis, [(i, (i + amount) % count) for i in range(count)])]
  transfers between devices with their start and end apart: 31 -> 29, of which waited for: 15 -> 12; matrix products, arithmetic and copies ran while one was open for 5% -> 5% of each run, Pallas kernels for 25% -> 25%
where the time goes in v3:
time: 166 us; the launch traced here: 165 us
  starting transfers between devices  51.4 us (31%)
  Pallas kernels  43.5 us (26%)
  waiting for transfers between devices  43.2 us (26%)
  between operations  14.3 us (9%)
  local copies, waits for them, and re-layouts  7.01 us (4%)
  other arithmetic  5.37 us (3%)
    ppermute x23, waiting for transfers between devices, shift(): lax.ppermute(value, axis, [(i, (i + amount) % count) for i in range(count)])  32.5 us
    ppermute x23, starting transfers between devices, shift(): lax.ppermute(value, axis, [(i, (i + amount) % count) for i in range(count)])  25.1 us
    pallas_call x1, Pallas kernels, forward(): call(forward_kernel, 'forward', (16 // GROUP,), [column(tokens), column(t...  10.9 us
    pallas_call x1, Pallas kernels, norm_backward(): call(norm_kernel, 'norm_backward', (8,), [whole(tokens, width), column(wi...  9.84 us
    pallas_call x1, Pallas kernels, input_backward(): call(input_kernel, 'input_backward', (16 // GROUP,), [column(tokens), col...  9.05 us
    all_to_all x1, starting transfers between devices, step(): merged = lax.all_to_all(merged, Z, 0, 0, tiled=True)  8.78 us
    ppermute x1, waiting for transfers between devices, step(): halo = lax.ppermute(glu_tail, SP, [(i, (i + 1) % 16) for i in range(16)])  7.53 us
    all_to_all x1, starting transfers between devices, from_everyone(): lax.all_to_all(jnp.broadcast_to(shard[None], (count, *shard.shape)), axis...  7.03 us
  transfers between devices with their start and end apart: 29, of which 12 were waited for; matrix products, arithmetic and copies ran while one was open for 5% of the time, Pallas kernels for 25%

profile of v3, /device:TPU:32, one launch (start us, length us, event | category | flops | bytes accessed | tf_op | source)
XLA Modules:
  0.0 164.9 jit_solution(9678926403799959712)
XLA Ops:
  7.9 0.7 pad.4
  8.6 0.7 broadcast_in_dim.10
  9.4 7.0 %all-to-all-start = ((f32[16,32,128]{2,1,0:T(8,128)}), f32[16,32,128]{2,1,0:T(8,128)S(1)}, u32[]{:S(2)}, u32[]{:S(2)}) async-start(f32[16,32,128]{2,1,0:T(8,128)} %broadcast_in_dim.10), calls=%async_computation | async-start | bytes 524288 | tf_op jit(solution)/shard_map/all_to_all | solution.py:409
  16.4 1.1 fusion.10
  17.5 2.0 %collective-permute-start = (bf16[32,2048]{1,0:T(8,128)(2,1)S(1)}, bf16[32,2048]{1,0:T(8,128)(2,1)S(1)}, u32[]{:S(2)}, u32[]{:S(2)}) collective-permute-start(bf16[32,2048]{1,0:T(8,128)(2,1)S(1)} %fusion.10), channel_id=1, source_target_pairs={{0,16},{16,32},{32,48},{48,64},{64,80},{80,96},{96,112},{112,128},... | collective-permute-start | bytes 393224 | tf_op jit(solution)/shard_map/ppermute | solution.py:434
  20.1 7.5 %collective-permute-done.halo = bf16[32,2048]{1,0:T(8,128)(2,1)S(1)} collective-permute-done((bf16[32,2048]{1,0:T(8,128)(2,1)S(1)}, bf16[32,2048]{1,0:T(8,128)(2,1)S(1)}, u32[]{:S(2)}, u32[]{:S(2)}) %collective-permute-start) | collective-permute-done | bytes 131104 | tf_op jit(solution)/shard_map/ppermute | solution.py:434
  28.4 10.9 %shard_map.101 = (bf16[256,2048]{1,0:T(8,128)(2,1)}, bf16[256,2048]{1,0:T(8,128)(2,1)}, bf16[256,2048]{1,0:T(8,128)(2,1)}, f32[256,128]{1,0:T(8,128)}, f32[256,128]{1,0:T(8,128)}) custom-call(s32[4]{0:T(128)} %pad_add_fusion.ring, bf16[256,2048]{1,0:T(8,128)(2,1)} %bitcast.64, bf16[256,2048]{1,0:T(8,128)(2,1)} %bitcast.66, bf16[32,2048]{1,0:T(8,128)(2,1)} %copy-done.8, ...), custom_call_target="tpu_custom_call" | custom-call | flops 3250585600 | bytes 5242880 | tf_op jit(solution)/shard_map/pallas_call | solution.py:101
  39.4 1.7 %shard_map.102 = (bf16[8,128,256]{2,1,0:T(8,128)(2,1)S(1)}, bf16[8,128,256]{2,1,0:T(8,128)(2,1)S(1)}) custom-call(s32[4]{0:T(128)S(1)} %copy-done.4, bf16[256,2048]{1,0:T(8,128)(2,1)S(1)} %bitcast.56), custom_call_target="tpu_custom_call" | custom-call | flops 52428800 | bytes 2097152 | tf_op jit(solution)/shard_map/pallas_call | solution.py:144
  41.7 1.7 %collective-permute-done.1.turned_other = bf16[8,128,256]{2,1,0:T(8,128)(2,1)S(1)} collective-permute-done((bf16[8,128,256]{2,1,0:T(8,128)(2,1)S(1)}, bf16[8,128,256]{2,1,0:T(8,128)(2,1)S(1)}, u32[]{:S(2)}, u32[]{:S(2)}) %collective-permute-start.1) | collective-permute-done | bytes 524320 | tf_op jit(solution)/shard_map/ppermute | solution.py:43
  43.4 1.2 copy-done.7
  44.7 1.9 %shard_map.104 = (bf16[4,512,128]{2,1,0:T(8,128)(2,1)S(1)}, bf16[4,512,128]{2,1,0:T(8,128)(2,1)S(1)}, bf16[4,512,128]{2,1,0:T(8,128)(2,1)S(1)}, bf16[4,512,128]{2,1,0:T(8,128)(2,1)S(1)}) custom-call(s32[4]{0:T(128)S(1)} %copy-done.4, bf16[8,128,256]{2,1,0:T(8,128)(2,1)S(1)} %get-tuple-element.34.turned, ...), custom_call_target="tpu_custom_call" | custom-call | flops 1073741824 | bytes 4194304 | tf_op jit(solution)/shard_map/pallas_call | solution.py:185
  46.6 2.0 %collective-permute-start.3 = (bf16[4,512,128]{2,1,0:T(8,128)(2,1)S(1)}, bf16[4,512,128]{2,1,0:T(8,128)(2,1)S(1)}, u32[]{:S(2)}, u32[]{:S(2)}) collective-permute-start(bf16[4,512,128]{2,1,0:T(8,128)(2,1)S(1)} %get-tuple-element.37), channel_id=1, source_target_pairs={{0,16},{16,32},{32,48},{48,0},{1,17},{17,33},{33,49},{49,1},{2,18}... | collective-permute-start | bytes 1572872 | tf_op jit(solution)/shard_map/ppermute | solution.py:43
  48.6 1.0 collective-permute-start.6
  49.7 1.0 collective-permute-start.5
  50.7 1.9 %shard_map.103 = (bf16[2,512,128]{2,1,0:T(8,128)(2,1)S(1)}, bf16[2,512,128]{2,1,0:T(8,128)(2,1)S(1)}, bf16[4,512,128]{2,1,0:T(8,128)(2,1)S(1)}, bf16[2,512,128]{...) custom-call(s32[4]{0:T(128)S(1)} %copy-done.4, ...), custom_call_target="tpu_custom_call" | custom-call | flops 1073741824 | bytes 4194304 | tf_op jit(solution)/shard_map/pallas_call | solution.py:185
  52.5 8.2 %collective-permute-done.4 = bf16[4,512,128]{2,1,0:T(8,128)(2,1)S(1)} collective-permute-done((bf16[4,512,128]{2,1,0:T(8,128)(2,1)S(1)}, bf16[4,512,128]{2,1,0:T(8,128)(2,1)S(1)}, u32[]{:S(2)}, u32[]{:S(2)}) %collective-permute-start.4) | collective-permute-done | bytes 524320 | tf_op jit(solution)/shard_map/ppermute | solution.py:43
  60.8 1.6 collective-permute-start.10
  63.1 1.7 %collective-permute-start.15 = (bf16[2,512,128]{2,1,0:T(8,128)(2,1)S(1)}, bf16[2,512,128]{2,1,0:T(8,128)(2,1)S(1)}, u32[]{:S(2)}, u32[]{:S(2)}) collective-permute-start(bf16[2,512,128]{2,1,0:T(8,128)(2,1)S(1)} %add_convert_fusion.2), channel_id=1, source_target_pairs={{0,192},{64,0},{128,64},{192,128},{1,193},{65,1},{129,65},{193,129... | collective-permute-start | bytes 786440 | tf_op jit(solution)/shard_map/ppermute | solution.py:43
  65.6 3.0 %collective-permute-done.10 = bf16[2,512,128]{2,1,0:T(8,128)(2,1)S(1)} collective-permute-done((bf16[2,512,128]{2,1,0:T(8,128)(2,1)S(1)}, bf16[2,512,128]{2,1,0:T(8,128)(2,1)S(1)}, u32[]{:S(2)}, u32[]{:S(2)}) %collective-permute-start.10) | collective-permute-done | bytes 262176 | tf_op jit(solution)/shard_map/ppermute | solution.py:43
  68.6 2.8 %collective-permute-done.8 = bf16[2,512,128]{2,1,0:T(8,128)(2,1)S(1)} collective-permute-done((bf16[2,512,128]{2,1,0:T(8,128)(2,1)S(1)}, bf16[2,512,128]{2,1,0:T(8,128)(2,1)S(1)}, u32[]{:S(2)}, u32[]{:S(2)}) %collective-permute-start.8) | collective-permute-done | bytes 262176 | tf_op jit(solution)/shard_map/ppermute | solution.py:43
  71.6 0.7 slice_bitcast_fusion.5
  72.3 1.0 collective-permute-start.11
  73.3 1.2 collective-permute-start.12
  74.5 0.9 collective-permute-start.9
  75.7 0.8 slice_bitcast_fusion.3
  76.4 1.9 %collective-permute-start.17 = (bf16[512,128]{1,0:T(8,128)(2,1)}, bf16[512,128]{1,0:T(8,128)(2,1)}, u32[]{:S(2)}, u32[]{:S(2)}) collective-permute-start(bf16[512,128]{1,0:T(8,128)(2,1)} %get-tuple-element.62), channel_id=1, source_target_pairs={{0,48},{16,0},{32,16},{48,32},{1,49},{17,1},{33,17},{49,33},{2,50}... | collective-permute-start | bytes 393224 | tf_op jit(solution)/shard_map/ppermute | solution.py:43
  78.4 9.8 %shard_map.105 = (bf16[256,2048]{1,0:T(8,128)(2,1)S(1)}, bf16[32,2048]{1,0:T(8,128)(2,1)S(1)}, f32[16,128]{1,0:T(8,128)S(1)}) custom-call(s32[4]{0:T(128)S(1)} %copy-done.4, bf16[256,2048]{1,0:T(8,128)(2,1)} %bitcast.55, bf16[2048,2048]{1,0:T(8,128)(2,1)} %all-gather.2.cloned.1.call-done.weight, bf16[256,2048]{1,0:T(8,128)(2,1)} %get-tuple-element.29.conv, ...), custom_call_target="tpu_custom_call" | custom-call | flops 2147483648 | bytes 11534336 | tf_op jit(solution)/shard_map/pallas_call | solution.py:307
  88.3 6.7 %shard_map.107 = f32[16,48,128]{2,1,0:T(8,128)} custom-call(s32[4]{0:T(128)S(1)} %copy-done.4, bf16[256,2048]{1,0:T(8,128)(2,1)S(1)} %copy-done.10, bf16[32,2048]{1,0:T(8,128)(2,1)S(1)} %copy-done.9, bf16[256,2048]{1,0:T(8,128)(2,1)S(1)} %get-tuple-element.45.grad, f32[16,128]{1,0:T(8,128)S(1)} %get-tuple-element.52.gain_part), custom_call_target="tpu_custom_call" | custom-call | flops 3250585600 | bytes 2097152 | tf_op jit(solution)/shard_map/pallas_call | solution.py:354
  95.0 5.5 %all-to-all-start.1 = ((f32[16,48,128]{2,1,0:T(8,128)}), f32[16,48,128]{2,1,0:T(8,128)S(1)}, u32[]{:S(2)}, u32[]{:S(2)}) async-start(f32[16,48,128]{2,1,0:T(8,128)} %shard_map.107), calls=%async_computation.1 | async-start | bytes 786432 | tf_op jit(solution)/shard_map/all_to_all | solution.py:459
  100.5 2.0 %collective-permute-start.14 = (bf16[512,128]{1,0:T(8,128)(2,1)S(1)}, bf16[512,128]{1,0:T(8,128)(2,1)S(1)}, u32[]{:S(2)}, u32[]{:S(2)}) collective-permute-start(bf16[512,128]{1,0:T(8,128)(2,1)S(1)} %fusion.9), channel_id=1, source_target_pairs={{0,16},{16,32},{32,48},{48,0},{1,17},{17,33},{33,49},{49,1},{2,18}... | collective-permute-start | bytes 393224 | tf_op jit(solution)/shard_map/ppermute | solution.py:43
  102.5 1.0 fusion.7
  103.6 5.3 %collective-permute-done.14 = bf16[512,128]{1,0:T(8,128)(2,1)S(1)} collective-permute-done((bf16[512,128]{1,0:T(8,128)(2,1)S(1)}, bf16[512,128]{1,0:T(8,128)(2,1)S(1)}, u32[]{:S(2)}, u32[]{:S(2)}) %collective-permute-start.14) | collective-permute-done | bytes 131104 | tf_op jit(solution)/shard_map/ppermute | solution.py:43
  108.9 1.1 fusion.3
  110.2 1.2 collective-permute-done.18
  111.4 0.8 pad_maximum_fusion
  112.1 8.8 %all-to-all-start.2 = ((bf16[8,176,128]{2,1,0:T(8,128)(2,1)}), bf16[8,176,128]{2,1,0:T(8,128)(2,1)S(1)}, u32[]{:S(2)}, u32[]{:S(2)}) async-start(bf16[8,176,128]{2,1,0:T(8,128)(2,1)} %pad_maximum_fusion), calls=%async_computation.2 | async-start | bytes 720896 | tf_op jit(solution)/shard_map/all_to_all | solution.py:465
  120.9 3.0 %collective-permute-start.7 = (bf16[32,2048]{1,0:T(8,128)(2,1)S(1)}, bf16[32,2048]{1,0:T(8,128)(2,1)S(1)}, u32[]{:S(2)}, u32[]{:S(2)}) collective-permute-start(bf16[32,2048]{1,0:T(8,128)(2,1)S(1)} %get-tuple-element.46), channel_id=1, source_target_pairs={{16,0},{32,16},{48,32},{64,48},{80,64},{96,80},{112,96},{128,112},... | collective-permute-start | bytes 393224 | tf_op jit(solution)/shard_map/ppermute | solution.py:452
  123.9 2.5 %collective-permute-done.7.tail = bf16[32,2048]{1,0:T(8,128)(2,1)S(1)} collective-permute-done((bf16[32,2048]{1,0:T(8,128)(2,1)S(1)}, bf16[32,2048]{1,0:T(8,128)(2,1)S(1)}, u32[]{:S(2)}, u32[]{:S(2)}) %collective-permute-start.7) | collective-permute-done | bytes 131104 | tf_op jit(solution)/shard_map/ppermute | solution.py:452
  127.0 9.1 %shard_map.106 = (bf16[256,2048]{1,0:T(8,128)(2,1)}, bf16[256,2048]{1,0:T(8,128)(2,1)}) custom-call(s32[4]{0:T(128)} %pad_add_fusion.ring, bf16[256,2048]{1,0:T(8,128)(2,1)} %copy-done.6, bf16[32,2048]{1,0:T(8,128)(2,1)} %copy-done.13, f32[16,32,128]{2,1,0:T(8,128)} %copy-done.12, bf16[256,2048]{1,0:T(8,128)(2,1)} %bitcast.65, bf16[256,2048]{1,0:T(8,128)(2,1)} %bitcast.67), custom_call_target="tpu_custom_call" | custom-call | flops 3250585600 | bytes 5242880 | tf_op jit(solution)/shard_map/pallas_call | solution.py:388
  136.2 2.6 %collective-permute-start.19 = (bf16[128,128]{1,0:T(8,128)(2,1)S(1)}, bf16[128,128]{1,0:T(8,128)(2,1)S(1)}, u32[]{:S(2)}, u32[]{:S(2)}) collective-permute-start(bf16[128,128]{1,0:T(8,128)(2,1)S(1)} %get-tuple-element.54), channel_id=1, source_target_pairs={{0,48},{16,0},{32,16},{48,32},{1,49},{17,1},{33,17},{49,33},{2,50}... | collective-permute-start | bytes 98312 | tf_op jit(solution)/shard_map/ppermute | solution.py:43
  138.7 1.2 collective-permute-start.21
  140.5 3.7 %collective-permute-done.20 = bf16[128,128]{1,0:T(8,128)(2,1)S(1)} collective-permute-done((bf16[128,128]{1,0:T(8,128)(2,1)S(1)}, bf16[128,128]{1,0:T(8,128)(2,1)S(1)}, u32[]{:S(2)}, u32[]{:S(2)}) %collective-permute-start.20) | collective-permute-done | bytes 32800 | tf_op jit(solution)/shard_map/ppermute | solution.py:43
  144.2 4.0 %collective-permute-start.22 = (bf16[4,128,128]{2,1,0:T(8,128)(2,1)S(1)}, bf16[4,128,128]{2,1,0:T(8,128)(2,1)S(1)}, u32[]{:S(2)}, u32[]{:S(2)}) collective-permute-start(bf16[4,128,128]{2,1,0:T(8,128)(2,1)S(1)} %pad_maximum_fusion.2), channel_id=1, source_target_pairs={{0,192},{64,0},{128,64},{192,128},{1,193},{65,1},{129,65},{193,129... | collective-permute-start | bytes 393224 | tf_op jit(solution)/shard_map/ppermute | solution.py:43
  148.2 1.0 collective-permute-start.24
  149.2 2.9 %collective-permute-done.22 = bf16[4,128,128]{2,1,0:T(8,128)(2,1)S(1)} collective-permute-done((bf16[4,128,128]{2,1,0:T(8,128)(2,1)S(1)}, bf16[4,128,128]{2,1,0:T(8,128)(2,1)S(1)}, u32[]{:S(2)}, u32[]{:S(2)}) %collective-permute-start.22) | collective-permute-done | bytes 131104 | tf_op jit(solution)/shard_map/ppermute | solution.py:43
  152.2 2.6 %collective-permute-done.23 = bf16[4,128,128]{2,1,0:T(8,128)(2,1)S(1)} collective-permute-done((bf16[4,128,128]{2,1,0:T(8,128)(2,1)S(1)}, bf16[4,128,128]{2,1,0:T(8,128)(2,1)S(1)}, u32[]{:S(2)}, u32[]{:S(2)}) %collective-permute-start.23) | collective-permute-done | bytes 131104 | tf_op jit(solution)/shard_map/ppermute | solution.py:43
  154.8 1.0 collective-permute-done.24
  156.4 1.6 shard_map.108
  (79 shorter events, 7.1 us)
Async XLA Ops:
  7.2 32.3 %copy-start = (bf16[1,256,2048]{2,1,0:T(8,128)(2,1)S(1)}, bf16[1,256,2048]{2,1,0:T(8,128)(2,1)}, u32[]{:S(2)}) copy-start(bf16[1,256,2048]{2,1,0:T(8,128)(2,1)} %param.8) | copy-start | bytes 3145732
  7.2 71.2 %all-gather.2.cloned.1.call-start = ((), (), s32[]{:S(2)}) async-start(), calls=%async_computation.3 | async-start | bytes 8912896 | tf_op jit(solution)/shard_map/all_gather | solution.py:431
  9.4 18.2 %all-to-all-start = ((f32[16,32,128]{2,1,0:T(8,128)}), f32[16,32,128]{2,1,0:T(8,128)S(1)}, u32[]{:S(2)}, u32[]{:S(2)}) async-start(f32[16,32,128]{2,1,0:T(8,128)} %broadcast_in_dim.10), calls=%async_computation | async-start | bytes 524288 | tf_op jit(solution)/shard_map/all_to_all | solution.py:409
  17.5 10.1 %collective-permute-start = (bf16[32,2048]{1,0:T(8,128)(2,1)S(1)}, bf16[32,2048]{1,0:T(8,128)(2,1)S(1)}, u32[]{:S(2)}, u32[]{:S(2)}) collective-permute-start(bf16[32,2048]{1,0:T(8,128)(2,1)S(1)} %fusion.10), channel_id=1, source_target_pairs={{0,16},{16,32},{32,48},{48,64},{64,80},{80,96},{96,112},{112,128},... | collective-permute-start | bytes 393224 | tf_op jit(solution)/shard_map/ppermute | solution.py:434
  20.1 19.4 %copy-start.4 = (s32[4]{0:T(128)S(1)}, s32[4]{0:T(128)}, u32[]{:S(2)}) copy-start(s32[4]{0:T(128)} %pad_add_fusion.ring) | copy-start | bytes 52
  27.6 0.7 copy-start.8
  27.6 0.8 copy-start.12
  39.3 4.1 %collective-permute-start.2 = (bf16[256,2048]{1,0:T(8,128)(2,1)}, bf16[256,2048]{1,0:T(8,128)(2,1)S(1)}, u32[]{:S(2)}, u32[]{:S(2)}) collective-permute-start(bf16[256,2048]{1,0:T(8,128)(2,1)} %get-tuple-element.32.act), channel_id=1, source_target_pairs={{0,1},{1,0},{2,3},{3,2},{4,5},{5,4},{6,7},{7,6},{8,9},{9,8},{10,11... | collective-permute-start | bytes 3145736 | tf_op jit(solution)/shard_map/ppermute | solution.py:43
  41.1 2.3 %collective-permute-start.1 = (bf16[8,128,256]{2,1,0:T(8,128)(2,1)S(1)}, bf16[8,128,256]{2,1,0:T(8,128)(2,1)S(1)}, u32[]{:S(2)}, u32[]{:S(2)}) collective-permute-start(bf16[8,128,256]{2,1,0:T(8,128)(2,1)S(1)} %get-tuple-element.35), channel_id=1, source_target_pairs={{0,1},{1,0},{2,3},{3,2},{4,5},{5,4},{6,7},{7,6},{8,9},{9,8},{10,11... | collective-permute-start | bytes 1572872 | tf_op jit(solution)/shard_map/ppermute | solution.py:43
  43.4 1.2 copy-start.7
  44.6 33.8 %copy-start.1 = (f32[256,128]{1,0:T(8,128)S(1)}, f32[256,128]{1,0:T(8,128)}, u32[]{:S(2)}) copy-start(f32[256,128]{1,0:T(8,128)} %get-tuple-element.30.mean) | copy-start | bytes 393220
  44.7 33.8 %copy-start.2 = (f32[256,128]{1,0:T(8,128)S(1)}, f32[256,128]{1,0:T(8,128)}, u32[]{:S(2)}) copy-start(f32[256,128]{1,0:T(8,128)} %get-tuple-element.31.inv) | copy-start | bytes 393220
  44.7 33.8 %copy-start.3 = (f32[2048]{0:T(1024)S(1)}, f32[2048]{0:T(1024)}, u32[]{:S(2)}) copy-start(f32[2048]{0:T(1024)} %param.10) | copy-start | bytes 24580
  46.5 14.2 %collective-permute-start.4 = (bf16[4,512,128]{2,1,0:T(8,128)(2,1)S(1)}, bf16[4,512,128]{2,1,0:T(8,128)(2,1)S(1)}, u32[]{:S(2)}, u32[]{:S(2)}) collective-permute-start(bf16[4,512,128]{2,1,0:T(8,128)(2,1)S(1)} %get-tuple-element.39), channel_id=1, source_target_pairs={{0,48},{16,0},{32,16},{48,32},{1,49},{17,1},{33,17},{49,33},{2,50}... | collective-permute-start | bytes 1572872 | tf_op jit(solution)/shard_map/ppermute | solution.py:43
  46.6 15.7 %collective-permute-start.3 = (bf16[4,512,128]{2,1,0:T(8,128)(2,1)S(1)}, bf16[4,512,128]{2,1,0:T(8,128)(2,1)S(1)}, u32[]{:S(2)}, u32[]{:S(2)}) collective-permute-start(bf16[4,512,128]{2,1,0:T(8,128)(2,1)S(1)} %get-tuple-element.37), channel_id=1, source_target_pairs={{0,16},{16,32},{32,48},{48,0},{1,17},{17,33},{33,49},{49,1},{2,18}... | collective-permute-start | bytes 1572872 | tf_op jit(solution)/shard_map/ppermute | solution.py:43
  48.6 14.4 %collective-permute-start.6 = (bf16[4,512,128]{2,1,0:T(8,128)(2,1)S(1)}, bf16[4,512,128]{2,1,0:T(8,128)(2,1)S(1)}, u32[]{:S(2)}, u32[]{:S(2)}) collective-permute-start(bf16[4,512,128]{2,1,0:T(8,128)(2,1)S(1)} %get-tuple-element.43), channel_id=1, source_target_pairs={{0,192},{64,0},{128,64},{192,128},{1,193},{65,1},{129,65},{193,129... | collective-permute-start | bytes 1572872 | tf_op jit(solution)/shard_map/ppermute | solution.py:43
  49.7 15.2 %collective-permute-start.5 = (bf16[4,512,128]{2,1,0:T(8,128)(2,1)S(1)}, bf16[4,512,128]{2,1,0:T(8,128)(2,1)S(1)}, u32[]{:S(2)}, u32[]{:S(2)}) collective-permute-start(bf16[4,512,128]{2,1,0:T(8,128)(2,1)S(1)} %get-tuple-element.41), channel_id=1, source_target_pairs={{0,64},{64,128},{128,192},{192,0},{1,65},{65,129},{129,193},{193,1... | collective-permute-start | bytes 1572872 | tf_op jit(solution)/shard_map/ppermute | solution.py:43
  60.8 7.8 %collective-permute-start.10 = (bf16[2,512,128]{2,1,0:T(8,128)(2,1)S(1)}, bf16[2,512,128]{2,1,0:T(8,128)(2,1)S(1)}, u32[]{:S(2)}, u32[]{:S(2)}) collective-permute-start(bf16[2,512,128]{2,1,0:T(8,128)(2,1)S(1)} %add_convert_fusion.4), channel_id=1, source_target_pairs={{0,48},{16,0},{32,16},{48,32},{1,49},{17,1},{33,17},{49,33},{2,50}... | collective-permute-start | bytes 786440 | tf_op jit(solution)/shard_map/ppermute | solution.py:43
  62.4 8.9 %collective-permute-start.8 = (bf16[2,512,128]{2,1,0:T(8,128)(2,1)S(1)}, bf16[2,512,128]{2,1,0:T(8,128)(2,1)S(1)}, u32[]{:S(2)}, u32[]{:S(2)}) collective-permute-start(bf16[2,512,128]{2,1,0:T(8,128)(2,1)S(1)} %add_convert_fusion.5), channel_id=1, source_target_pairs={{0,16},{16,32},{32,48},{48,0},{1,17},{17,33},{33,49},{49,1},{2,18}... | collective-permute-start | bytes 786440 | tf_op jit(solution)/shard_map/ppermute | solution.py:43
  63.1 12.3 %collective-permute-start.15 = (bf16[2,512,128]{2,1,0:T(8,128)(2,1)S(1)}, bf16[2,512,128]{2,1,0:T(8,128)(2,1)S(1)}, u32[]{:S(2)}, u32[]{:S(2)}) collective-permute-start(bf16[2,512,128]{2,1,0:T(8,128)(2,1)S(1)} %add_convert_fusion.2), channel_id=1, source_target_pairs={{0,192},{64,0},{128,64},{192,128},{1,193},{65,1},{129,65},{193,129... | collective-permute-start | bytes 786440 | tf_op jit(solution)/shard_map/ppermute | solution.py:43
  64.9 10.6 %collective-permute-start.13 = (bf16[2,512,128]{2,1,0:T(8,128)(2,1)S(1)}, bf16[2,512,128]{2,1,0:T(8,128)(2,1)S(1)}, u32[]{:S(2)}, u32[]{:S(2)}) collective-permute-start(bf16[2,512,128]{2,1,0:T(8,128)(2,1)S(1)} %add_convert_fusion.3), channel_id=1, source_target_pairs={{0,64},{64,128},{128,192},{192,0},{1,65},{65,129},{129,193},{193,1... | collective-permute-start | bytes 786440 | tf_op jit(solution)/shard_map/ppermute | solution.py:43
  71.4 16.9 %copy-start.9 = (bf16[32,2048]{1,0:T(8,128)(2,1)S(1)}, bf16[32,2048]{1,0:T(8,128)(2,1)}, u32[]{:S(2)}) copy-start(bf16[32,2048]{1,0:T(8,128)(2,1)} %copy-done.8) | copy-start | bytes 393220
  71.4 16.9 %copy-start.10 = (bf16[256,2048]{1,0:T(8,128)(2,1)S(1)}, bf16[256,2048]{1,0:T(8,128)(2,1)}, u32[]{:S(2)}) copy-start(bf16[256,2048]{1,0:T(8,128)(2,1)} %get-tuple-element.51.glu) | copy-start | bytes 3145732
  72.3 28.2 %collective-permute-start.11 = (bf16[512,128]{1,0:T(8,128)(2,1)}, bf16[512,128]{1,0:T(8,128)(2,1)S(1)}, u32[]{:S(2)}, u32[]{:S(2)}) collective-permute-start(bf16[512,128]{1,0:T(8,128)(2,1)} %get-tuple-element.59), channel_id=1, source_target_pairs={{0,128},{64,192},{128,0},{192,64},{1,129},{65,193},{129,1},{193,65... | collective-permute-start | bytes 393224 | tf_op jit(solution)/shard_map/ppermute | solution.py:43
  73.3 29.1 %collective-permute-start.12 = (bf16[512,128]{1,0:T(8,128)(2,1)}, bf16[512,128]{1,0:T(8,128)(2,1)}, u32[]{:S(2)}, u32[]{:S(2)}) collective-permute-start(bf16[512,128]{1,0:T(8,128)(2,1)} %get-tuple-element.60), channel_id=1, source_target_pairs={{0,192},{64,0},{128,64},{192,128},{1,193},{65,1},{129,65},{193,129... | collective-permute-start | bytes 393224 | tf_op jit(solution)/shard_map/ppermute | solution.py:43
  74.5 28.0 %collective-permute-start.9 = (bf16[512,128]{1,0:T(8,128)(2,1)S(1)}, bf16[512,128]{1,0:T(8,128)(2,1)}, u32[]{:S(2)}, u32[]{:S(2)}) collective-permute-start(bf16[512,128]{1,0:T(8,128)(2,1)S(1)} %fusion.8), channel_id=1, source_target_pairs={{0,64},{64,128},{128,192},{192,0},{1,65},{65,129},{129,193},{193,1... | collective-permute-start | bytes 393224 | tf_op jit(solution)/shard_map/ppermute | solution.py:43
  75.7 2.7 %copy-start.11 = (f32[2,512,128]{2,1,0:T(8,128)}, f32[2,512,128]{2,1,0:T(8,128)S(1)}, u32[]{:S(2)}) copy-start(f32[2,512,128]{2,1,0:T(8,128)S(1)} %get-tuple-element.58) | copy-start | bytes 1572868
  76.4 27.1 %collective-permute-start.16 = (bf16[512,128]{1,0:T(8,128)(2,1)}, bf16[512,128]{1,0:T(8,128)(2,1)}, u32[]{:S(2)}, u32[]{:S(2)}) collective-permute-start(bf16[512,128]{1,0:T(8,128)(2,1)} %get-tuple-element.61), channel_id=1, source_target_pairs={{0,32},{16,48},{32,0},{48,16},{1,33},{17,49},{33,1},{49,17},{2,34}... | collective-permute-start | bytes 393224 | tf_op jit(solution)/shard_map/ppermute | solution.py:43
  76.4 27.1 %collective-permute-start.17 = (bf16[512,128]{1,0:T(8,128)(2,1)}, bf16[512,128]{1,0:T(8,128)(2,1)}, u32[]{:S(2)}, u32[]{:S(2)}) collective-permute-start(bf16[512,128]{1,0:T(8,128)(2,1)} %get-tuple-element.62), channel_id=1, source_target_pairs={{0,48},{16,0},{32,16},{48,32},{1,49},{17,1},{33,17},{49,33},{2,50}... | collective-permute-start | bytes 393224 | tf_op jit(solution)/shard_map/ppermute | solution.py:43
  88.3 23.8 %copy-start.6 = (bf16[256,2048]{1,0:T(8,128)(2,1)}, bf16[256,2048]{1,0:T(8,128)(2,1)S(1)}, u32[]{:S(2)}) copy-start(bf16[256,2048]{1,0:T(8,128)(2,1)S(1)} %get-tuple-element.45.grad) | copy-start | bytes 3145732
  95.0 15.0 %all-to-all-start.1 = ((f32[16,48,128]{2,1,0:T(8,128)}), f32[16,48,128]{2,1,0:T(8,128)S(1)}, u32[]{:S(2)}, u32[]{:S(2)}) async-start(f32[16,48,128]{2,1,0:T(8,128)} %shard_map.107), calls=%async_computation.1 | async-start | bytes 786432 | tf_op jit(solution)/shard_map/all_to_all | solution.py:459
  100.5 8.4 %collective-permute-start.14 = (bf16[512,128]{1,0:T(8,128)(2,1)S(1)}, bf16[512,128]{1,0:T(8,128)(2,1)S(1)}, u32[]{:S(2)}, u32[]{:S(2)}) collective-permute-start(bf16[512,128]{1,0:T(8,128)(2,1)S(1)} %fusion.9), channel_id=1, source_target_pairs={{0,16},{16,32},{32,48},{48,0},{1,17},{17,33},{33,49},{49,1},{2,18}... | collective-permute-start | bytes 393224 | tf_op jit(solution)/shard_map/ppermute | solution.py:43
  110.0 46.4 %copy-start.5 = (s32[4]{0:T(128)S(1)}, s32[4]{0:T(128)}, u32[]{:S(2)}) copy-start(s32[4]{0:T(128)} %pad_add_fusion.ring) | copy-start | bytes 52
  110.0 1.3 collective-permute-start.18
  112.1 24.0 %all-to-all-start.2 = ((bf16[8,176,128]{2,1,0:T(8,128)(2,1)}), bf16[8,176,128]{2,1,0:T(8,128)(2,1)S(1)}, u32[]{:S(2)}, u32[]{:S(2)}) async-start(bf16[8,176,128]{2,1,0:T(8,128)(2,1)} %pad_maximum_fusion), calls=%async_computation.2 | async-start | bytes 720896 | tf_op jit(solution)/shard_map/all_to_all | solution.py:465
  120.9 5.5 %collective-permute-start.7 = (bf16[32,2048]{1,0:T(8,128)(2,1)S(1)}, bf16[32,2048]{1,0:T(8,128)(2,1)S(1)}, u32[]{:S(2)}, u32[]{:S(2)}) collective-permute-start(bf16[32,2048]{1,0:T(8,128)(2,1)S(1)} %get-tuple-element.46), channel_id=1, source_target_pairs={{16,0},{32,16},{48,32},{64,48},{80,64},{96,80},{112,96},{128,112},... | collective-permute-start | bytes 393224 | tf_op jit(solution)/shard_map/ppermute | solution.py:452
  126.4 0.7 copy-start.13
  136.2 4.3 %collective-permute-start.19 = (bf16[128,128]{1,0:T(8,128)(2,1)S(1)}, bf16[128,128]{1,0:T(8,128)(2,1)S(1)}, u32[]{:S(2)}, u32[]{:S(2)}) collective-permute-start(bf16[128,128]{1,0:T(8,128)(2,1)S(1)} %get-tuple-element.54), channel_id=1, source_target_pairs={{0,48},{16,0},{32,16},{48,32},{1,49},{17,1},{33,17},{49,33},{2,50}... | collective-permute-start | bytes 98312 | tf_op jit(solution)/shard_map/ppermute | solution.py:43
  138.7 5.5 %collective-permute-start.20 = (bf16[128,128]{1,0:T(8,128)(2,1)S(1)}, bf16[128,128]{1,0:T(8,128)(2,1)S(1)}, u32[]{:S(2)}, u32[]{:S(2)}) collective-permute-start(bf16[128,128]{1,0:T(8,128)(2,1)S(1)} %get-tuple-element.54), channel_id=1, source_target_pairs={{0,32},{16,48},{32,0},{48,16},{1,33},{17,49},{33,1},{49,17},{2,34}... | collective-permute-start | bytes 98312 | tf_op jit(solution)/shard_map/ppermute | solution.py:43
  138.7 5.5 %collective-permute-start.21 = (bf16[128,128]{1,0:T(8,128)(2,1)S(1)}, bf16[128,128]{1,0:T(8,128)(2,1)S(1)}, u32[]{:S(2)}, u32[]{:S(2)}) collective-permute-start(bf16[128,128]{1,0:T(8,128)(2,1)S(1)} %get-tuple-element.54), channel_id=1, source_target_pairs={{0,16},{16,32},{32,48},{48,0},{1,17},{17,33},{33,49},{49,1},{2,18}... | collective-permute-start | bytes 98312 | tf_op jit(solution)/shard_map/ppermute | solution.py:43
  144.2 7.9 %collective-permute-start.22 = (bf16[4,128,128]{2,1,0:T(8,128)(2,1)S(1)}, bf16[4,128,128]{2,1,0:T(8,128)(2,1)S(1)}, u32[]{:S(2)}, u32[]{:S(2)}) collective-permute-start(bf16[4,128,128]{2,1,0:T(8,128)(2,1)S(1)} %pad_maximum_fusion.2), channel_id=1, source_target_pairs={{0,192},{64,0},{128,64},{192,128},{1,193},{65,1},{129,65},{193,129... | collective-permute-start | bytes 393224 | tf_op jit(solution)/shard_map/ppermute | solution.py:43
  148.2 6.6 %collective-permute-start.23 = (bf16[4,128,128]{2,1,0:T(8,128)(2,1)S(1)}, bf16[4,128,128]{2,1,0:T(8,128)(2,1)S(1)}, u32[]{:S(2)}, u32[]{:S(2)}) collective-permute-start(bf16[4,128,128]{2,1,0:T(8,128)(2,1)S(1)} %pad_maximum_fusion.2), channel_id=1, source_target_pairs={{0,128},{64,192},{128,0},{192,64},{1,129},{65,193},{129,1},{193,65... | collective-permute-start | bytes 393224 | tf_op jit(solution)/shard_map/ppermute | solution.py:43
  148.2 7.6 %collective-permute-start.24 = (bf16[4,128,128]{2,1,0:T(8,128)(2,1)S(1)}, bf16[4,128,128]{2,1,0:T(8,128)(2,1)S(1)}, u32[]{:S(2)}, u32[]{:S(2)}) collective-permute-start(bf16[4,128,128]{2,1,0:T(8,128)(2,1)S(1)} %pad_maximum_fusion.2), channel_id=1, source_target_pairs={{0,64},{64,128},{128,192},{192,0},{1,65},{65,129},{129,193},{193,1... | collective-permute-start | bytes 393224 | tf_op jit(solution)/shard_map/ppermute | solution.py:43
Sparse Core Ops, SparseCore 0:
  9.8 56.6 all-gather.1

commit v4 on v3

--- a/solution.py
+++ b/solution.py
@@ -244,12 +244,17 @@
     )(ring, blocks)
 
 
+def around(value, axis):
+    across = shift(value, axis, -2)
+    return [value, shift(value, axis, -1), across, shift(value, axis, -3)]
+
+
 def plane_row(shard):
-    return jnp.stack([shard] + [shift(shard, X, -k) for k in range(1, 4)])
+    return jnp.stack(around(shard, X))
 
 
 def plane_column(row):
-    return jnp.concatenate([row] + [shift(row, Y, -k) for k in range(1, 4)])
+    return jnp.concatenate(around(row, Y))
 
 
 def norm_kernel(
@@ -451,14 +456,16 @@
     grad, grad_head, gain_part = norm_backward(ring, upstream, weight, conv, mean, inv, tie(gain, sums))
     next_head = lax.ppermute(grad_head, SP, [((i + 1) % 16, i) for i in range(16)])
 
-    closed = []
-    for axis, (low, high) in zip((Y, X), halves):
-        sent = ((1, low[1]), (2, high[0]), (3, high[1]))
-        closed.append(add(low[0], *[shift(block.astype(BF16), axis, k) for k, block in sent]))
     terms = taps_backward(ring, glu, halo, grad, gain_part)
     mine = lax.all_to_all(terms, SP, 0, 0, tiled=True)
     mine = jnp.sum(mine, axis=0)
     mine = mine + shift(mine, CORE, 1)
+
+    closed = []
+    for axis, (low, high) in zip((Y, X), halves):
+        sent = ((1, low[1]), (2, high[0]), (3, high[1]))
+        got = tie([shift(block.astype(BF16), axis, k) for k, block in sent], mine)
+        closed.append(add(low[0], *got))
 
     scattered = jnp.concatenate(closed).reshape(8, lanes, lanes)
     merged = jnp.concatenate([scattered, jnp.broadcast_to(mine[None], (8, *mine.shape))], axis=1).astype(BF16)

time: 166 us -> 168 us (1.012)
  waiting for transfers between devices: 43.2 us -> 47.8 us
  starting transfers between devices: 51.4 us -> 47.5 us
  other arithmetic: 5.37 us -> 7.21 us
    all_to_all x1, waiting for transfers between devices: 0.01 us -> 4.45 us  [step(): mine = lax.all_to_all(terms, SP, 0, 0, tiled=True)]
    ppermute x1, starting transfers between devices: 2.97 us -> 0.93 us  [step(): lax.ppermute(grad_head, SP, [((i + 1) % 16, i) for i in range(16)])]
  transfers between devices with their start and end apart: 29 -> 29, of which waited for: 12 -> 13; matrix products, arithmetic and copies ran while one was open for 5% -> 5% of each run, Pallas kernels for 25% -> 25%
where the time goes in v4:
time: 168 us; the launch traced here: 167 us
  waiting for transfers between devices  47.8 us (28%)
  starting transfers between devices  47.5 us (28%)
  Pallas kernels  43.5 us (26%)
  between operations  14.4 us (9%)
  other arithmetic  7.21 us (4%)
  local copies, waits for them, and re-layouts  6.9 us (4%)
    ppermute x23, waiting for transfers between devices, shift(): lax.ppermute(value, axis, [(i, (i + amount) % count) for i in range(count)])  31.1 us
    ppermute x23, starting transfers between devices, shift(): lax.ppermute(value, axis, [(i, (i + amount) % count) for i in range(count)])  24.9 us
    pallas_call x1, Pallas kernels, forward(): call(forward_kernel, 'forward', (16 // GROUP,), [column(tokens), column(t...  10.9 us
    pallas_call x1, Pallas kernels, norm_backward(): call(norm_kernel, 'norm_backward', (8,), [whole(tokens, width), column(wi...  9.79 us
    pallas_call x1, Pallas kernels, input_backward(): call(input_kernel, 'input_backward', (16 // GROUP,), [column(tokens), col...  9.05 us
    all_to_all x1, starting transfers between devices, step(): merged = lax.all_to_all(merged, Z, 0, 0, tiled=True)  8.78 us
    ppermute x1, waiting for transfers between devices, step(): halo = lax.ppermute(glu_tail, SP, [(i, (i + 1) % 16) for i in range(16)])  7.48 us
    all_to_all x1, starting transfers between devices, from_everyone(): lax.all_to_all(jnp.broadcast_to(shard[None], (count, *shard.shape)), axis...  7.03 us
  transfers between devices with their start and end apart: 29, of which 13 were waited for; matrix products, arithmetic and copies ran while one was open for 5% of the time, Pallas kernels for 25%

profile of v4, /device:TPU:32, one launch (start us, length us, event | category | flops | bytes accessed | tf_op | source)
XLA Modules:
  0.0 167.3 jit_solution(13945178661728228075)
XLA Ops:
  9.4 7.0 %all-to-all-start = ((f32[16,32,128]{2,1,0:T(8,128)}), f32[16,32,128]{2,1,0:T(8,128)S(1)}, u32[]{:S(2)}, u32[]{:S(2)}) async-start(f32[16,32,128]{2,1,0:T(8,128)} %broadcast_in_dim.10), calls=%async_computation | async-start | bytes 524288 | tf_op jit(solution)/shard_map/all_to_all | solution.py:414
  16.4 1.1 fusion.10
  17.5 2.0 %collective-permute-start = (bf16[32,2048]{1,0:T(8,128)(2,1)S(1)}, bf16[32,2048]{1,0:T(8,128)(2,1)S(1)}, u32[]{:S(2)}, u32[]{:S(2)}) collective-permute-start(bf16[32,2048]{1,0:T(8,128)(2,1)S(1)} %fusion.10), channel_id=1, source_target_pairs={{0,16},{16,32},{32,48},{48,64},{64,80},{80,96},{96,112},{112,128},... | collective-permute-start | bytes 393224 | tf_op jit(solution)/shard_map/ppermute | solution.py:439
  20.1 7.5 %collective-permute-done.halo = bf16[32,2048]{1,0:T(8,128)(2,1)S(1)} collective-permute-done((bf16[32,2048]{1,0:T(8,128)(2,1)S(1)}, bf16[32,2048]{1,0:T(8,128)(2,1)S(1)}, u32[]{:S(2)}, u32[]{:S(2)}) %collective-permute-start) | collective-permute-done | bytes 131104 | tf_op jit(solution)/shard_map/ppermute | solution.py:439
  28.4 10.9 %shard_map.101 = (bf16[256,2048]{1,0:T(8,128)(2,1)}, bf16[256,2048]{1,0:T(8,128)(2,1)}, bf16[256,2048]{1,0:T(8,128)(2,1)}, f32[256,128]{1,0:T(8,128)}, f32[256,128]{1,0:T(8,128)}) custom-call(s32[4]{0:T(128)} %pad_add_fusion.ring, bf16[256,2048]{1,0:T(8,128)(2,1)} %bitcast.64, bf16[256,2048]{1,0:T(8,128)(2,1)} %bitcast.66, bf16[32,2048]{1,0:T(8,128)(2,1)} %copy-done.8, ...), custom_call_target="tpu_custom_call" | custom-call | flops 3250585600 | bytes 5242880 | tf_op jit(solution)/shard_map/pallas_call | solution.py:101
  39.4 1.7 shard_map.102
  41.7 1.7 %collective-permute-done.1.turned_other = bf16[8,128,256]{2,1,0:T(8,128)(2,1)S(1)} collective-permute-done((bf16[8,128,256]{2,1,0:T(8,128)(2,1)S(1)}, bf16[8,128,256]{2,1,0:T(8,128)(2,1)S(1)}, u32[]{:S(2)}, u32[]{:S(2)}) %collective-permute-start.1) | collective-permute-done | bytes 524320 | tf_op jit(solution)/shard_map/ppermute | solution.py:43
  43.4 1.2 copy-done.7
  44.6 1.9 %shard_map.104 = (bf16[4,512,128]{2,1,0:T(8,128)(2,1)S(1)}, bf16[4,512,128]{2,1,0:T(8,128)(2,1)S(1)}, bf16[4,512,128]{2,1,0:T(8,128)(2,1)S(1)}, bf16[4,512,128]{2,1,0:T(8,128)(2,1)S(1)}) custom-call(s32[4]{0:T(128)S(1)} %copy-done.4, bf16[8,128,256]{2,1,0:T(8,128)(2,1)S(1)} %get-tuple-element.40.turned, ...), custom_call_target="tpu_custom_call" | custom-call | flops 1073741824 | bytes 4194304 | tf_op jit(solution)/shard_map/pallas_call | solution.py:185
  46.6 2.0 %collective-permute-start.3 = (bf16[4,512,128]{2,1,0:T(8,128)(2,1)S(1)}, bf16[4,512,128]{2,1,0:T(8,128)(2,1)S(1)}, u32[]{:S(2)}, u32[]{:S(2)}) collective-permute-start(bf16[4,512,128]{2,1,0:T(8,128)(2,1)S(1)} %get-tuple-element.43), channel_id=1, source_target_pairs={{0,16},{16,32},{32,48},{48,0},{1,17},{17,33},{33,49},{49,1},{2,18}... | collective-permute-start | bytes 1572872 | tf_op jit(solution)/shard_map/ppermute | solution.py:43
  48.6 1.0 collective-permute-start.6
  49.7 1.0 collective-permute-start.5
  50.6 1.9 %shard_map.103 = (bf16[2,512,128]{2,1,0:T(8,128)(2,1)S(1)}, bf16[2,512,128]{2,1,0:T(8,128)(2,1)S(1)}, bf16[4,512,128]{2,1,0:T(8,128)(2,1)S(1)}, bf16[2,512,128]{...) custom-call(s32[4]{0:T(128)S(1)} %copy-done.4, ...), custom_call_target="tpu_custom_call" | custom-call | flops 1073741824 | bytes 4194304 | tf_op jit(solution)/shard_map/pallas_call | solution.py:185
  52.5 8.2 %collective-permute-done.4 = bf16[4,512,128]{2,1,0:T(8,128)(2,1)S(1)} collective-permute-done((bf16[4,512,128]{2,1,0:T(8,128)(2,1)S(1)}, bf16[4,512,128]{2,1,0:T(8,128)(2,1)S(1)}, u32[]{:S(2)}, u32[]{:S(2)}) %collective-permute-start.4) | collective-permute-done | bytes 524320 | tf_op jit(solution)/shard_map/ppermute | solution.py:43
  60.8 1.6 collective-permute-start.10
  63.0 0.8 add_convert_fusion.2
  63.9 1.4 collective-permute-start.16
  65.3 0.9 add_convert_fusion.3
  66.8 1.8 %collective-permute-done.10 = bf16[2,512,128]{2,1,0:T(8,128)(2,1)S(1)} collective-permute-done((bf16[2,512,128]{2,1,0:T(8,128)(2,1)S(1)}, bf16[2,512,128]{2,1,0:T(8,128)(2,1)S(1)}, u32[]{:S(2)}, u32[]{:S(2)}) %collective-permute-start.10) | collective-permute-done | bytes 262176 | tf_op jit(solution)/shard_map/ppermute | solution.py:43
  68.6 2.8 %collective-permute-done.8 = bf16[2,512,128]{2,1,0:T(8,128)(2,1)S(1)} collective-permute-done((bf16[2,512,128]{2,1,0:T(8,128)(2,1)S(1)}, bf16[2,512,128]{2,1,0:T(8,128)(2,1)S(1)}, u32[]{:S(2)}, u32[]{:S(2)}) %collective-permute-start.8) | collective-permute-done | bytes 262176 | tf_op jit(solution)/shard_map/ppermute | solution.py:43
  71.6 0.8 slice_bitcast_fusion.4
  72.3 1.0 collective-permute-start.11
  73.3 1.2 collective-permute-start.12
  75.2 0.8 collective-permute-start.9
  76.1 9.8 %shard_map.105 = (bf16[256,2048]{1,0:T(8,128)(2,1)S(1)}, bf16[32,2048]{1,0:T(8,128)(2,1)S(1)}, f32[16,128]{1,0:T(8,128)S(1)}) custom-call(s32[4]{0:T(128)S(1)} %copy-done.4, bf16[256,2048]{1,0:T(8,128)(2,1)} %bitcast.55, bf16[2048,2048]{1,0:T(8,128)(2,1)} %all-gather.2.cloned.1.call-done.weight, bf16[256,2048]{1,0:T(8,128)(2,1)} %get-tuple-element.35.conv, ...), custom_call_target="tpu_custom_call" | custom-call | flops 2147483648 | bytes 11534336 | tf_op jit(solution)/shard_map/pallas_call | solution.py:312
  85.9 6.7 %shard_map.107 = f32[16,48,128]{2,1,0:T(8,128)} custom-call(s32[4]{0:T(128)S(1)} %copy-done.4, bf16[256,2048]{1,0:T(8,128)(2,1)S(1)} %copy-done.10, bf16[32,2048]{1,0:T(8,128)(2,1)S(1)} %copy-done.9, bf16[256,2048]{1,0:T(8,128)(2,1)S(1)} %get-tuple-element.51.grad, f32[16,128]{1,0:T(8,128)S(1)} %get-tuple-element.57.gain_part), custom_call_target="tpu_custom_call" | custom-call | flops 3250585600 | bytes 2097152 | tf_op jit(solution)/shard_map/pallas_call | solution.py:359
  92.6 3.9 %all-to-all-start.1 = ((f32[16,48,128]{2,1,0:T(8,128)}), f32[16,48,128]{2,1,0:T(8,128)S(1)}, u32[]{:S(2)}, u32[]{:S(2)}) async-start(f32[16,48,128]{2,1,0:T(8,128)} %shard_map.107), calls=%async_computation.1 | async-start | bytes 786432 | tf_op jit(solution)/shard_map/all_to_all | solution.py:460
  96.5 1.4 add_convert_fusion
  97.9 3.5 %collective-permute-start.17 = (bf16[512,128]{1,0:T(8,128)(2,1)S(1)}, bf16[512,128]{1,0:T(8,128)(2,1)S(1)}, u32[]{:S(2)}, u32[]{:S(2)}) collective-permute-start(bf16[512,128]{1,0:T(8,128)(2,1)S(1)} %get-tuple-element.74), channel_id=1, source_target_pairs={{0,32},{16,48},{32,0},{48,16},{1,33},{17,49},{33,1},{49,17},{2,34}... | collective-permute-start | bytes 393224 | tf_op jit(solution)/shard_map/ppermute | solution.py:43
  101.4 4.4 %all-to-all-done.1 = f32[16,48,128]{2,1,0:T(8,128)S(1)} async-done(((f32[16,48,128]{2,1,0:T(8,128)}), f32[16,48,128]{2,1,0:T(8,128)S(1)}, u32[]{:S(2)}, u32[]{:S(2)}) %all-to-all-start.1) | async-done | bytes 393248 | tf_op jit(solution)/shard_map/all_to_all | solution.py:460
  106.0 1.5 collective-permute-start.18
  108.2 3.8 %collective-permute-done.18 = bf16[512,128]{1,0:T(8,128)(2,1)S(1)} collective-permute-done((bf16[512,128]{1,0:T(8,128)(2,1)S(1)}, bf16[512,128]{1,0:T(8,128)(2,1)S(1)}, u32[]{:S(2)}, u32[]{:S(2)}) %collective-permute-start.18) | collective-permute-done | bytes 131104 | tf_op jit(solution)/shard_map/ppermute | solution.py:43
  112.0 2.4 %collective-permute-done.15 = bf16[512,128]{1,0:T(8,128)(2,1)S(1)} collective-permute-done((bf16[512,128]{1,0:T(8,128)(2,1)S(1)}, bf16[512,128]{1,0:T(8,128)(2,1)S(1)}, u32[]{:S(2)}, u32[]{:S(2)}) %collective-permute-start.15) | collective-permute-done | bytes 131104 | tf_op jit(solution)/shard_map/ppermute | solution.py:43
  114.4 1.2 fusion.3
  115.6 0.8 pad_maximum_fusion
  116.4 8.8 %all-to-all-start.2 = ((bf16[8,176,128]{2,1,0:T(8,128)(2,1)}), bf16[8,176,128]{2,1,0:T(8,128)(2,1)S(1)}, u32[]{:S(2)}, u32[]{:S(2)}) async-start(bf16[8,176,128]{2,1,0:T(8,128)(2,1)} %pad_maximum_fusion), calls=%async_computation.2 | async-start | bytes 720896 | tf_op jit(solution)/shard_map/all_to_all | solution.py:472
  125.2 0.9 collective-permute-start.7
  126.1 4.0 %collective-permute-done.7.tail = bf16[32,2048]{1,0:T(8,128)(2,1)S(1)} collective-permute-done((bf16[32,2048]{1,0:T(8,128)(2,1)S(1)}, bf16[32,2048]{1,0:T(8,128)(2,1)S(1)}, u32[]{:S(2)}, u32[]{:S(2)}) %collective-permute-start.7) | collective-permute-done | bytes 131104 | tf_op jit(solution)/shard_map/ppermute | solution.py:457
  130.8 9.1 %shard_map.106 = (bf16[256,2048]{1,0:T(8,128)(2,1)}, bf16[256,2048]{1,0:T(8,128)(2,1)}) custom-call(s32[4]{0:T(128)} %pad_add_fusion.ring, bf16[256,2048]{1,0:T(8,128)(2,1)} %copy-done.6, bf16[32,2048]{1,0:T(8,128)(2,1)} %copy-done.16, f32[16,32,128]{2,1,0:T(8,128)} %copy-done.15, bf16[256,2048]{1,0:T(8,128)(2,1)} %bitcast.65, bf16[256,2048]{1,0:T(8,128)(2,1)} %bitcast.67), custom_call_target="tpu_custom_call" | custom-call | flops 3250585600 | bytes 5242880 | tf_op jit(solution)/shard_map/pallas_call | solution.py:393
  139.9 2.5 %collective-permute-start.19 = (bf16[128,128]{1,0:T(8,128)(2,1)S(1)}, bf16[128,128]{1,0:T(8,128)(2,1)S(1)}, u32[]{:S(2)}, u32[]{:S(2)}) collective-permute-start(bf16[128,128]{1,0:T(8,128)(2,1)S(1)} %get-tuple-element.66), channel_id=1, source_target_pairs={{0,48},{16,0},{32,16},{48,32},{1,49},{17,1},{33,17},{49,33},{2,50}... | collective-permute-start | bytes 98312 | tf_op jit(solution)/shard_map/ppermute | solution.py:43
  142.4 1.2 collective-permute-start.21
  144.1 3.7 %collective-permute-done.20 = bf16[128,128]{1,0:T(8,128)(2,1)S(1)} collective-permute-done((bf16[128,128]{1,0:T(8,128)(2,1)S(1)}, bf16[128,128]{1,0:T(8,128)(2,1)S(1)}, u32[]{:S(2)}, u32[]{:S(2)}) %collective-permute-start.20) | collective-permute-done | bytes 32800 | tf_op jit(solution)/shard_map/ppermute | solution.py:43
  147.9 2.5 %collective-permute-start.22 = (bf16[4,128,128]{2,1,0:T(8,128)(2,1)S(1)}, bf16[4,128,128]{2,1,0:T(8,128)(2,1)S(1)}, u32[]{:S(2)}, u32[]{:S(2)}) collective-permute-start(bf16[4,128,128]{2,1,0:T(8,128)(2,1)S(1)} %pad_maximum_fusion.2), channel_id=1, source_target_pairs={{0,192},{64,0},{128,64},{192,128},{1,193},{65,1},{129,65},{193,129... | collective-permute-start | bytes 393224 | tf_op jit(solution)/shard_map/ppermute | solution.py:43
  150.6 0.7 collective-permute-start.24
  151.3 2.9 %collective-permute-done.22 = bf16[4,128,128]{2,1,0:T(8,128)(2,1)S(1)} collective-permute-done((bf16[4,128,128]{2,1,0:T(8,128)(2,1)S(1)}, bf16[4,128,128]{2,1,0:T(8,128)(2,1)S(1)}, u32[]{:S(2)}, u32[]{:S(2)}) %collective-permute-start.22) | collective-permute-done | bytes 131104 | tf_op jit(solution)/shard_map/ppermute | solution.py:43
  154.3 2.6 %collective-permute-done.23 = bf16[4,128,128]{2,1,0:T(8,128)(2,1)S(1)} collective-permute-done((bf16[4,128,128]{2,1,0:T(8,128)(2,1)S(1)}, bf16[4,128,128]{2,1,0:T(8,128)(2,1)S(1)}, u32[]{:S(2)}, u32[]{:S(2)}) %collective-permute-start.23) | collective-permute-done | bytes 131104 | tf_op jit(solution)/shard_map/ppermute | solution.py:43
  157.0 1.2 collective-permute-done.24
  158.8 1.6 shard_map.108
  (84 shorter events, 9.6 us)
Async XLA Ops:
  7.2 32.2 %copy-start = (bf16[1,256,2048]{2,1,0:T(8,128)(2,1)S(1)}, bf16[1,256,2048]{2,1,0:T(8,128)(2,1)}, u32[]{:S(2)}) copy-start(bf16[1,256,2048]{2,1,0:T(8,128)(2,1)} %param.8) | copy-start | bytes 3145732
  7.2 68.9 %all-gather.2.cloned.1.call-start = ((), (), s32[]{:S(2)}) async-start(), calls=%async_computation.3 | async-start | bytes 8912896 | tf_op jit(solution)/shard_map/all_gather | solution.py:436
  9.4 18.2 %all-to-all-start = ((f32[16,32,128]{2,1,0:T(8,128)}), f32[16,32,128]{2,1,0:T(8,128)S(1)}, u32[]{:S(2)}, u32[]{:S(2)}) async-start(f32[16,32,128]{2,1,0:T(8,128)} %broadcast_in_dim.10), calls=%async_computation | async-start | bytes 524288 | tf_op jit(solution)/shard_map/all_to_all | solution.py:414
  17.5 10.1 %collective-permute-start = (bf16[32,2048]{1,0:T(8,128)(2,1)S(1)}, bf16[32,2048]{1,0:T(8,128)(2,1)S(1)}, u32[]{:S(2)}, u32[]{:S(2)}) collective-permute-start(bf16[32,2048]{1,0:T(8,128)(2,1)S(1)} %fusion.10), channel_id=1, source_target_pairs={{0,16},{16,32},{32,48},{48,64},{64,80},{80,96},{96,112},{112,128},... | collective-permute-start | bytes 393224 | tf_op jit(solution)/shard_map/ppermute | solution.py:439
  20.1 19.3 %copy-start.4 = (s32[4]{0:T(128)S(1)}, s32[4]{0:T(128)}, u32[]{:S(2)}) copy-start(s32[4]{0:T(128)} %pad_add_fusion.ring) | copy-start | bytes 52
  27.6 0.6 copy-start.8
  27.6 0.8 copy-start.15
  39.3 36.8 %copy-start.1 = (f32[256,128]{1,0:T(8,128)S(1)}, f32[256,128]{1,0:T(8,128)}, u32[]{:S(2)}) copy-start(f32[256,128]{1,0:T(8,128)} %get-tuple-element.36.mean) | copy-start | bytes 393220
  39.3 36.8 %copy-start.2 = (f32[256,128]{1,0:T(8,128)S(1)}, f32[256,128]{1,0:T(8,128)}, u32[]{:S(2)}) copy-start(f32[256,128]{1,0:T(8,128)} %get-tuple-element.37.inv) | copy-start | bytes 393220
  39.3 36.8 %copy-start.3 = (f32[2048]{0:T(1024)S(1)}, f32[2048]{0:T(1024)}, u32[]{:S(2)}) copy-start(f32[2048]{0:T(1024)} %param.10) | copy-start | bytes 24580
  39.3 4.1 %collective-permute-start.2 = (bf16[256,2048]{1,0:T(8,128)(2,1)}, bf16[256,2048]{1,0:T(8,128)(2,1)S(1)}, u32[]{:S(2)}, u32[]{:S(2)}) collective-permute-start(bf16[256,2048]{1,0:T(8,128)(2,1)} %get-tuple-element.38.act), channel_id=1, source_target_pairs={{0,1},{1,0},{2,3},{3,2},{4,5},{5,4},{6,7},{7,6},{8,9},{9,8},{10,11... | collective-permute-start | bytes 3145736 | tf_op jit(solution)/shard_map/ppermute | solution.py:43
  41.1 2.3 %collective-permute-start.1 = (bf16[8,128,256]{2,1,0:T(8,128)(2,1)S(1)}, bf16[8,128,256]{2,1,0:T(8,128)(2,1)S(1)}, u32[]{:S(2)}, u32[]{:S(2)}) collective-permute-start(bf16[8,128,256]{2,1,0:T(8,128)(2,1)S(1)} %get-tuple-element.41), channel_id=1, source_target_pairs={{0,1},{1,0},{2,3},{3,2},{4,5},{5,4},{6,7},{7,6},{8,9},{9,8},{10,11... | collective-permute-start | bytes 1572872 | tf_op jit(solution)/shard_map/ppermute | solution.py:43
  43.4 1.2 copy-start.7
  46.5 14.2 %collective-permute-start.4 = (bf16[4,512,128]{2,1,0:T(8,128)(2,1)S(1)}, bf16[4,512,128]{2,1,0:T(8,128)(2,1)S(1)}, u32[]{:S(2)}, u32[]{:S(2)}) collective-permute-start(bf16[4,512,128]{2,1,0:T(8,128)(2,1)S(1)} %get-tuple-element.45), channel_id=1, source_target_pairs={{0,48},{16,0},{32,16},{48,32},{1,49},{17,1},{33,17},{49,33},{2,50}... | collective-permute-start | bytes 1572872 | tf_op jit(solution)/shard_map/ppermute | solution.py:43
  46.6 15.8 %collective-permute-start.3 = (bf16[4,512,128]{2,1,0:T(8,128)(2,1)S(1)}, bf16[4,512,128]{2,1,0:T(8,128)(2,1)S(1)}, u32[]{:S(2)}, u32[]{:S(2)}) collective-permute-start(bf16[4,512,128]{2,1,0:T(8,128)(2,1)S(1)} %get-tuple-element.43), channel_id=1, source_target_pairs={{0,16},{16,32},{32,48},{48,0},{1,17},{17,33},{33,49},{49,1},{2,18}... | collective-permute-start | bytes 1572872 | tf_op jit(solution)/shard_map/ppermute | solution.py:43
  48.6 14.4 %collective-permute-start.6 = (bf16[4,512,128]{2,1,0:T(8,128)(2,1)S(1)}, bf16[4,512,128]{2,1,0:T(8,128)(2,1)S(1)}, u32[]{:S(2)}, u32[]{:S(2)}) collective-permute-start(bf16[4,512,128]{2,1,0:T(8,128)(2,1)S(1)} %get-tuple-element.49), channel_id=1, source_target_pairs={{0,192},{64,0},{128,64},{192,128},{1,193},{65,1},{129,65},{193,129... | collective-permute-start | bytes 1572872 | tf_op jit(solution)/shard_map/ppermute | solution.py:43
  49.7 15.7 %collective-permute-start.5 = (bf16[4,512,128]{2,1,0:T(8,128)(2,1)S(1)}, bf16[4,512,128]{2,1,0:T(8,128)(2,1)S(1)}, u32[]{:S(2)}, u32[]{:S(2)}) collective-permute-start(bf16[4,512,128]{2,1,0:T(8,128)(2,1)S(1)} %get-tuple-element.47), channel_id=1, source_target_pairs={{0,64},{64,128},{128,192},{192,0},{1,65},{65,129},{129,193},{193,1... | collective-permute-start | bytes 1572872 | tf_op jit(solution)/shard_map/ppermute | solution.py:43
  60.7 25.2 %copy-start.9 = (bf16[32,2048]{1,0:T(8,128)(2,1)S(1)}, bf16[32,2048]{1,0:T(8,128)(2,1)}, u32[]{:S(2)}) copy-start(bf16[32,2048]{1,0:T(8,128)(2,1)} %copy-done.8) | copy-start | bytes 393220
  60.7 25.2 %copy-start.10 = (bf16[256,2048]{1,0:T(8,128)(2,1)S(1)}, bf16[256,2048]{1,0:T(8,128)(2,1)}, u32[]{:S(2)}) copy-start(bf16[256,2048]{1,0:T(8,128)(2,1)} %get-tuple-element.56.glu) | copy-start | bytes 3145732
  60.8 7.8 %collective-permute-start.10 = (bf16[2,512,128]{2,1,0:T(8,128)(2,1)S(1)}, bf16[2,512,128]{2,1,0:T(8,128)(2,1)S(1)}, u32[]{:S(2)}, u32[]{:S(2)}) collective-permute-start(bf16[2,512,128]{2,1,0:T(8,128)(2,1)S(1)} %add_convert_fusion.4), channel_id=1, source_target_pairs={{0,48},{16,0},{32,16},{48,32},{1,49},{17,1},{33,17},{49,33},{2,50}... | collective-permute-start | bytes 786440 | tf_op jit(solution)/shard_map/ppermute | solution.py:43
  62.4 8.9 %collective-permute-start.8 = (bf16[2,512,128]{2,1,0:T(8,128)(2,1)S(1)}, bf16[2,512,128]{2,1,0:T(8,128)(2,1)S(1)}, u32[]{:S(2)}, u32[]{:S(2)}) collective-permute-start(bf16[2,512,128]{2,1,0:T(8,128)(2,1)S(1)} %add_convert_fusion.5), channel_id=1, source_target_pairs={{0,16},{16,32},{32,48},{48,0},{1,17},{17,33},{33,49},{49,1},{2,18}... | collective-permute-start | bytes 786440 | tf_op jit(solution)/shard_map/ppermute | solution.py:43
  63.0 8.3 %copy-start.13 = (bf16[4,512,128]{2,1,0:T(8,128)(2,1)}, bf16[4,512,128]{2,1,0:T(8,128)(2,1)S(1)}, u32[]{:S(2)}) copy-start(bf16[4,512,128]{2,1,0:T(8,128)(2,1)S(1)} %collective-permute-done.6) | copy-start | bytes 1572868
  63.9 32.6 %collective-permute-start.16 = (bf16[2,512,128]{2,1,0:T(8,128)(2,1)}, bf16[2,512,128]{2,1,0:T(8,128)(2,1)}, u32[]{:S(2)}, u32[]{:S(2)}) collective-permute-start(bf16[2,512,128]{2,1,0:T(8,128)(2,1)} %add_convert_fusion.2), channel_id=1, source_target_pairs={{0,192},{64,0},{128,64},{192,128},{1,193},{65,1},{129,65},{193,129... | collective-permute-start | bytes 786440 | tf_op jit(solution)/shard_map/ppermute | solution.py:43
  65.3 10.7 %copy-start.14 = (bf16[4,512,128]{2,1,0:T(8,128)(2,1)}, bf16[4,512,128]{2,1,0:T(8,128)(2,1)S(1)}, u32[]{:S(2)}) copy-start(bf16[4,512,128]{2,1,0:T(8,128)(2,1)S(1)} %collective-permute-done.5) | copy-start | bytes 1572868
  66.2 30.3 %collective-permute-start.14 = (bf16[2,512,128]{2,1,0:T(8,128)(2,1)}, bf16[2,512,128]{2,1,0:T(8,128)(2,1)}, u32[]{:S(2)}, u32[]{:S(2)}) collective-permute-start(bf16[2,512,128]{2,1,0:T(8,128)(2,1)} %add_convert_fusion.3), channel_id=1, source_target_pairs={{0,64},{64,128},{128,192},{192,0},{1,65},{65,129},{129,193},{193,1... | collective-permute-start | bytes 786440 | tf_op jit(solution)/shard_map/ppermute | solution.py:43
  71.6 4.5 %copy-start.11 = (f32[2,512,128]{2,1,0:T(8,128)}, f32[2,512,128]{2,1,0:T(8,128)S(1)}, u32[]{:S(2)}) copy-start(f32[2,512,128]{2,1,0:T(8,128)S(1)} %get-tuple-element.68) | copy-start | bytes 1572868
  72.3 33.7 %collective-permute-start.11 = (bf16[512,128]{1,0:T(8,128)(2,1)}, bf16[512,128]{1,0:T(8,128)(2,1)}, u32[]{:S(2)}, u32[]{:S(2)}) collective-permute-start(bf16[512,128]{1,0:T(8,128)(2,1)} %get-tuple-element.72), channel_id=1, source_target_pairs={{0,128},{64,192},{128,0},{192,64},{1,129},{65,193},{129,1},{193,65... | collective-permute-start | bytes 393224 | tf_op jit(solution)/shard_map/ppermute | solution.py:43
  73.3 34.8 %collective-permute-start.12 = (bf16[512,128]{1,0:T(8,128)(2,1)}, bf16[512,128]{1,0:T(8,128)(2,1)}, u32[]{:S(2)}, u32[]{:S(2)}) collective-permute-start(bf16[512,128]{1,0:T(8,128)(2,1)} %get-tuple-element.71), channel_id=1, source_target_pairs={{0,192},{64,0},{128,64},{192,128},{1,193},{65,1},{129,65},{193,129... | collective-permute-start | bytes 393224 | tf_op jit(solution)/shard_map/ppermute | solution.py:43
  75.2 33.0 %collective-permute-start.9 = (bf16[512,128]{1,0:T(8,128)(2,1)}, bf16[512,128]{1,0:T(8,128)(2,1)}, u32[]{:S(2)}, u32[]{:S(2)}) collective-permute-start(bf16[512,128]{1,0:T(8,128)(2,1)} %fusion.8), channel_id=1, source_target_pairs={{0,64},{64,128},{128,192},{192,0},{1,65},{65,129},{129,193},{193,1... | collective-permute-start | bytes 393224 | tf_op jit(solution)/shard_map/ppermute | solution.py:43
  85.9 29.7 %copy-start.6 = (bf16[256,2048]{1,0:T(8,128)(2,1)}, bf16[256,2048]{1,0:T(8,128)(2,1)S(1)}, u32[]{:S(2)}) copy-start(bf16[256,2048]{1,0:T(8,128)(2,1)S(1)} %get-tuple-element.51.grad) | copy-start | bytes 3145732
  85.9 28.5 %copy-start.12 = (f32[2,512,128]{2,1,0:T(8,128)S(1)}, f32[2,512,128]{2,1,0:T(8,128)}, u32[]{:S(2)}) copy-start(f32[2,512,128]{2,1,0:T(8,128)} %copy-done.11) | copy-start | bytes 1572868
  92.6 13.3 %all-to-all-start.1 = ((f32[16,48,128]{2,1,0:T(8,128)}), f32[16,48,128]{2,1,0:T(8,128)S(1)}, u32[]{:S(2)}, u32[]{:S(2)}) async-start(f32[16,48,128]{2,1,0:T(8,128)} %shard_map.107), calls=%async_computation.1 | async-start | bytes 786432 | tf_op jit(solution)/shard_map/all_to_all | solution.py:460
  97.9 10.3 %collective-permute-start.17 = (bf16[512,128]{1,0:T(8,128)(2,1)S(1)}, bf16[512,128]{1,0:T(8,128)(2,1)S(1)}, u32[]{:S(2)}, u32[]{:S(2)}) collective-permute-start(bf16[512,128]{1,0:T(8,128)(2,1)S(1)} %get-tuple-element.74), channel_id=1, source_target_pairs={{0,32},{16,48},{32,0},{48,16},{1,33},{17,49},{33,1},{49,17},{2,34}... | collective-permute-start | bytes 393224 | tf_op jit(solution)/shard_map/ppermute | solution.py:43
  105.9 1.7 collective-permute-start.13
  106.0 6.0 %collective-permute-start.18 = (bf16[512,128]{1,0:T(8,128)(2,1)S(1)}, bf16[512,128]{1,0:T(8,128)(2,1)S(1)}, u32[]{:S(2)}, u32[]{:S(2)}) collective-permute-start(bf16[512,128]{1,0:T(8,128)(2,1)S(1)} %get-tuple-element.73), channel_id=1, source_target_pairs={{0,48},{16,0},{32,16},{48,32},{1,49},{17,1},{33,17},{49,33},{2,50}... | collective-permute-start | bytes 393224 | tf_op jit(solution)/shard_map/ppermute | solution.py:43
  107.5 6.8 %collective-permute-start.15 = (bf16[512,128]{1,0:T(8,128)(2,1)S(1)}, bf16[512,128]{1,0:T(8,128)(2,1)S(1)}, u32[]{:S(2)}, u32[]{:S(2)}) collective-permute-start(bf16[512,128]{1,0:T(8,128)(2,1)S(1)} %fusion.9), channel_id=1, source_target_pairs={{0,16},{16,32},{32,48},{48,0},{1,17},{17,33},{33,49},{49,1},{2,18}... | collective-permute-start | bytes 393224 | tf_op jit(solution)/shard_map/ppermute | solution.py:43
  108.2 50.6 %copy-start.5 = (s32[4]{0:T(128)S(1)}, s32[4]{0:T(128)}, u32[]{:S(2)}) copy-start(s32[4]{0:T(128)} %pad_add_fusion.ring) | copy-start | bytes 52
  116.4 23.4 %all-to-all-start.2 = ((bf16[8,176,128]{2,1,0:T(8,128)(2,1)}), bf16[8,176,128]{2,1,0:T(8,128)(2,1)S(1)}, u32[]{:S(2)}, u32[]{:S(2)}) async-start(bf16[8,176,128]{2,1,0:T(8,128)(2,1)} %pad_maximum_fusion), calls=%async_computation.2 | async-start | bytes 720896 | tf_op jit(solution)/shard_map/all_to_all | solution.py:472
  125.2 5.0 %collective-permute-start.7 = (bf16[32,2048]{1,0:T(8,128)(2,1)S(1)}, bf16[32,2048]{1,0:T(8,128)(2,1)S(1)}, u32[]{:S(2)}, u32[]{:S(2)}) collective-permute-start(bf16[32,2048]{1,0:T(8,128)(2,1)S(1)} %get-tuple-element.52), channel_id=1, source_target_pairs={{16,0},{32,16},{48,32},{64,48},{80,64},{96,80},{112,96},{128,112},... | collective-permute-start | bytes 393224 | tf_op jit(solution)/shard_map/ppermute | solution.py:457
  130.1 0.6 copy-start.16
  139.9 4.2 %collective-permute-start.19 = (bf16[128,128]{1,0:T(8,128)(2,1)S(1)}, bf16[128,128]{1,0:T(8,128)(2,1)S(1)}, u32[]{:S(2)}, u32[]{:S(2)}) collective-permute-start(bf16[128,128]{1,0:T(8,128)(2,1)S(1)} %get-tuple-element.66), channel_id=1, source_target_pairs={{0,48},{16,0},{32,16},{48,32},{1,49},{17,1},{33,17},{49,33},{2,50}... | collective-permute-start | bytes 98312 | tf_op jit(solution)/shard_map/ppermute | solution.py:43
  142.4 5.5 %collective-permute-start.20 = (bf16[128,128]{1,0:T(8,128)(2,1)S(1)}, bf16[128,128]{1,0:T(8,128)(2,1)S(1)}, u32[]{:S(2)}, u32[]{:S(2)}) collective-permute-start(bf16[128,128]{1,0:T(8,128)(2,1)S(1)} %get-tuple-element.66), channel_id=1, source_target_pairs={{0,32},{16,48},{32,0},{48,16},{1,33},{17,49},{33,1},{49,17},{2,34}... | collective-permute-start | bytes 98312 | tf_op jit(solution)/shard_map/ppermute | solution.py:43
  142.4 5.5 %collective-permute-start.21 = (bf16[128,128]{1,0:T(8,128)(2,1)S(1)}, bf16[128,128]{1,0:T(8,128)(2,1)S(1)}, u32[]{:S(2)}, u32[]{:S(2)}) collective-permute-start(bf16[128,128]{1,0:T(8,128)(2,1)S(1)} %get-tuple-element.66), channel_id=1, source_target_pairs={{0,16},{16,32},{32,48},{48,0},{1,17},{17,33},{33,49},{49,1},{2,18}... | collective-permute-start | bytes 98312 | tf_op jit(solution)/shard_map/ppermute | solution.py:43
  147.9 6.4 %collective-permute-start.22 = (bf16[4,128,128]{2,1,0:T(8,128)(2,1)S(1)}, bf16[4,128,128]{2,1,0:T(8,128)(2,1)S(1)}, u32[]{:S(2)}, u32[]{:S(2)}) collective-permute-start(bf16[4,128,128]{2,1,0:T(8,128)(2,1)S(1)} %pad_maximum_fusion.2), channel_id=1, source_target_pairs={{0,192},{64,0},{128,64},{192,128},{1,193},{65,1},{129,65},{193,129... | collective-permute-start | bytes 393224 | tf_op jit(solution)/shard_map/ppermute | solution.py:43
  150.4 6.6 %collective-permute-start.23 = (bf16[4,128,128]{2,1,0:T(8,128)(2,1)S(1)}, bf16[4,128,128]{2,1,0:T(8,128)(2,1)S(1)}, u32[]{:S(2)}, u32[]{:S(2)}) collective-permute-start(bf16[4,128,128]{2,1,0:T(8,128)(2,1)S(1)} %pad_maximum_fusion.2), channel_id=1, source_target_pairs={{0,128},{64,192},{128,0},{192,64},{1,129},{65,193},{129,1},{193,65... | collective-permute-start | bytes 393224 | tf_op jit(solution)/shard_map/ppermute | solution.py:43
  150.6 7.6 %collective-permute-start.24 = (bf16[4,128,128]{2,1,0:T(8,128)(2,1)S(1)}, bf16[4,128,128]{2,1,0:T(8,128)(2,1)S(1)}, u32[]{:S(2)}, u32[]{:S(2)}) collective-permute-start(bf16[4,128,128]{2,1,0:T(8,128)(2,1)S(1)} %pad_maximum_fusion.2), channel_id=1, source_target_pairs={{0,64},{64,128},{128,192},{192,0},{1,65},{65,129},{129,193},{193,1... | collective-permute-start | bytes 393224 | tf_op jit(solution)/shard_map/ppermute | solution.py:43
Sparse Core Ops, SparseCore 0:
  9.8 56.6 all-gather.1
